TPU v7x, 256 devices: a whole 4x4x8 slice. The times are simulated.
256 devices in a mesh: ep: 64 (over z, x, core), tp: 4 (over y).
Axes of the slice: x: 4, y: 4, z: 8, core: 2. Of those that a mesh axis runs over, the one named last changes fastest.
Arguments:
- memory_query_matrix: bfloat16 [32768, 1024], P('ep', 'tp'), may hold values from -0.59765625 to 2
- memory_key_matrix: bfloat16 [32768, 1024], P('ep', 'tp'), may hold values from -0.59765625 to 2
- memory_value_matrix: bfloat16 [32768, 1024], P('ep', 'tp'), may hold values from -6 to 6
- input_gate_logits: float32 [4, 32768], P('tp', 'ep'), may hold values from -6 to 260
- forget_gate_logits: float32 [4, 32768], P('tp', 'ep'), may hold values from -1 to 20
- forget_log_boosts: float32 [4, 32768], P('tp', 'ep'), may hold values from -0.7 to 0
- head_norm_scale: float32 [1024], P('tp'), may hold values from 0.1 to 1.9
- memory_output_matrix: bfloat16 [1024, 2048], replicated, may hold values from -0.1875 to 0.1875
- projection_norm_scale: float32 [2048], replicated, may hold values from 0.1 to 1.9
- second_batch_rows: bfloat16 [49152, 2048], P(('ep', 'tp')), may hold values from -6 to 6
- expert_prenorm_scale: float32 [2048], replicated, may hold values from 0.1 to 1.9
- selected_expert_index: int32 [49152, 2], P(('ep', 'tp')), may hold values from 0 to 63, all different within a row; in each aligned block of 192 rows (0 to 191, 192 to 383, ...) at most 12 rows name the same one
- group_route_probability: float32 [49152], P(('ep', 'tp')), may hold values from 0.2 to 1
- expert_choice_scores: float32 [49152, 2], P(('ep', 'tp')), may hold values from -6 to 6
- expert_gate_matrix: bfloat16 [64, 2048, 512], P('ep'), may hold values from -0.125 to 0.125
- expert_up_matrix: bfloat16 [64, 2048, 512], P('ep'), may hold values from -0.125 to 0.125
- expert_down_matrix: bfloat16 [64, 512, 2048], P('ep'), may hold values from -0.25 to 0.25
Outputs:
- mixed_rows: bfloat16 [32768, 2048], P(('ep', 'tp'))
- routed_rows: bfloat16 [49152, 2048], P(('ep', 'tp'))
Inputs may be any that keep to these rules, and one draw needn't show every extreme that they name: `selected_expert_index`: each row names 2 different experts; among the rows of one device no expert is named more than 12 times, and in some device one expert is named exactly that often.
All inputs are finite; a program needn't handle non-finite values.
Results may differ from a plain program's by a relative error of at most 0.013.
Values may be sent and summed in bfloat16 or wider, within the bound.
No kernel may reach another device: no remote copies, remote signals or barrier semaphores. Data moves between devices by JAX's collectives and lax.ppermute only.
A program may use at most 128 MiB of HBM per device.

v0:
```python
import jax
import jax.numpy as jnp
from jax import lax
from jax.sharding import Mesh
from jax.sharding import PartitionSpec as P

SPAN = 128
EP = ("ep_0", "ep_1", "ep_2")
EP_TP = ("ep_0", "ep_1", "ep_2", "tp")


floor_log = -1e30
norm_eps = 1e-06


def neutral_like(array, identity):
    return jax.tree.map(
        lambda part, zero: jnp.zeros_like(part) + jnp.asarray(zero, part.dtype), array, identity
    )


def collected_together(array, axis):
    leaves = jax.tree.leaves(array)
    order = sorted(range(len(leaves)), key=lambda k: -leaves[k].size)
    width = (1, *leaves[order[0]].shape)[-1]
    lines = [
        jnp.pad(leaves[k].reshape(-1), (0, -leaves[k].size % width)).reshape(-1, width)
        for k in order
    ]
    both, at, found = (lax.all_gather(jnp.concatenate(lines), axis), 0, {})
    for k, line in zip(order, lines):
        piece = both[:, at : at + len(line)].reshape(len(both), -1)
        found[k] = piece[:, : leaves[k].size].reshape(-1, *leaves[k].shape)
        at += len(line)
    numbers = iter(range(len(leaves)))
    return jax.tree.map(lambda _: found[next(numbers)], array)


def entering_2(array, axes, combine, identity):
    before = start = neutral_like(array, identity)
    subtotal = array
    for axis in reversed(axes):
        devices, position = (lax.axis_size(axis), lax.axis_index(axis))
        pieces = collected_together(subtotal, axis)
        inside, subtotal = (start, start)
        for k in range(devices):
            passed = k < position
            subtotal = combine(subtotal, jax.tree.map(lambda part: part[k], pieces))
            inside = jax.tree.map(lambda new, old: jnp.where(passed, new, old), subtotal, inside)
        before = combine(inside, before)
    return before


def cut_along(array, dim, devices):
    before, after = (array.shape[:dim], array.shape[dim + 1 :])
    return jnp.moveaxis(array.reshape(*before, devices, -1, *after), dim, 0)


def sent_and_summed(array, axis, dim):
    pieces = cut_along(array, dim, lax.axis_size(axis))
    arrived = lax.all_to_all(pieces, axis, split_axis=0, concat_axis=0, tiled=True)
    return arrived.astype(jnp.float32).sum(axis=0)


def rms_scale(values, gain):
    squares = jnp.mean(values * values, axis=-1, keepdims=True)
    return values * lax.rsqrt(squares + norm_eps) * gain


def span_step(carry, inputs):
    memory, normer, stabil = carry
    query, keyrow, valrow, in_gate, log_retain_factor = inputs
    key_scale = query.shape[-1] ** (-0.5)
    length = query.shape[1]
    causal = jnp.tril(jnp.ones((length, length), dtype=bool))
    cumulative = jnp.cumsum(log_retain_factor, axis=-1)
    decay_map = cumulative[:, :, None] - cumulative[:, None, :] + in_gate[:, None, :]
    decay_map = jnp.where(causal[None], decay_map, -jnp.inf)
    carried = cumulative + stabil[:, None]
    peak = jnp.maximum(carried, jnp.max(decay_map, axis=-1))
    within = jnp.exp(decay_map - peak[:, :, None])
    across = jnp.exp(carried - peak)
    products = jnp.einsum("htd,hsd->hts", query, keyrow, preferred_element_type=jnp.float32)
    scores = products * key_scale * within
    qfloat = query.astype(jnp.float32)
    denominator = jnp.sum(scores, axis=-1) + across * jnp.einsum("hd,htd->ht", normer, qfloat)
    weights = scores.astype(jnp.bfloat16)
    numerator = jnp.einsum("hts,hsd->htd", weights, valrow, preferred_element_type=jnp.float32)
    numerator = numerator + across[:, :, None] * jnp.einsum("hed,htd->hte", memory, qfloat)
    output = numerator / jnp.maximum(jnp.abs(denominator), jnp.exp(-peak))[:, :, None]
    span_end = cumulative[:, -1]
    gap_log = span_end[:, None] - cumulative + in_gate
    new_peak = jnp.maximum(span_end + stabil, jnp.max(gap_log, axis=-1))
    shrink = jnp.exp(span_end + stabil - new_peak)
    spread = jnp.exp(gap_log - new_peak[:, None]) * key_scale
    keys_weighted = keyrow.astype(jnp.float32) * spread[:, :, None]
    memory = shrink[:, None, None] * memory + jnp.einsum(
        "hse,hsd->hed", valrow.astype(jnp.float32), keys_weighted
    )
    normer = shrink[:, None] * normer + jnp.sum(keys_weighted, axis=1)
    return ((memory, normer, new_peak), output)


def span_summary(keyrow, valrow, in_gate, log_retain_factor):
    key_scale = keyrow.shape[-1] ** (-0.5)
    cumulative = jnp.cumsum(log_retain_factor, axis=-1)
    span_end = cumulative[:, -1]
    gap_log = span_end[:, None] - cumulative + in_gate
    peak = jnp.max(gap_log, axis=-1)
    spread = jnp.exp(gap_log - peak[:, None]) * key_scale
    keys_weighted = keyrow.astype(jnp.float32) * spread[:, :, None]
    memory = jnp.einsum("hse,hsd->hed", valrow.astype(jnp.float32), keys_weighted)
    return (span_end, peak, memory, jnp.sum(keys_weighted, axis=1))


def join_states(earlier, later):
    total_early, peak_early, memory_early, normer_early = earlier
    total_late, peak_late, memory_late, normer_late = later
    peak = jnp.maximum(total_late + peak_early, peak_late)
    factor_early = jnp.exp(total_late + peak_early - peak)
    factor_late = jnp.exp(peak_late - peak)
    memory = factor_early[:, None, None] * memory_early + factor_late[:, None, None] * memory_late
    normer = factor_early[:, None] * normer_early + factor_late[:, None] * normer_late
    return (total_early + total_late, peak, memory, normer)


def shards(
    memory_query_matrix,
    memory_key_matrix,
    memory_value_matrix,
    input_gate_logits,
    forget_gate_logits,
    forget_log_boosts,
    head_norm_scale,
    memory_output_matrix,
    projection_norm_scale,
    second_batch_rows,
    expert_prenorm_scale,
    selected_expert_index,
    group_route_probability,
    expert_choice_scores,
    expert_gate_matrix,
    expert_up_matrix,
    expert_down_matrix,
):
    local_heads = input_gate_logits.shape[0]
    positions = input_gate_logits.shape[1]
    head_size = memory_query_matrix.shape[1] // local_heads
    spans = positions // SPAN

    def by_head(rows):
        return rows.reshape(positions, local_heads, head_size).transpose(1, 0, 2)

    def to_spans(values):
        shaped = values.reshape((local_heads, spans, SPAN) + values.shape[2:])
        return jnp.moveaxis(shaped, 1, 0)

    query = by_head(memory_query_matrix)
    keyrow = by_head(memory_key_matrix)
    valrow = by_head(memory_value_matrix)
    log_retain_factor = jax.nn.log_sigmoid(forget_gate_logits) + forget_log_boosts
    summary = span_summary(keyrow, valrow, input_gate_logits, log_retain_factor)
    neutral = (
        jnp.zeros((local_heads,), jnp.float32),
        jnp.full((local_heads,), floor_log, jnp.float32),
        jnp.zeros((local_heads, head_size, head_size), jnp.float32),
        jnp.zeros((local_heads, head_size), jnp.float32),
    )
    entering = entering_2(summary, EP, join_states, neutral)
    start = (entering[2], entering[3], entering[1])
    inputs = (
        to_spans(query),
        to_spans(keyrow),
        to_spans(valrow),
        to_spans(input_gate_logits),
        to_spans(log_retain_factor),
    )
    _, cells = lax.scan(span_step, start, inputs)
    cells = jnp.moveaxis(cells, 0, 1).reshape(local_heads, positions, head_size)
    scaled = (cells * head_norm_scale.reshape(local_heads, 1, head_size)).astype(jnp.bfloat16)
    head_out = scaled.transpose(1, 0, 2).reshape(positions, local_heads * head_size)
    first_row = lax.axis_index("tp") * head_out.shape[1]
    weight_rows = lax.dynamic_slice_in_dim(memory_output_matrix, first_row, head_out.shape[1], 0)
    projected = sent_and_summed(
        jnp.dot(head_out, weight_rows, preferred_element_type=jnp.float32).astype(jnp.bfloat16),
        "tp",
        0,
    )
    mixed_rows = rms_scale(projected, projection_norm_scale).astype(jnp.bfloat16)
    token_count = second_batch_rows.shape[0]
    choices_per = selected_expert_index.shape[1]
    experts = lax.axis_size(EP)
    capacity = 2 * choices_per * token_count // experts
    ffn_rows = rms_scale(second_batch_rows.astype(jnp.float32), expert_prenorm_scale).astype(
        jnp.bfloat16
    )
    flat_ids = selected_expert_index.reshape(-1)
    onehot = (flat_ids[:, None] == jnp.arange(experts, dtype=jnp.int32)[None, :]).astype(jnp.int32)
    rank = jnp.sum((jnp.cumsum(onehot, axis=0) - onehot) * onehot, axis=1)
    slot = flat_ids * capacity + rank
    placing = (jnp.arange(experts * capacity, dtype=jnp.int32)[:, None] == slot[None, :]).astype(
        jnp.bfloat16
    )
    placing = jnp.sum(placing.reshape(experts * capacity, token_count, choices_per), axis=-1)
    outgoing = jnp.dot(placing, ffn_rows, preferred_element_type=jnp.float32).astype(jnp.bfloat16)
    outgoing = outgoing.reshape(experts, capacity, ffn_rows.shape[1])
    w_gate = expert_gate_matrix[0]
    w_up = expert_up_matrix[0]
    w_down = expert_down_matrix[0]
    received = lax.all_to_all(outgoing, EP, split_axis=0, concat_axis=0, tiled=True)
    flat_rows = received.reshape(-1, received.shape[2])
    gate = jnp.dot(flat_rows, w_gate, preferred_element_type=jnp.float32)
    upper = jnp.dot(flat_rows, w_up, preferred_element_type=jnp.float32)
    hidden = (jax.nn.silu(gate) * upper).astype(jnp.bfloat16)
    answer = jnp.dot(hidden, w_down, preferred_element_type=jnp.float32).astype(jnp.bfloat16)
    answers = answer.reshape(received.shape)
    back = lax.all_to_all(answers, EP, split_axis=0, concat_axis=0, tiled=True)
    picked = back.reshape(experts * capacity, back.shape[2])[slot].reshape(
        token_count, choices_per, back.shape[2]
    )
    route_weight = group_route_probability[:, None] * jax.nn.softmax(expert_choice_scores, axis=-1)
    routed_rows = jnp.sum(route_weight[:, :, None] * picked.astype(jnp.float32), axis=1).astype(
        jnp.bfloat16
    )
    return (mixed_rows, routed_rows)


def solution(mesh):
    finer = Mesh(mesh.devices.reshape(8, 4, 2, mesh.shape["tp"]), ("ep_0", "ep_1", "ep_2", "tp"))
    in_specs = (
        P(EP, "tp"),
        P(EP, "tp"),
        P(EP, "tp"),
        P("tp", EP),
        P("tp", EP),
        P("tp", EP),
        P("tp"),
        P(),
        P(),
        P(EP_TP, None),
        P(),
        P(EP_TP, None),
        P(EP_TP),
        P(EP_TP, None),
        P(EP, None, None),
        P(EP, None, None),
        P(EP, None, None),
    )
    out_specs = (P(EP_TP, None), P(EP_TP, None))
    return jax.shard_map(
        shards, mesh=finer, in_specs=in_specs, out_specs=out_specs, check_vma=False
    )
```

profile of v0, /device:TPU:8, one launch (start us, length us, event | category | flops | bytes accessed | tf_op | source)
XLA Modules:
  0.0 370.1 jit_solution(2868822607457588346)
XLA Ops:
  9.4 1.9 fusion.114
  11.4 2.0 exponential_multiply_fusion.1
  17.2 2.2 all-gather.3
  26.9 29.7 %all-gather.9.cloned.1.call-done = f32[4,259,256]{2,1,0:T(8,128)} async-done(((f32[1,259,256]{2,1,0:T(8,128)}), f32[4,259,256]{2,1,0:T(8,128)}) %all-gather.9.cloned.1.call-update) | async-done | bytes 1060880 | tf_op jit(solution)/shard_map/all_gather | solution.py:30
  75.6 3.9 %convolution_convert_fusion.1 = bf16[768,2048]{1,0:T(8,128)(2,1)} fusion(bf16[768,192]{0,1:T(8,128)(2,1)S(1)} %fusion.59, bf16[192,2048]{1,0:T(8,128)(2,1)} %param.28, f32[2048]{0:T(1024)S(1)} %copy-done.5, f32[192]{0:T(256)S(1)} %add_rsqrt_fusion), kind=kOutput, calls=%fused_computation.59 | convolution fusion | flops 607125504 | bytes 4236032 | tf_op jit(solution)/shard_map/dot_general | solution.py:205
  79.5 6.1 %reshape.1288 = bf16[64,12,2048]{2,1,0:T(8,128)(2,1)} reshape(bf16[768,2048]{1,0:T(8,128)(2,1)} %convolution_convert_fusion.1) | data formatting | bytes 6291456 | tf_op jit(solution)/shard_map/reshape | solution.py:206
  85.5 9.9 %all-to-all-start.1 = ((bf16[64,12,2048]{2,1,0:T(8,128)(2,1)}), bf16[64,12,2048]{2,1,0:T(8,128)(2,1)}, u32[]{:S(2)}, u32[]{:S(2)}) async-start(bf16[64,12,2048]{2,1,0:T(8,128)(2,1)} %reshape.1288), calls=%async_computation.1 | async-start | bytes 8388608 | tf_op jit(solution)/shard_map/all_to_all | solution.py:210
  96.9 43.6 %all-gather.11.cloned.1.call-done = f32[8,259,256]{2,1,0:T(8,128)} async-done(((f32[1,259,256]{2,1,0:T(8,128)}), f32[8,259,256]{2,1,0:T(8,128)}) %all-gather.11.cloned.1.call-update) | async-done | bytes 2121744 | tf_op jit(solution)/shard_map/all_gather | solution.py:30
  159.5 2.4 fusion.65
  162.0 33.3 %while.16 = (s32[]{:T(128)}, f32[1,256,256]{2,1,0:T(8,128)S(1)}, f32[1,256]{1,0:T(1,128)S(1)}, f32[1]{0:T(128)}, f32[4,1,128,256]{3,2,1,0:T(8,128)}, /*index=5*/...) while((s32[]{:T(128)}, f32[1,256,256]{2,1,0:T(8,128)S(1)}, ...), condition=%wide.region_10.11_spmd, body=%wide.region_4.10_spmd.sunk | while | flops 51037956 | bytes 1794273 | solution.py:178
  168.1 1.7 fusion.177
  196.4 3.3 convolution_convert_fusion.2
  200.7 5.0 %all-to-all-start = ((bf16[4,128,2048]{2,1,0:T(8,128)(2,1)}), bf16[4,128,2048]{2,1,0:T(8,128)(2,1)}, u32[]{:S(2)}, u32[]{:S(2)}) async-start(bf16[4,128,2048]{2,1,0:T(8,128)(2,1)} %bitcast.349), calls=%async_computation | async-start | bytes 4194304 | tf_op jit(solution)/shard_map/all_to_all | solution.py:61
  205.7 6.2 %reshape.1289 = bf16[768,2048]{1,0:T(8,128)(2,1)} reshape(bf16[64,12,2048]{2,1,0:T(8,128)(2,1)} %all-to-all-done.1) | data formatting | bytes 6291456 | tf_op jit(solution)/shard_map/reshape | solution.py:211
  211.8 5.5 %fusion.45 = f32[768,512]{1,0:T(8,128)} fusion(bf16[768,2048]{1,0:T(8,128)(2,1)} %reshape.1289, bf16[1,2048,512]{2,1,0:T(8,128)(2,1)} %param.33), kind=kOutput, calls=%fused_computation.65 | convolution fusion | flops 1610612736 | bytes 6815744 | tf_op jit(solution)/shard_map/dot_general | solution.py:212
  217.3 8.2 %convolution_convert_fusion = bf16[768,2048]{1,0:T(8,128)(2,1)} fusion(bf16[1,512,2048]{2,1,0:T(8,128)(2,1)S(1)} %copy-done, f32[768,512]{1,0:T(8,128)} %fusion.45, bf16[768,2048]{1,0:T(8,128)(2,1)} %reshape.1289, bf16[1,2048,512]{2,1,0:T(8,128)(2,1)} %param.34), kind=kOutput, calls=%fused_computation.58 | convolution fusion | flops 3225157632 | bytes 12058624 | tf_op jit(solution)/shard_map/dot_general | solution.py:215
  225.5 6.1 %reshape.1290 = bf16[64,12,2048]{2,1,0:T(8,128)(2,1)} reshape(bf16[768,2048]{1,0:T(8,128)(2,1)} %convolution_convert_fusion) | data formatting | bytes 6291456 | tf_op jit(solution)/shard_map/reshape | solution.py:216
  231.6 9.4 %all-to-all-start.2 = ((bf16[64,12,2048]{2,1,0:T(8,128)(2,1)}), bf16[64,12,2048]{2,1,0:T(8,128)(2,1)}, u32[]{:S(2)}, u32[]{:S(2)}) async-start(bf16[64,12,2048]{2,1,0:T(8,128)(2,1)} %reshape.1290), calls=%async_computation.2 | async-start | bytes 8388608 | tf_op jit(solution)/shard_map/all_to_all | solution.py:217
  241.4 2.1 convert_reduce_fusion
  244.7 92.6 %all-to-all-done.2 = bf16[64,12,2048]{2,1,0:T(8,128)(2,1)} async-done(((bf16[64,12,2048]{2,1,0:T(8,128)(2,1)}), bf16[64,12,2048]{2,1,0:T(8,128)(2,1)}, u32[]{:S(2)}, u32[]{:S(2)}) %all-to-all-start.2) | async-done | bytes 3145760 | tf_op jit(solution)/shard_map/all_to_all | solution.py:217
  337.3 6.2 %reshape.1291 = bf16[768,2048]{1,0:T(8,128)(2,1)} reshape(bf16[64,12,2048]{2,1,0:T(8,128)(2,1)} %all-to-all-done.2) | data formatting | bytes 6291456 | tf_op jit(solution)/shard_map/reshape | solution.py:218
  343.4 7.3 %gather_fusion = bf16[384,2048]{1,0:T(8,128)(2,1)} fusion(bf16[768,2048]{1,0:T(8,128)(2,1)} %reshape.1291, s32[1024]{0:T(1024)S(1)} %pad_clamp_fusion), kind=kCustom, calls=%fused_computation | custom fusion | bytes 3147264 | tf_op jit(solution)/shard_map/gather | solution.py:218
  350.8 4.7 %reshape.1302 = f32[192,2,2048]{2,1,0:T(2,128)} reshape(bf16[384,2048]{1,0:T(8,128)(2,1)} %gather_fusion) | data formatting | bytes 4718592 | tf_op jit(solution)/shard_map/convert_element_type | solution.py:222
  355.5 7.8 %multiply_reduce_fusion = bf16[192,2048]{1,0:T(8,128)(2,1)} fusion(f32[192,2,2048]{2,1,0:T(2,128)} %reshape.1302, f32[192,2]{1,0:T(8,128)S(1)} %copy.31), kind=kLoop, calls=%fused_computation.60 | loop fusion | flops 1179648 | bytes 3933696 | tf_op jit(solution)/shard_map/reduce_sum | solution.py:222
  (145 shorter events, 49.7 us)
Async XLA Ops:
  7.2 210.2 %copy-start = (bf16[1,512,2048]{2,1,0:T(8,128)(2,1)S(1)}, bf16[1,512,2048]{2,1,0:T(8,128)(2,1)}, u32[]{:S(2)}) copy-start(bf16[1,512,2048]{2,1,0:T(8,128)(2,1)} %param.35) | copy-start | bytes 6291460
  7.2 49.4 %all-gather.9.cloned.1.call-start = ((), (), s32[]{:S(2)}) async-start(), calls=%async_computation.3 | async-start | bytes 1351680 | tf_op jit(solution)/shard_map/all_gather | solution.py:30
  19.4 52.6 %copy-start.7 = (s32[192,2]{0,1:T(2,128)S(1)}, s32[192,2]{0,1:T(2,128)}, u32[]{:S(2)}) copy-start(s32[192,2]{0,1:T(2,128)} %param.30) | copy-start | bytes 4612
  26.8 113.6 %all-gather.11.cloned.1.call-start = ((), (), s32[]{:S(2)}) async-start(), calls=%async_computation.4 | async-start | bytes 2433024 | tf_op jit(solution)/shard_map/all_gather | solution.py:30
  69.2 6.4 %copy-start.5 = (f32[2048]{0:T(1024)S(1)}, f32[2048]{0:T(1024)}, u32[]{:S(2)}) copy-start(f32[2048]{0:T(1024)} %param.29) | copy-start | bytes 24580
  85.5 115.1 %all-to-all-start.1 = ((bf16[64,12,2048]{2,1,0:T(8,128)(2,1)}), bf16[64,12,2048]{2,1,0:T(8,128)(2,1)}, u32[]{:S(2)}, u32[]{:S(2)}) async-start(bf16[64,12,2048]{2,1,0:T(8,128)(2,1)} %reshape.1288), calls=%async_computation.1 | async-start | bytes 8388608 | tf_op jit(solution)/shard_map/all_to_all | solution.py:210
  148.9 13.1 %copy-start.1 = (bf16[512,256]{1,0:T(8,128)(2,1)S(1)}, bf16[512,256]{1,0:T(8,128)(2,1)}, u32[]{:S(2)}) copy-start(bf16[512,256]{1,0:T(8,128)(2,1)} %param.20) | copy-start | bytes 786436
  148.9 13.1 %copy-start.2 = (bf16[512,256]{1,0:T(8,128)(2,1)S(1)}, bf16[512,256]{1,0:T(8,128)(2,1)}, u32[]{:S(2)}) copy-start(bf16[512,256]{1,0:T(8,128)(2,1)} %param.21) | copy-start | bytes 786436
  148.9 13.1 %copy-start.3 = (f32[1,512]{1,0:T(1,128)S(1)}, f32[1,512]{1,0:T(1,128)}, u32[]{:S(2)}) copy-start(f32[1,512]{1,0:T(1,128)} %param.22) | copy-start | bytes 6148
  162.0 33.3 %copy-start.8 = (f32[256]{0:T(256)S(1)}, f32[256]{0:T(256)}, u32[]{:S(2)}) copy-start(f32[256]{0:T(256)} %param.25) | copy-start | bytes 3076
  200.7 30.9 %all-to-all-start = ((bf16[4,128,2048]{2,1,0:T(8,128)(2,1)}), bf16[4,128,2048]{2,1,0:T(8,128)(2,1)}, u32[]{:S(2)}, u32[]{:S(2)}) async-start(bf16[4,128,2048]{2,1,0:T(8,128)(2,1)} %bitcast.349), calls=%async_computation | async-start | bytes 4194304 | tf_op jit(solution)/shard_map/all_to_all | solution.py:61
  231.6 9.6 %copy-start.4 = (f32[192,2]{0,1:T(2,128)S(1)}, f32[192,2]{0,1:T(2,128)}, u32[]{:S(2)}) copy-start(f32[192,2]{0,1:T(2,128)} %param.32) | copy-start | bytes 4612
  231.6 9.6 %copy-start.9 = (f32[192]{0:T(256)S(1)}, f32[192]{0:T(256)}, u32[]{:S(2)}) copy-start(f32[192]{0:T(256)} %param.31) | copy-start | bytes 2308
  231.6 105.7 %all-to-all-start.2 = ((bf16[64,12,2048]{2,1,0:T(8,128)(2,1)}), bf16[64,12,2048]{2,1,0:T(8,128)(2,1)}, u32[]{:S(2)}, u32[]{:S(2)}) async-start(bf16[64,12,2048]{2,1,0:T(8,128)(2,1)} %reshape.1290), calls=%async_computation.2 | async-start | bytes 8388608 | tf_op jit(solution)/shard_map/all_to_all | solution.py:217
  241.4 2.3 copy-start.6
Sparse Core Ops, SparseCore 0:
  26.9 29.5 all-gather.8
  72.1 68.2 all-gather.10
where the time goes:
time: 373 us; the launch traced here: 370 us
  waiting for transfers between devices  167 us (45%)
  between operations  47.8 us (13%)
  local copies, waits for them, and re-layouts  47.5 us (13%)
  matrix products  39.2 us (11%)
  other arithmetic  37.3 us (10%)
  starting transfers between devices  24.3 us (7%)
  loops' own time  4.96 us (1%)
    all_to_all x1, waiting for transfers between devices, shards(): back = lax.all_to_all(answers, EP, split_axis=0, concat_axis=0, tiled=True)  92.6 us
    all_gather x2, waiting for transfers between devices, collected_together(): both, at, found = (lax.all_gather(jnp.concatenate(lines), axis), 0, {})  73.2 us
    all_to_all x1, starting transfers between devices, shards(): lax.all_to_all(outgoing, EP, split_axis=0, concat_axis=0, tiled=True)  9.85 us
    all_to_all x1, starting transfers between devices, shards(): back = lax.all_to_all(answers, EP, split_axis=0, concat_axis=0, tiled=True)  9.41 us
    dot_general x1, matrix products, shards(): jnp.dot(hidden, w_down, preferred_element_type=jnp.float32)  8.2 us
    reduce_sum x1, other arithmetic, shards(): jnp.sum(route_weight[:, :, None] * picked.astype(jnp.float32), axis=1)  7.76 us
  transfers between devices with their start and end apart: 5, of which 4 were waited for; matrix products, arithmetic and copies ran while one was open for 22% of the time, Pallas kernels for 0%

commit v1 on v0

v1 whole, which is shorter than its diff:
```python
import jax
import jax.numpy as jnp
from jax import lax
from jax.experimental import pallas as pl
from jax.experimental.pallas import tpu as pltpu
from jax.sharding import Mesh
from jax.sharding import PartitionSpec as P

EP = ("ep_0", "ep_1", "ep_2")
EP_TP = ("ep_0", "ep_1", "ep_2", "tp")

floor_log = -1e30
norm_eps = 1e-06
f32, bf16, i32 = jnp.float32, jnp.bfloat16, jnp.int32


def iota(shape, dim):
    return lax.broadcasted_iota(i32, shape, dim)


def mm(a, b):
    return lax.dot_general(a, b, (((1,), (0,)), ((), ())), preferred_element_type=f32)


def mm_t(a, b):
    return lax.dot_general(a, b, (((1,), (1,)), ((), ())), preferred_element_type=f32)


def thirds(x):
    hi = x.astype(bf16).astype(f32)
    mid = (x - hi).astype(bf16).astype(f32)
    return hi, mid, (x - hi - mid).astype(bf16).astype(f32)


def halves(x):
    hi = x.astype(bf16)
    return hi, (x - hi.astype(f32)).astype(bf16)


def call(body, out_shape, *args, cost, scratch=(), specs=None, out_specs=None, grid=None, vmem=40):
    extra = {}
    if grid is not None:
        extra = dict(grid=grid, in_specs=specs, out_specs=out_specs)
    elif specs is not None:
        extra = dict(in_specs=specs)
    return pl.pallas_call(
        body,
        out_shape=out_shape,
        scratch_shapes=list(scratch),
        compiler_params=pltpu.CompilerParams(vmem_limit_bytes=vmem << 20),
        cost_estimate=pl.CostEstimate(flops=cost, bytes_accessed=cost // 500, transcendentals=0),
        **extra,
    )(*args)


def struct(shape, dtype):
    return jax.ShapeDtypeStruct(shape, dtype)


def build_body(ids, rows, gain, out, ranks):
    x = rows[...].astype(f32)
    tokens, d = x.shape
    half = d // 2
    experts = ranks.shape[0]
    mean = jnp.mean(x * x, axis=-1, keepdims=True)
    xn = (x * lax.rsqrt(mean + norm_eps) * gain[...]).astype(bf16)
    expert = iota((experts, tokens), 0)
    chosen = (ids[0:1, :] == expert) | (ids[1:2, :] == expert)
    ahead = (iota((tokens, tokens), 0) < iota((tokens, tokens), 1)).astype(f32).astype(bf16)
    count = mm(chosen.astype(f32).astype(bf16), ahead)
    rank = jnp.where(chosen, count, -1.0)
    ranks[...] = rank
    row = iota((experts, 8, tokens), 1)
    held = rank[:, None, :]

    def placing(hit):
        return hit.astype(f32).reshape(experts * 8, tokens).astype(bf16)

    out[:, :d] = mm(placing(held == row.astype(f32)), xn).astype(bf16)
    late = held == ((row & 3) + 8).astype(f32)
    first, last = placing(late & (row < 4)), placing(late & (row >= 4))
    out[:, d:] = (mm(first, xn[:, :half]) + mm(last, xn[:, half:])).astype(bf16)


def shares_body(ids, prob, scores, ranks, share8, share4):
    rank = ranks[...]
    experts, tokens = rank.shape
    s0, s1 = scores[0:1, :], scores[1:2, :]
    top = jnp.maximum(s0, s1)
    e0, e1 = jnp.exp(s0 - top), jnp.exp(s1 - top)
    both = e0 + e1
    w0, w1 = prob[...] * (e0 / both), prob[...] * (e1 / both)
    expert = iota((experts, tokens), 0)
    share = jnp.where(ids[0:1, :] == expert, w0, 0.0) + jnp.where(ids[1:2, :] == expert, w1, 0.0)
    row = iota((experts, 8, tokens), 1)

    def placed(hit, out):
        at = jnp.where(hit, share[:, None, :], 0.0).reshape(experts * 8, tokens).T
        out[:tokens], out[tokens:] = halves(at)

    placed(rank[:, None, :] == row.astype(f32), share8)
    hit = rank[:, None, :] == ((row & 3) + 8).astype(f32)
    for h in range(2):
        placed(hit & ((row >> 2) == h), share4.at[h])


def silu_mul(gate, upper):
    return (gate / (1.0 + jnp.exp(-gate)) * upper).astype(bf16)


def ffn_body(x, wg, wu, wd, out):
    d, width = wg.shape
    half = d // 2
    x8 = x[:, :d]
    hidden = silu_mul(mm(x8, wg[...]), mm(x8, wu[...]))
    out[:, :d] = mm(hidden, wd[...]).astype(bf16)
    x4 = x[:, d:]
    rows = x4.shape[0]
    first = (iota((rows, 1), 0) & 4) == 0

    def joined(w):
        z = jnp.where(first, mm(x4, w[:half, :]), mm(x4, w[half:, :]))
        z3 = z.reshape(rows // 8, 8, width)
        return (z3 + pltpu.roll(z3, 4, 1)).reshape(rows, width)

    hidden = silu_mul(joined(wg), joined(wu))
    out[:, d:] = jnp.where(first, mm(hidden, wd[:, :half]), mm(hidden, wd[:, half:])).astype(bf16)


def combine_body(share8, share4, back, out):
    tokens, d = out.shape
    half = d // 2
    late = back[:, d:]
    for h in range(2):
        cols = slice(h * half, (h + 1) * half)
        total = mm(share8[...], back[:, cols]) + mm(share4[h], late)
        out[:, cols] = (total[:tokens] + total[tokens:]).astype(bf16)


def running_keep(forget, boosts):
    x = forget[...]
    keep = boosts[...] - (jnp.maximum(-x, 0.0) + jnp.log1p(jnp.exp(-jnp.abs(x))))
    length = keep.shape[1]
    pieces = jnp.concatenate([*thirds(keep), jnp.zeros((5, length), f32)], axis=0).astype(bf16)
    upto = (iota((length, length), 0) <= iota((length, length), 1)).astype(f32).astype(bf16)
    return jnp.sum(mm(pieces, upto), axis=0, keepdims=True)


def side_rows(normer, total, peak):
    width = normer.shape[1]
    hi = normer.astype(bf16).astype(f32)
    lane = iota((1, width), 1)
    info = jnp.zeros((1, width), f32)
    for at, piece in enumerate((*thirds(total), *thirds(peak))):
        info = jnp.where(lane == at, piece, info)
    return jnp.concatenate([hi, normer - hi, info, jnp.zeros((5, width), f32)], axis=0)


def read_side(side):
    normer = side[0:1, :] + side[1:2, :]
    info = side[2:3, :]
    total = info[:, 0:1] + info[:, 1:2] + info[:, 2:3]
    peak = info[:, 3:4] + info[:, 4:5] + info[:, 5:6]
    return normer, total, peak


def summary_body(keys, values, gates, forget, boosts, out):
    b = running_keep(forget, boosts)
    length = b.shape[1]
    width = keys.shape[1]
    last = b[:, length - 1 : length]
    gap = last - b + gates[...]
    peak = jnp.max(gap, axis=1, keepdims=True)
    spread = jnp.exp(gap - peak) * (width**-0.5)
    k = keys[...]
    scaled = (values[...].astype(f32).T * spread).astype(bf16)
    out[:width, :] = mm(scaled, k).astype(bf16)
    hi, lo = halves(spread)
    two = jnp.concatenate([hi.astype(f32), lo.astype(f32), jnp.zeros((6, length), f32)], axis=0)
    normer = jnp.sum(mm(two.astype(bf16), k), axis=0, keepdims=True)
    out[width:, :] = side_rows(normer, last, peak).astype(bf16)


def weighted(pieces, logs, floor):
    stabil = floor
    for level in logs:
        stabil = jnp.maximum(stabil, level)
    memory, normer = None, None
    for (piece, n), level in zip(pieces, logs):
        factor = jnp.exp(level - stabil)
        memory = factor * piece if memory is None else memory + factor * piece
        normer = factor * n if normer is None else normer + factor * n
    return memory, normer, stabil


def before(mine, totals, peaks):
    logs, kept = [], []
    floor = jnp.full((1, 1), floor_log, f32)
    for j in range(len(totals)):
        level = peaks[j]
        for l in range(j + 1, len(totals)):
            level = level + jnp.where(l < mine, totals[l], 0.0)
        kept.append(j < mine)
        logs.append(jnp.where(j < mine, level, floor))
    return logs, kept


def masked(kept, pieces):
    return [(jnp.where(k, c, 0.0), jnp.where(k, n, 0.0)) for k, (c, n) in zip(kept, pieces)]


def plane_body(where, got, out, own, small, whole_memory):
    mine = where[1]
    width = got.shape[2]
    count = got.shape[0]
    pieces, totals, peaks = [], [], []
    for j in range(count):
        normer, total, peak = read_side(got[j, width:, :].astype(f32))
        pieces.append((got[j, :width, :].astype(f32), normer))
        totals.append(total)
        peaks.append(peak)
    logs = []
    for j in range(count):
        level = peaks[j]
        for l in range(j + 1, count):
            level = level + totals[l]
        logs.append(level)
    memory, normer, stabil = weighted(pieces, logs, logs[0])
    everything = totals[0]
    for total in totals[1:]:
        everything = everything + total
    whole_memory[...] = memory
    part = width // count
    out[:part, :] = whole_memory[pl.ds(pl.multiple_of(mine * part, 8), part), :].astype(bf16)
    out[part:, :] = side_rows(normer, everything, stabil).astype(bf16)
    logs, kept = before(mine, totals, peaks)
    memory, normer, stabil = weighted(
        masked(kept, pieces), logs, jnp.full((1, 1), floor_log, f32)
    )
    own[...] = memory
    passed = jnp.zeros((1, 1), f32)
    for l in range(count):
        passed = passed + jnp.where(l < mine, totals[l], 0.0)
    small[0:1, :] = normer
    small[1:2, :] = jnp.broadcast_to(stabil, (1, width))
    small[2:3, :] = jnp.broadcast_to(passed, (1, width))
    small[3:8, :] = jnp.zeros((5, width), f32)


def line_body(where, got, out, small):
    mine = where[0]
    part = out.shape[0]
    width = got.shape[2]
    pieces, totals, peaks = [], [], []
    for j in range(got.shape[0]):
        normer, total, peak = read_side(got[j, part:, :].astype(f32))
        pieces.append((got[j, :part, :].astype(f32), normer))
        totals.append(total)
        peaks.append(peak)
    logs, kept = before(mine, totals, peaks)
    memory, normer, stabil = weighted(
        masked(kept, pieces), logs, jnp.full((1, 1), floor_log, f32)
    )
    out[...] = memory.astype(bf16)
    small[0:1, :] = normer
    small[1:2, :] = jnp.broadcast_to(stabil, (1, width))
    small[2:8, :] = jnp.zeros((6, width), f32)


def cell_body(query, keys, values, gates, forget, boosts, state, line, own, near, scale, out):
    b = running_keep(forget, boosts)
    length = b.shape[1]
    width = keys.shape[1]
    b_col = jnp.broadcast_to(b, (128, length)).T
    far_log = near[2:3, 0:1] + line[1:2, 0:1]
    near_log = near[1:2, 0:1]
    stabil = jnp.maximum(far_log, near_log)
    far, close = jnp.exp(far_log - stabil), jnp.exp(near_log - stabil)
    normer = far * line[0:1, :] + close * near[0:1, :]
    memory = (far * state[...].astype(f32) + close * own[...]).astype(bf16)
    source = gates[...] - b
    block = 128
    for start in range(0, length, block):
        upto = start + block
        rows = slice(start, upto)
        q = query[rows, :]
        bt = b_col[rows, 0:1]
        decay = bt + source[:, :upto]
        seen = iota((block, upto), 1) <= iota((block, upto), 0) + start
        decay = jnp.where(seen, decay, -jnp.inf)
        carried = bt + stabil
        peak = jnp.maximum(carried, jnp.max(decay, axis=1, keepdims=True))
        across = jnp.exp(carried - peak)
        scores = mm_t(q, keys[:upto, :]) * (width**-0.5) * jnp.exp(decay - peak)
        den = jnp.sum(scores, axis=1, keepdims=True) + across * jnp.sum(
            q.astype(f32) * normer, axis=1, keepdims=True
        )
        num = mm(scores.astype(bf16), values[:upto, :]) + across * mm_t(q, memory)
        cell = num / jnp.maximum(jnp.abs(den), jnp.exp(-peak))
        out[rows, :] = (cell * scale[...]).astype(bf16)


def project_body(where, *refs):
    heads, (weight, gain, out) = refs[:-3], refs[-3:]
    count = len(heads)
    width = heads[0].shape[-1]
    total = None
    for step, head in enumerate(heads):
        source = lax.rem(where[2] + count - step, count)
        rows = weight[pl.ds(pl.multiple_of(source * width, width), width), :]
        product = mm(head[...], rows)
        total = product if total is None else total + product
    mean = jnp.mean(total * total, axis=-1, keepdims=True)
    out[...] = (total * lax.rsqrt(mean + norm_eps) * gain[...]).astype(bf16)


def exchanged(array, axes):
    return lax.all_to_all(array, axes, split_axis=0, concat_axis=0, tiled=True)


def after(array, *earlier):
    return lax.optimization_barrier((array, *earlier))[0]


def shards(
    query,
    keys,
    values,
    in_gates,
    forget,
    boosts,
    head_scale,
    out_weight,
    out_gain,
    rows,
    row_gain,
    ids,
    prob,
    scores,
    w_gate,
    w_up,
    w_down,
):
    devices = lax.axis_size(EP)
    positions, width = query.shape
    tokens, d = rows.shape
    hidden = w_gate.shape[2]
    slots = devices * 8
    plane = lax.axis_size(("ep_1", "ep_2"))
    planes = lax.axis_size("tp")
    wg, wu, wd = w_gate[0], w_up[0], w_down[0]
    ids_t = ids.T
    vm = pl.BlockSpec(memory_space=pltpu.VMEM)
    sm = pl.BlockSpec(memory_space=pltpu.SMEM)
    where = jnp.stack(
        [lax.axis_index("ep_0"), lax.axis_index(("ep_1", "ep_2")), lax.axis_index("tp")]
    ).astype(i32)

    out, ranks = call(
        build_body,
        (struct((slots, d + d // 2), bf16), struct((devices, tokens), f32)),
        ids_t,
        rows,
        row_gain.reshape(1, d),
        cost=4 * slots * tokens * d,
    )
    got = exchanged(out.reshape(devices, 8, d + d // 2), EP)
    send = call(
        summary_body,
        struct((width + 8, width), bf16),
        after(keys, out),
        values,
        in_gates,
        forget,
        boosts,
        cost=2 * positions * width * width * 4,
    )
    states = lax.all_gather(send, ("ep_1", "ep_2"))
    send, own, near = call(
        plane_body,
        (
            struct((width // plane + 8, width), bf16),
            struct((width, width), f32),
            struct((8, width), f32),
        ),
        where,
        states,
        cost=4 * plane * width * width * 100,
        scratch=(pltpu.VMEM((width, width), f32),),
        specs=[sm, vm],
    )
    states = lax.all_gather(send, "ep_0")
    send, far = call(
        line_body,
        (struct((width // plane, width), bf16), struct((8, width), f32)),
        where,
        states,
        cost=4 * width * width * 100,
        specs=[sm, vm],
    )
    share8, share4 = call(
        shares_body,
        (struct((2 * tokens, slots), bf16), struct((2, 2 * tokens, slots), bf16)),
        ids_t,
        prob.reshape(1, tokens),
        scores.T,
        after(ranks, out),
        cost=slots * tokens * 1000,
    )
    block = 128
    answers = call(
        ffn_body,
        struct((slots, d + d // 2), bf16),
        got.reshape(slots, d + d // 2),
        wg,
        wu,
        wd,
        cost=12 * slots * d * hidden,
        grid=(slots // block,),
        specs=[pl.BlockSpec((block, d + d // 2), lambda i: (i, 0)), vm, vm, vm],
        out_specs=pl.BlockSpec((block, d + d // 2), lambda i: (i, 0)),
    )
    back = exchanged(answers.reshape(devices, 8, d + d // 2), EP)
    state = lax.all_gather(send, ("ep_1", "ep_2"), tiled=True)
    heads = call(
        cell_body,
        struct((positions, width), bf16),
        query,
        keys,
        values,
        in_gates,
        forget,
        boosts,
        state,
        far,
        own,
        near,
        head_scale.reshape(1, width),
        cost=2 * positions * positions * width * 40,
    )
    share = positions // planes
    me = where[2]
    pieces = []
    for step in range(planes):
        first = lax.rem(me + step, planes) * share
        piece = lax.dynamic_slice_in_dim(heads, first, share, 0)
        if step:
            ring = [(i, (i + step) % planes) for i in range(planes)]
            piece = lax.ppermute(piece, "tp", ring)
        pieces.append(piece)
    mixed_rows = call(
        project_body,
        struct((share, d), bf16),
        where,
        *pieces,
        out_weight,
        out_gain.reshape(1, d),
        cost=20 * positions * width * d,
        specs=[sm] + [vm] * (planes + 2),
    )
    routed_rows = call(
        combine_body,
        struct((tokens, d), bf16),
        share8,
        share4,
        back.reshape(slots, d + d // 2),
        cost=12 * tokens * slots * d,
    )
    return (mixed_rows, routed_rows)


def solution(mesh):
    finer = Mesh(mesh.devices.reshape(8, 4, 2, mesh.shape["tp"]), ("ep_0", "ep_1", "ep_2", "tp"))
    in_specs = (
        P(EP, "tp"),
        P(EP, "tp"),
        P(EP, "tp"),
        P("tp", EP),
        P("tp", EP),
        P("tp", EP),
        P("tp"),
        P(),
        P(),
        P(EP_TP, None),
        P(),
        P(EP_TP, None),
        P(EP_TP),
        P(EP_TP, None),
        P(EP, None, None),
        P(EP, None, None),
        P(EP, None, None),
    )
    out_specs = (P(EP_TP, None), P(EP_TP, None))
    return jax.shard_map(
        shards, mesh=finer, in_specs=in_specs, out_specs=out_specs, check_vma=False
    )
```

time: 373 us -> 244 us (0.65)
  blocking collectives: 2.19 us -> 152 us
  waiting for transfers between devices: 167 us -> 31.3 us
  matrix products: 39.2 us -> 0 us
  other arithmetic: 37.3 us -> 0.08 us
  local copies, waits for them, and re-layouts: 47.5 us -> 11.3 us
  between operations: 47.8 us -> 14.3 us
  Pallas kernels: 0 us -> 20.6 us
  starting transfers between devices: 24.3 us -> 10.7 us
  loops' own time: 4.96 us -> 0 us
    all_to_all x3 -> x1, waiting for transfers between devices: 93.6 us -> 0.01 us  [exchanged(): return lax.all_to_all(array, axes, split_axis=0, concat_axis=0, tiled=True)]
    all_to_all x0 -> x1, blocking collectives: none -> 85.8 us  [exchanged(): return lax.all_to_all(array, axes, split_axis=0, concat_axis=0, tiled=True)]
    all_gather x1 -> x2, blocking collectives: 2.19 us -> 65.8 us  [the longest x1 52.7 us: shards(): states = lax.all_gather(send, 'ep_0')]
    all_gather x2 -> x1, waiting for transfers between devices: 73.2 us -> 30.1 us  [shards(): states = lax.all_gather(send, ('ep_1', 'ep_2'))]
    dot_general x25 -> x0, matrix products: 39.2 us -> none  [the longest x1 8.2 us: shards(): jnp.dot(hidden, w_down, preferred_element_type=jnp.float32)]
    reshape x4 -> x0, local copies, waits for them, and re-layouts: 24.5 us -> none  [the longest x1 6.17 us: shards(): back.reshape(experts * capacity, back.shape[2])[slot]]
    pallas_call x0 -> x9, Pallas kernels: none -> 20.6 us  [call(): pl.pallas_call(body, out_shape=out_shape, scratch_shapes=list(scratch), c...]
    all_to_all x3 -> x1, starting transfers between devices: 24.2 us -> 5.71 us  [exchanged(): return lax.all_to_all(array, axes, split_axis=0, concat_axis=0, tiled=True)]
  transfers between devices with their start and end apart: 5 -> 5, of which waited for: 4 -> 3; matrix products, arithmetic and copies ran while one was open for 22% -> 0% of each run, Pallas kernels for 0% -> 3%
where the time goes in v1:
time: 244 us; the launch traced here: 240 us
  blocking collectives  152 us (62%)
  waiting for transfers between devices  31.3 us (13%)
  Pallas kernels  20.6 us (8%)
  between operations  14.3 us (6%)
  local copies, waits for them, and re-layouts  11.3 us (5%)
  starting transfers between devices  10.7 us (4%)
    all_to_all x1, blocking collectives, exchanged(): return lax.all_to_all(array, axes, split_axis=0, concat_axis=0, tiled=True)  85.8 us
    all_gather x1, blocking collectives, shards(): states = lax.all_gather(send, 'ep_0')  52.7 us
    all_gather x1, waiting for transfers between devices, shards(): states = lax.all_gather(send, ('ep_1', 'ep_2'))  30.1 us
    pallas_call x9, Pallas kernels, call(): pl.pallas_call(body, out_shape=out_shape, scratch_shapes=list(scratch), c...  20.6 us
    all_gather x1, blocking collectives, shards(): state = lax.all_gather(send, ('ep_1', 'ep_2'), tiled=True)  13 us
    unnamed x52, local copies, waits for them, and re-layouts  11.2 us
    all_to_all x1, starting transfers between devices, exchanged(): return lax.all_to_all(array, axes, split_axis=0, concat_axis=0, tiled=True)  5.71 us
    ppermute x3, starting transfers between devices, shards(): piece = lax.ppermute(piece, 'tp', ring)  5 us
  transfers between devices with their start and end apart: 5, of which 3 were waited for; matrix products, arithmetic and copies ran while one was open for 0% of the time, Pallas kernels for 3%

profile of v1, /device:TPU:8, one launch (start us, length us, event | category | flops | bytes accessed | tf_op | source)
XLA Modules:
  0.0 239.8 jit_solution(2259653370688427170)
XLA Ops:
  7.2 1.1 copy-done.6
  9.7 1.6 shard_map.176
  11.3 85.8 %all_to_all.10 = bf16[64,8,3072]{2,1,0:T(8,128)(2,1)S(1)} all-to-all(bf16[64,8,3072]{2,1,0:T(8,128)(2,1)S(1)} %bitcast.20), channel_id=1, replica_groups=mesh['ep_0'=8,'ep_1'=4,'ep_2'=2,'tp'=4] {'ep_0','ep_1','ep_2'}, dimensions={0} | all-to-all | bytes 6291456 | tf_op jit(solution)/shard_map/all_to_all | solution.py:318
  97.1 8.2 %shard_map.183 = bf16[512,3072]{1,0:T(8,128)(2,1)S(1)} custom-call(bf16[512,3072]{1,0:T(8,128)(2,1)S(1)} %bitcast.21, bf16[2048,512]{1,0:T(8,128)(2,1)S(1)} %bitcast.24, bf16[2048,512]{1,0:T(8,128)(2,1)S(1)} %bitcast.25, bf16[512,2048]{1,0:T(8,128)(2,1)S(1)} %bitcast.26), custom_call_target="tpu_custom_call" | custom-call | flops 6442450944 | bytes 12884901 | tf_op jit(solution)/shard_map/pallas_call | solution.py:46
  105.4 1.6 copy-done
  107.0 5.7 %all-to-all-start.1 = ((bf16[64,8,3072]{2,1,0:T(8,128)(2,1)}), bf16[64,8,3072]{2,1,0:T(8,128)(2,1)S(1)}, u32[]{:S(2)}, u32[]{:S(2)}) async-start(bf16[64,8,3072]{2,1,0:T(8,128)(2,1)} %bitcast.19), calls=%async_computation.1 | async-start | bytes 6291456 | tf_op jit(solution)/shard_map/all_to_all | solution.py:318
  112.9 0.9 copy-done.8
  113.8 0.9 copy-done.10
  114.7 1.3 shard_map.177
  116.2 30.1 %all-gather.4.cloned.1.call-done = bf16[2112,256]{1,0:T(8,128)(2,1)} async-done(((bf16[264,256]{1,0:T(8,128)(2,1)}), bf16[2112,256]{1,0:T(8,128)(2,1)}) %all-gather.4.cloned.1.call-update) | async-done | bytes 1081360 | tf_op jit(solution)/shard_map/all_gather | solution.py:378
  146.3 1.2 copy-done.1
  147.5 1.5 shard_map.178
  149.0 52.7 %all-gather.1 = bf16[320,256]{1,0:T(8,128)(2,1)S(1)} all-gather(bf16[40,256]{1,0:T(8,128)(2,1)S(1)} %get-tuple-element.15), channel_id=3, replica_groups=mesh['ep_0'=8,'ep_1'=4,'ep_2'=2,'tp'=4] {'ep_0'}, dimensions={0}, use_global_device_ids=true | all-gather | bytes 184320 | tf_op jit(solution)/shard_map/all_gather | solution.py:392
  201.8 0.8 shard_map.179
  202.6 13.0 %all_gather.19.state = bf16[256,256]{1,0:T(8,128)(2,1)S(1)} all-gather(bf16[32,256]{1,0:T(8,128)(2,1)S(1)} %get-tuple-element.16), channel_id=1, replica_groups=mesh['ep_0'=8,'ep_1'=4,'ep_2'=2,'tp'=4] {'ep_1','ep_2'}, dimensions={0}, use_global_device_ids=true | all-gather | bytes 147456 | tf_op jit(solution)/shard_map/all_gather | solution.py:424
  215.6 0.9 copy-done.9
  216.6 0.9 copy-done.11
  217.6 1.7 shard_map.180
  219.9 2.6 %collective-permute-start.1 = (bf16[128,256]{1,0:T(8,128)(2,1)S(1)}, bf16[128,256]{1,0:T(8,128)(2,1)S(1)}, u32[]{:S(2)}, u32[]{:S(2)}) collective-permute-start(bf16[128,256]{1,0:T(8,128)(2,1)S(1)} %get-tuple-element.25), channel_id=1, source_target_pairs={{0,2},{1,3},{2,0},{3,1},{4,6},{5,7},{6,4},{7,5},{8,10},{9,11},{10,... | collective-permute-start | bytes 196616 | tf_op jit(solution)/shard_map/ppermute | solution.py:449
  222.4 1.9 collective-permute-start
  224.9 0.9 copy-done.22
  226.9 2.2 shard_map.181
  229.2 1.1 copy-done.23
  230.3 2.7 %shard_map.184 = bf16[192,2048]{1,0:T(8,128)(2,1)} custom-call(bf16[384,512]{1,0:T(8,128)(2,1)S(1)} %get-tuple-element.22.share8, bf16[2,384,512]{2,1,0:T(8,128)(2,1)S(1)} %copy-done.23, bf16[512,3072]{1,0:T(8,128)(2,1)S(1)} %bitcast.18), custom_call_target="tpu_custom_call" | custom-call | flops 2415919104 | bytes 4831838 | tf_op jit(solution)/shard_map/pallas_call | solution.py:46
  (53 shorter events, 3.9 us)
Async XLA Ops:
  7.2 1.1 copy-start.6
  11.3 85.8 %copy-start.24 = (f32[64,192]{1,0:T(8,128)}, f32[64,192]{1,0:T(8,128)S(1)}, u32[]{:S(2)}) copy-start(f32[64,192]{1,0:T(8,128)S(1)} %get-tuple-element.21.ranks) | copy-start | bytes 147460
  11.3 85.8 %copy-start.3 = (bf16[1,2048,512]{2,1,0:T(8,128)(2,1)S(1)}, bf16[1,2048,512]{2,1,0:T(8,128)(2,1)}, u32[]{:S(2)}) copy-start(bf16[1,2048,512]{2,1,0:T(8,128)(2,1)} %param.31) | copy-start | bytes 6291460
  11.3 85.8 %copy-start.4 = (bf16[1,2048,512]{2,1,0:T(8,128)(2,1)S(1)}, bf16[1,2048,512]{2,1,0:T(8,128)(2,1)}, u32[]{:S(2)}) copy-start(bf16[1,2048,512]{2,1,0:T(8,128)(2,1)} %param.32) | copy-start | bytes 6291460
  11.3 85.8 %copy-start.5 = (bf16[1,512,2048]{2,1,0:T(8,128)(2,1)S(1)}, bf16[1,512,2048]{2,1,0:T(8,128)(2,1)}, u32[]{:S(2)}) copy-start(bf16[1,512,2048]{2,1,0:T(8,128)(2,1)} %param.33) | copy-start | bytes 6291460
  105.4 1.6 copy-start
  107.0 5.8 %copy-start.14 = (f32[1,512]{1,0:T(1,128)S(1)}, f32[1,512]{1,0:T(1,128)}, u32[]{:S(2)}) copy-start(f32[1,512]{1,0:T(1,128)} %gates.3) | copy-start | bytes 6148
  107.0 5.8 %copy-start.15 = (f32[1,512]{1,0:T(1,128)S(1)}, f32[1,512]{1,0:T(1,128)}, u32[]{:S(2)}) copy-start(f32[1,512]{1,0:T(1,128)} %forget.3) | copy-start | bytes 6148
  107.0 5.8 %copy-start.16 = (f32[1,512]{1,0:T(1,128)S(1)}, f32[1,512]{1,0:T(1,128)}, u32[]{:S(2)}) copy-start(f32[1,512]{1,0:T(1,128)} %boosts.3) | copy-start | bytes 6148
  107.0 108.6 %copy-start.7 = (bf16[512,256]{1,0:T(8,128)(2,1)S(1)}, bf16[512,256]{1,0:T(8,128)(2,1)}, u32[]{:S(2)}) copy-start(bf16[512,256]{1,0:T(8,128)(2,1)} %query.1) | copy-start | bytes 786436
  107.0 108.6 %copy-start.20 = (f32[256]{0:T(256)S(1)}, f32[256]{0:T(256)}, u32[]{:S(2)}) copy-start(f32[256]{0:T(256)} %param.23) | copy-start | bytes 3076
  107.0 122.1 %all-to-all-start.1 = ((bf16[64,8,3072]{2,1,0:T(8,128)(2,1)}), bf16[64,8,3072]{2,1,0:T(8,128)(2,1)S(1)}, u32[]{:S(2)}, u32[]{:S(2)}) async-start(bf16[64,8,3072]{2,1,0:T(8,128)(2,1)} %bitcast.19), calls=%async_computation.1 | async-start | bytes 6291456 | tf_op jit(solution)/shard_map/all_to_all | solution.py:318
  112.8 33.5 %all-gather.4.cloned.1.call-start = ((), (), s32[]{:S(2)}) async-start(), calls=%async_computation.2 | async-start | bytes 1216512 | tf_op jit(solution)/shard_map/all_gather | solution.py:378
  146.3 1.2 copy-start.1
  217.5 6.8 %copy-start.18 = (s32[192,2]{0,1:T(2,128)S(1)}, s32[192,2]{0,1:T(2,128)}, u32[]{:S(2)}) copy-start(s32[192,2]{0,1:T(2,128)} %param.28) | copy-start | bytes 4612
  217.5 6.8 %copy-start.19 = (f32[192,2]{0,1:T(2,128)S(1)}, f32[192,2]{0,1:T(2,128)}, u32[]{:S(2)}) copy-start(f32[192,2]{0,1:T(2,128)} %param.30) | copy-start | bytes 4612
  217.5 6.8 %copy-start.21 = (f32[192]{0:T(256)S(1)}, f32[192]{0:T(256)}, u32[]{:S(2)}) copy-start(f32[192]{0:T(256)} %param.29) | copy-start | bytes 2308
  217.5 6.8 %copy-start.25 = (f32[64,192]{1,0:T(8,128)S(1)}, f32[64,192]{1,0:T(8,128)}, u32[]{:S(2)}) copy-start(f32[64,192]{1,0:T(8,128)} %copy-done.24) | copy-start | bytes 147460
  217.6 9.4 %copy-start.2 = (bf16[1024,2048]{1,0:T(8,128)(2,1)S(1)}, bf16[1024,2048]{1,0:T(8,128)(2,1)}, u32[]{:S(2)}) copy-start(bf16[1024,2048]{1,0:T(8,128)(2,1)} %refs_4_.1) | copy-start | bytes 12582916
  217.6 9.4 %copy-start.13 = (f32[2048]{0:T(1024)S(1)}, f32[2048]{0:T(1024)}, u32[]{:S(2)}) copy-start(f32[2048]{0:T(1024)} %param.25) | copy-start | bytes 24580
  219.3 6.4 %collective-permute-start.2 = (bf16[128,256]{1,0:T(8,128)(2,1)S(1)}, bf16[128,256]{1,0:T(8,128)(2,1)S(1)}, u32[]{:S(2)}, u32[]{:S(2)}) collective-permute-start(bf16[128,256]{1,0:T(8,128)(2,1)S(1)} %get-tuple-element.24), channel_id=1, source_target_pairs={{0,3},{1,0},{2,1},{3,2},{4,7},{5,4},{6,5},{7,6},{8,11},{9,8},{10,9... | collective-permute-start | bytes 196616 | tf_op jit(solution)/shard_map/ppermute | solution.py:449
  219.9 6.3 %collective-permute-start.1 = (bf16[128,256]{1,0:T(8,128)(2,1)S(1)}, bf16[128,256]{1,0:T(8,128)(2,1)S(1)}, u32[]{:S(2)}, u32[]{:S(2)}) collective-permute-start(bf16[128,256]{1,0:T(8,128)(2,1)S(1)} %get-tuple-element.25), channel_id=1, source_target_pairs={{0,2},{1,3},{2,0},{3,1},{4,6},{5,7},{6,4},{7,5},{8,10},{9,11},{10,... | collective-permute-start | bytes 196616 | tf_op jit(solution)/shard_map/ppermute | solution.py:449
  222.4 4.5 %collective-permute-start = (bf16[128,256]{1,0:T(8,128)(2,1)S(1)}, bf16[128,256]{1,0:T(8,128)(2,1)S(1)}, u32[]{:S(2)}, u32[]{:S(2)}) collective-permute-start(bf16[128,256]{1,0:T(8,128)(2,1)S(1)} %get-tuple-element.26), channel_id=1, source_target_pairs={{0,1},{1,2},{2,3},{3,0},{4,5},{5,6},{6,7},{7,4},{8,9},{9,10},{10,1... | collective-permute-start | bytes 196616 | tf_op jit(solution)/shard_map/ppermute | solution.py:449
  229.2 1.1 copy-start.23
  (7 other events, 6.1 us)
Sparse Core Ops, SparseCore 0:
  116.2 30.0 all-gather.3

commit v2 on v1

--- a/solution.py
+++ b/solution.py
@@ -9,6 +9,7 @@
 EP = ("ep_0", "ep_1", "ep_2")
 EP_TP = ("ep_0", "ep_1", "ep_2", "tp")
 
+
 floor_log = -1e30
 norm_eps = 1e-06
 f32, bf16, i32 = jnp.float32, jnp.bfloat16, jnp.int32
@@ -37,12 +38,18 @@
     return hi, (x - hi.astype(f32)).astype(bf16)
 
 
-def call(body, out_shape, *args, cost, scratch=(), specs=None, out_specs=None, grid=None, vmem=40):
+def whole(*shape):
+    return pl.BlockSpec(shape, lambda *_: (0,) * len(shape))
+
+
+def call(body, out_shape, *args, cost, scratch=(), specs=None, out_specs=None, grid=None, vmem=24):
     extra = {}
     if grid is not None:
         extra = dict(grid=grid, in_specs=specs, out_specs=out_specs)
     elif specs is not None:
         extra = dict(in_specs=specs)
+        if out_specs is not None:
+            extra["out_specs"] = out_specs
     return pl.pallas_call(
         body,
         out_shape=out_shape,
@@ -57,29 +64,36 @@
     return jax.ShapeDtypeStruct(shape, dtype)
 
 
-def build_body(ids, rows, gain, out, ranks):
-    x = rows[...].astype(f32)
-    tokens, d = x.shape
+def build_body(ids, rows, gain, out, ranks, normed, held):
+    d = rows.shape[1]
     half = d // 2
-    experts = ranks.shape[0]
-    mean = jnp.mean(x * x, axis=-1, keepdims=True)
-    xn = (x * lax.rsqrt(mean + norm_eps) * gain[...]).astype(bf16)
-    expert = iota((experts, tokens), 0)
-    chosen = (ids[0:1, :] == expert) | (ids[1:2, :] == expert)
-    ahead = (iota((tokens, tokens), 0) < iota((tokens, tokens), 1)).astype(f32).astype(bf16)
-    count = mm(chosen.astype(f32).astype(bf16), ahead)
-    rank = jnp.where(chosen, count, -1.0)
-    ranks[...] = rank
-    row = iota((experts, 8, tokens), 1)
-    held = rank[:, None, :]
+    experts, tokens = ranks.shape
+
+    @pl.when(pl.program_id(0) == 0)
+    def _():
+        x = rows[...].astype(f32)
+        mean = jnp.mean(x * x, axis=-1, keepdims=True)
+        normed[...] = (x * lax.rsqrt(mean + norm_eps) * gain[...]).astype(bf16)
+        expert = iota((experts, tokens), 0)
+        chosen = (ids[0:1, :] == expert) | (ids[1:2, :] == expert)
+        ahead = (iota((tokens, tokens), 0) < iota((tokens, tokens), 1)).astype(f32).astype(bf16)
+        count = mm(chosen.astype(f32).astype(bf16), ahead)
+        rank = jnp.where(chosen, count, -1.0)
+        ranks[...] = rank
+        held[...] = rank
+
+    part = out.shape[0] // 8
+    first_expert = pl.multiple_of(pl.program_id(0) * part, 8)
+    rank = held[pl.ds(first_expert, part), :][:, None, :]
+    row = iota((part, 8, tokens), 1)
 
     def placing(hit):
-        return hit.astype(f32).reshape(experts * 8, tokens).astype(bf16)
-
-    out[:, :d] = mm(placing(held == row.astype(f32)), xn).astype(bf16)
-    late = held == ((row & 3) + 8).astype(f32)
+        return hit.astype(f32).reshape(part * 8, tokens).astype(bf16)
+
+    out[:, :d] = mm(placing(rank == row.astype(f32)), normed[...]).astype(bf16)
+    late = rank == ((row & 3) + 8).astype(f32)
     first, last = placing(late & (row < 4)), placing(late & (row >= 4))
-    out[:, d:] = (mm(first, xn[:, :half]) + mm(last, xn[:, half:])).astype(bf16)
+    out[:, d:] = (mm(first, normed[:, :half]) + mm(last, normed[:, half:])).astype(bf16)
 
 
 def shares_body(ids, prob, scores, ranks, share8, share4):
@@ -108,33 +122,63 @@
     return (gate / (1.0 + jnp.exp(-gate)) * upper).astype(bf16)
 
 
-def ffn_body(x, wg, wu, wd, out):
+def ffn_body(x_far, wg_far, wu_far, wd_far, out, x, wg, wu, wd, made, sems, x_sems, out_sems):
     d, width = wg.shape
     half = d // 2
-    x8 = x[:, :d]
-    hidden = silu_mul(mm(x8, wg[...]), mm(x8, wu[...]))
-    out[:, :d] = mm(hidden, wd[...]).astype(bf16)
-    x4 = x[:, d:]
-    rows = x4.shape[0]
-    first = (iota((rows, 1), 0) & 4) == 0
-
-    def joined(w):
+    loads = [
+        pltpu.make_async_copy(far, near, sems.at[k])
+        for k, (far, near) in enumerate(((wg_far, wg), (wu_far, wu), (wd_far, wd)))
+    ]
+    block = made.shape[1]
+    steps = out.shape[0] // block
+    arrivals = [
+        pltpu.make_async_copy(
+            x_far.at[pl.ds(step * block, block), :],
+            x.at[pl.ds(step * block, block), :],
+            x_sems.at[step],
+        )
+        for step in range(steps)
+    ]
+    for load in (arrivals[0], *loads, *arrivals[1:]):
+        load.start()
+    first = (iota((block, 1), 0) & 4) == 0
+
+    def joined(x4, w):
         z = jnp.where(first, mm(x4, w[:half, :]), mm(x4, w[half:, :]))
-        z3 = z.reshape(rows // 8, 8, width)
-        return (z3 + pltpu.roll(z3, 4, 1)).reshape(rows, width)
-
-    hidden = silu_mul(joined(wg), joined(wu))
-    out[:, d:] = jnp.where(first, mm(hidden, wd[:, :half]), mm(hidden, wd[:, half:])).astype(bf16)
-
-
-def combine_body(share8, share4, back, out):
-    tokens, d = out.shape
-    half = d // 2
-    late = back[:, d:]
-    for h in range(2):
-        cols = slice(h * half, (h + 1) * half)
-        total = mm(share8[...], back[:, cols]) + mm(share4[h], late)
-        out[:, cols] = (total[:tokens] + total[tokens:]).astype(bf16)
+        z3 = z.reshape(block // 8, 8, width)
+        return (z3 + pltpu.roll(z3, 4, 1)).reshape(block, width)
+
+    def store(step):
+        return pltpu.make_async_copy(
+            made.at[step], out.at[pl.ds(step * block, block), :], out_sems.at[step]
+        )
+
+    for step in range(steps):
+        rows = slice(step * block, (step + 1) * block)
+        arrivals[step].wait()
+        x8, x4 = x[rows, :d], x[rows, d:]
+        if step == 0:
+            loads[0].wait()
+        gate8, gate4 = mm(x8, wg[...]), joined(x4, wg)
+        if step == 0:
+            loads[1].wait()
+        hidden8 = silu_mul(gate8, mm(x8, wu[...]))
+        hidden4 = silu_mul(gate4, joined(x4, wu))
+        if step == 0:
+            loads[2].wait()
+        made[step, :, :d] = mm(hidden8, wd[...]).astype(bf16)
+        made[step, :, d:] = jnp.where(
+            first, mm(hidden4, wd[:, :half]), mm(hidden4, wd[:, half:])
+        ).astype(bf16)
+        store(step).start()
+    for step in range(steps):
+        store(step).wait()
+
+
+def combine_body(share8, share4, early, late, out):
+    tokens = out.shape[0]
+    total = mm(share8[...], early[...]) + mm(share4[0], late[...])
+    out[...] = (total[:tokens] + total[tokens:]).astype(bf16)
 
 
 def running_keep(forget, boosts):
@@ -164,7 +208,7 @@
     return normer, total, peak
 
 
-def summary_body(keys, values, gates, forget, boosts, out):
+def summary_body(keys, values, gates, forget, boosts, out, rest):
     b = running_keep(forget, boosts)
     length = b.shape[1]
     width = keys.shape[1]
@@ -174,11 +218,14 @@
     spread = jnp.exp(gap - peak) * (width**-0.5)
     k = keys[...]
     scaled = (values[...].astype(f32).T * spread).astype(bf16)
-    out[:width, :] = mm(scaled, k).astype(bf16)
+    half = width // 2
+    memory = mm(scaled, k).astype(bf16)
+    out[:half, :] = memory[:half]
+    rest[...] = memory[half:]
     hi, lo = halves(spread)
     two = jnp.concatenate([hi.astype(f32), lo.astype(f32), jnp.zeros((6, length), f32)], axis=0)
     normer = jnp.sum(mm(two.astype(bf16), k), axis=0, keepdims=True)
-    out[width:, :] = side_rows(normer, last, peak).astype(bf16)
+    out[half:, :] = side_rows(normer, last, peak).astype(bf16)
 
 
 def weighted(pieces, logs, floor):
@@ -209,14 +256,16 @@
     return [(jnp.where(k, c, 0.0), jnp.where(k, n, 0.0)) for k, (c, n) in zip(kept, pieces)]
 
 
-def plane_body(where, got, out, own, small, whole_memory):
+def plane_body(where, got, more, out, own, small, whole_memory):
     mine = where[1]
     width = got.shape[2]
+    half = width // 2
     count = got.shape[0]
     pieces, totals, peaks = [], [], []
     for j in range(count):
-        normer, total, peak = read_side(got[j, width:, :].astype(f32))
-        pieces.append((got[j, :width, :].astype(f32), normer))
+        normer, total, peak = read_side(got[j, half:, :].astype(f32))
+        memory = jnp.concatenate([got[j, :half, :], more[j]], axis=0).astype(f32)
+        pieces.append((memory, normer))
         totals.append(total)
         peaks.append(peak)
     logs = []
@@ -247,20 +296,21 @@
     small[3:8, :] = jnp.zeros((5, width), f32)
 
 
-def line_body(where, got, out, small):
+def line_body(where, *refs):
+    got, (out, small) = refs[:-2], refs[-2:]
     mine = where[0]
-    part = out.shape[0]
-    width = got.shape[2]
-    pieces, totals, peaks = [], [], []
-    for j in range(got.shape[0]):
-        normer, total, peak = read_side(got[j, part:, :].astype(f32))
-        pieces.append((got[j, :part, :].astype(f32), normer))
-        totals.append(total)
-        peaks.append(peak)
-    logs, kept = before(mine, totals, peaks)
-    memory, normer, stabil = weighted(
-        masked(kept, pieces), logs, jnp.full((1, 1), floor_log, f32)
-    )
+    part, width = out.shape
+    floor = jnp.full((1, 1), floor_log, f32)
+    passed = jnp.zeros((1, 1), f32)
+    pieces, logs, kept = [], [], []
+    for step, piece in enumerate(got):
+        normer, total, peak = read_side(piece[part:, :].astype(f32))
+        near = step < mine
+        pieces.append((piece[:part, :].astype(f32), normer))
+        logs.append(jnp.where(near, peak + passed, floor))
+        kept.append(near)
+        passed = passed + jnp.where(near, total, 0.0)
+    memory, normer, stabil = weighted(masked(kept, pieces), logs, floor)
     out[...] = memory.astype(bf16)
     small[0:1, :] = normer
     small[1:2, :] = jnp.broadcast_to(stabil, (1, width))
@@ -346,12 +396,13 @@
     tokens, d = rows.shape
     hidden = w_gate.shape[2]
     slots = devices * 8
-    plane = lax.axis_size(("ep_1", "ep_2"))
+    line, plane = lax.axis_size("ep_0"), lax.axis_size(("ep_1", "ep_2"))
     planes = lax.axis_size("tp")
     wg, wu, wd = w_gate[0], w_up[0], w_down[0]
     ids_t = ids.T
     vm = pl.BlockSpec(memory_space=pltpu.VMEM)
     sm = pl.BlockSpec(memory_space=pltpu.SMEM)
+    far_away = pl.BlockSpec(memory_space=pltpu.HBM)
     where = jnp.stack(
         [lax.axis_index("ep_0"), lax.axis_index(("ep_1", "ep_2")), lax.axis_index("tp")]
     ).astype(i32)
@@ -363,11 +414,19 @@
         rows,
         row_gain.reshape(1, d),
         cost=4 * slots * tokens * d,
+        grid=(4,),
+        specs=[whole(2, tokens), whole(tokens, d), whole(1, d)],
+        out_specs=(
+            pl.BlockSpec((slots // 4, d + d // 2), lambda i: (i, 0)),
+            whole(devices, tokens),
+        ),
+        scratch=(pltpu.VMEM((tokens, d), bf16), pltpu.VMEM((devices, tokens), f32)),
+        vmem=60,
     )
     got = exchanged(out.reshape(devices, 8, d + d // 2), EP)
-    send = call(
+    send, rest = call(
         summary_body,
-        struct((width + 8, width), bf16),
+        (struct((width // 2 + 8, width), bf16), struct((width // 2, width), bf16)),
         after(keys, out),
         values,
         in_gates,
@@ -376,6 +435,7 @@
         cost=2 * positions * width * width * 4,
     )
     states = lax.all_gather(send, ("ep_1", "ep_2"))
+    more = lax.all_gather(after(rest, states), ("ep_1", "ep_2"))
     send, own, near = call(
         plane_body,
         (
@@ -385,18 +445,22 @@
         ),
         where,
         states,
+        more,
         cost=4 * plane * width * width * 100,
         scratch=(pltpu.VMEM((width, width), f32),),
-        specs=[sm, vm],
-    )
-    states = lax.all_gather(send, "ep_0")
+        specs=[sm, vm, vm],
+    )
+    states = [
+        lax.ppermute(send, "ep_0", [(i, i + step) for i in range(line - step)])
+        for step in range(1, line)
+    ]
     send, far = call(
         line_body,
         (struct((width // plane, width), bf16), struct((8, width), f32)),
         where,
-        states,
+        *states,
         cost=4 * width * width * 100,
-        specs=[sm, vm],
+        specs=[sm] + [vm] * (line - 1),
     )
     share8, share4 = call(
         shares_body,
@@ -411,14 +475,24 @@
     answers = call(
         ffn_body,
         struct((slots, d + d // 2), bf16),
-        got.reshape(slots, d + d // 2),
+        after(got, send).reshape(slots, d + d // 2),
         wg,
         wu,
         wd,
         cost=12 * slots * d * hidden,
-        grid=(slots // block,),
-        specs=[pl.BlockSpec((block, d + d // 2), lambda i: (i, 0)), vm, vm, vm],
-        out_specs=pl.BlockSpec((block, d + d // 2), lambda i: (i, 0)),
+        specs=[far_away] * 4,
+        out_specs=far_away,
+        scratch=(
+            pltpu.VMEM((slots, d + d // 2), bf16),
+            pltpu.VMEM((d, hidden), bf16),
+            pltpu.VMEM((d, hidden), bf16),
+            pltpu.VMEM((hidden, d), bf16),
+            pltpu.VMEM((slots // block, block, d + d // 2), bf16),
+            pltpu.SemaphoreType.DMA((3,)),
+            pltpu.SemaphoreType.DMA((slots // block,)),
+            pltpu.SemaphoreType.DMA((slots // block,)),
+        ),
+        vmem=50,
     )
     back = exchanged(answers.reshape(devices, 8, d + d // 2), EP)
     state = lax.all_gather(send, ("ep_1", "ep_2"), tiled=True)
@@ -458,13 +532,25 @@
         cost=20 * positions * width * d,
         specs=[sm] + [vm] * (planes + 2),
     )
+    part = d // 4
+    back = back.reshape(slots, d + d // 2)
     routed_rows = call(
         combine_body,
         struct((tokens, d), bf16),
         share8,
         share4,
-        back.reshape(slots, d + d // 2),
+        back,
+        back,
         cost=12 * tokens * slots * d,
+        grid=(4,),
+        specs=[
+            whole(2 * tokens, slots),
+            pl.BlockSpec((1, 2 * tokens, slots), lambda i: (i // 2, 0, 0)),
+            pl.BlockSpec((slots, part), lambda i: (0, i)),
+            pl.BlockSpec((slots, part), lambda i: (0, 4 + i % 2)),
+        ],
+        out_specs=pl.BlockSpec((tokens, part), lambda i: (0, i)),
+        vmem=60,
     )
     return (mixed_rows, routed_rows)
 

time: 244 us -> 195 us (0.80); the launches traced: 240 us -> 194 us
  blocking collectives: 152 us -> 49.7 us
  starting transfers between devices: 10.7 us -> 52.4 us
  waiting for transfers between devices: 31.3 us -> 61.8 us
  between operations: 14.3 us -> 0.98 us
  local copies, waits for them, and re-layouts: 11.3 us -> 1.73 us
  Pallas kernels: 20.6 us -> 27.8 us
    all_to_all x1 -> x0, blocking collectives: 85.8 us -> none  [exchanged(): return lax.all_to_all(array, axes, split_axis=0, concat_axis=0, tiled=True)]
    all_to_all x1 -> x2, waiting for transfers between devices: 0.01 us -> 44.9 us  [exchanged(): return lax.all_to_all(array, axes, split_axis=0, concat_axis=0, tiled=True)]
    all_gather x1 -> x0, waiting for transfers between devices: 30.1 us -> none  [shards(): states = lax.all_gather(send, ('ep_1', 'ep_2'))]
    ppermute x0 -> x7, starting transfers between devices: none -> 22.9 us  [shards(): lax.ppermute(send, 'ep_0', [(i, i + step) for i in range(line - step)])]
    all_gather x1 -> x2, blocking collectives: 52.7 us -> 32.5 us  [the longest x1 18.5 us: shards(): states = lax.all_gather(send, ('ep_1', 'ep_2'))]
    all_to_all x1 -> x2, starting transfers between devices: 5.71 us -> 24.5 us  [exchanged(): return lax.all_to_all(array, axes, split_axis=0, concat_axis=0, tiled=True)]
    ppermute x0 -> x7, waiting for transfers between devices: none -> 16.4 us  [shards(): lax.ppermute(send, 'ep_0', [(i, i + step) for i in range(line - step)])]
    unnamed x52 -> x32, local copies, waits for them, and re-layouts: 11.2 us -> 1.7 us
  transfers between devices with their start and end apart: 5 -> 12, of which waited for: 3 -> 4; matrix products, arithmetic and copies ran while one was open for 0% -> 0% of each run, Pallas kernels for 3% -> 4%
where the time goes in v2:
time: 195 us; the launch traced here: 194 us
  waiting for transfers between devices  61.8 us (32%)
  starting transfers between devices  52.4 us (27%)
  blocking collectives  49.7 us (25%)
  Pallas kernels  27.8 us (14%)
    all_to_all x2, waiting for transfers between devices, exchanged(): return lax.all_to_all(array, axes, split_axis=0, concat_axis=0, tiled=True)  44.9 us
    pallas_call x9, Pallas kernels, call(): pl.pallas_call(body, out_shape=out_shape, scratch_shapes=list(scratch), c...  27.8 us
    all_to_all x2, starting transfers between devices, exchanged(): return lax.all_to_all(array, axes, split_axis=0, concat_axis=0, tiled=True)  24.5 us
    ppermute x7, starting transfers between devices, shards(): lax.ppermute(send, 'ep_0', [(i, i + step) for i in range(line - step)])  22.9 us
    all_gather x1, blocking collectives, shards(): states = lax.all_gather(send, ('ep_1', 'ep_2'))  18.5 us
    all_gather x1, blocking collectives, shards(): state = lax.all_gather(send, ('ep_1', 'ep_2'), tiled=True)  17.2 us
    ppermute x7, waiting for transfers between devices, shards(): lax.ppermute(send, 'ep_0', [(i, i + step) for i in range(line - step)])  16.4 us
    all_gather x1, blocking collectives, shards(): more = lax.all_gather(after(rest, states), ('ep_1', 'ep_2'))  14 us
  transfers between devices with their start and end apart: 12, of which 4 were waited for; matrix products, arithmetic and copies ran while one was open for 0% of the time, Pallas kernels for 4%

profile of v2, /device:TPU:8, one launch (start us, length us, event | category | flops | bytes accessed | tf_op | source)
XLA Modules:
  0.0 194.4 jit_solution(5934081610399975941)
XLA Ops:
  0.6 4.6 %shard_map.176 = (bf16[512,3072]{1,0:T(8,128)(2,1)}, f32[64,192]{1,0:T(8,128)}) custom-call(s32[2,192]{1,0:T(2,128)} %bitcast.22, bf16[192,2048]{1,0:T(8,128)(2,1)} %rows.1, f32[1,2048]{1,0:T(1,128)} %bitcast.31), custom_call_target="tpu_custom_call" | custom-call | flops 805306368 | bytes 1610612 | tf_op jit(solution)/shard_map/pallas_call | solution.py:53
  5.3 12.3 %all-to-all-start = ((bf16[64,8,3072]{2,1,0:T(8,128)(2,1)}), bf16[64,8,3072]{2,1,0:T(8,128)(2,1)}, u32[]{:S(2)}, u32[]{:S(2)}) async-start(bf16[64,8,3072]{2,1,0:T(8,128)(2,1)} %bitcast.28), calls=%async_computation | async-start | bytes 6291456 | tf_op jit(solution)/shard_map/all_to_all | solution.py:368
  18.3 18.5 %all-gather = bf16[1088,256]{1,0:T(8,128)(2,1)S(1)} all-gather(bf16[136,256]{1,0:T(8,128)(2,1)S(1)} %get-tuple-element.19), channel_id=2, replica_groups=mesh['ep_0'=8,'ep_1'=4,'ep_2'=2,'tp'=4] {'ep_1','ep_2'}, dimensions={0}, use_global_device_ids=true | all-gather | bytes 626688 | tf_op jit(solution)/shard_map/all_gather | solution.py:437
  36.9 14.0 %all-gather.1 = bf16[1024,256]{1,0:T(8,128)(2,1)S(1)} all-gather(bf16[128,256]{1,0:T(8,128)(2,1)S(1)} %get-tuple-element.21), channel_id=3, replica_groups=mesh['ep_0'=8,'ep_1'=4,'ep_2'=2,'tp'=4] {'ep_1','ep_2'}, dimensions={0}, use_global_device_ids=true | all-gather | bytes 589824 | tf_op jit(solution)/shard_map/all_gather | solution.py:438
  50.9 1.5 shard_map.178
  52.4 7.9 %collective-permute-start.6 = (bf16[40,256]{1,0:T(8,128)(2,1)S(1)}, bf16[40,256]{1,0:T(8,128)(2,1)S(1)}, u32[]{:S(2)}, u32[]{:S(2)}) collective-permute-start(bf16[40,256]{1,0:T(8,128)(2,1)S(1)} %get-tuple-element.22), channel_id=1, source_target_pairs={{0,224},{1,225},{2,226},{3,227},{4,228},{5,229},{6,230},{7,231},{8... | collective-permute-start | bytes 61448 | tf_op jit(solution)/shard_map/ppermute | solution.py:454
  60.3 1.3 collective-permute-start.5
  61.6 1.3 collective-permute-start.4
  62.9 2.1 %collective-permute-start.3 = (bf16[40,256]{1,0:T(8,128)(2,1)S(1)}, bf16[40,256]{1,0:T(8,128)(2,1)S(1)}, u32[]{:S(2)}, u32[]{:S(2)}) collective-permute-start(bf16[40,256]{1,0:T(8,128)(2,1)S(1)} %get-tuple-element.22), channel_id=1, source_target_pairs={{0,128},{32,160},{64,192},{96,224},{1,129},{33,161},{65,193},{97,2... | collective-permute-start | bytes 61448 | tf_op jit(solution)/shard_map/ppermute | solution.py:454
  65.1 4.3 %collective-permute-start.2 = (bf16[40,256]{1,0:T(8,128)(2,1)S(1)}, bf16[40,256]{1,0:T(8,128)(2,1)S(1)}, u32[]{:S(2)}, u32[]{:S(2)}) collective-permute-start(bf16[40,256]{1,0:T(8,128)(2,1)S(1)} %get-tuple-element.22), channel_id=1, source_target_pairs={{0,96},{32,128},{64,160},{96,192},{128,224},{1,97},{33,129},{65,16... | collective-permute-start | bytes 61448 | tf_op jit(solution)/shard_map/ppermute | solution.py:454
  69.4 15.0 %collective-permute-done.6.refs_6_ = bf16[40,256]{1,0:T(8,128)(2,1)S(1)} collective-permute-done((bf16[40,256]{1,0:T(8,128)(2,1)S(1)}, bf16[40,256]{1,0:T(8,128)(2,1)S(1)}, u32[]{:S(2)}, u32[]{:S(2)}) %collective-permute-start.6) | collective-permute-done | bytes 20512 | tf_op jit(solution)/shard_map/ppermute | solution.py:454
  84.4 1.3 collective-permute-start.1
  85.7 4.7 %collective-permute-start = (bf16[40,256]{1,0:T(8,128)(2,1)S(1)}, bf16[40,256]{1,0:T(8,128)(2,1)S(1)}, u32[]{:S(2)}, u32[]{:S(2)}) collective-permute-start(bf16[40,256]{1,0:T(8,128)(2,1)S(1)} %get-tuple-element.22), channel_id=1, source_target_pairs={{0,32},{32,64},{64,96},{96,128},{128,160},{160,192},{192,224},{1,3... | collective-permute-start | bytes 61448 | tf_op jit(solution)/shard_map/ppermute | solution.py:454
  90.4 1.4 collective-permute-done.refs_0_
  92.7 10.3 %shard_map.183 = bf16[512,3072]{1,0:T(8,128)(2,1)} custom-call(bf16[512,3072]{1,0:T(8,128)(2,1)} %bitcast.12.x_far, bf16[2048,512]{1,0:T(8,128)(2,1)S(1)} %bitcast.20, bf16[2048,512]{1,0:T(8,128)(2,1)} %bitcast.29, bf16[512,2048]{1,0:T(8,128)(2,1)} %bitcast.30), custom_call_target="tpu_custom_call" | custom-call | flops 6442450944 | bytes 12884901 | tf_op jit(solution)/shard_map/pallas_call | solution.py:53
  103.0 12.2 %all-to-all-start.1 = ((bf16[64,8,3072]{2,1,0:T(8,128)(2,1)}), bf16[64,8,3072]{2,1,0:T(8,128)(2,1)}, u32[]{:S(2)}, u32[]{:S(2)}) async-start(bf16[64,8,3072]{2,1,0:T(8,128)(2,1)} %bitcast.27), calls=%async_computation.1 | async-start | bytes 6291456 | tf_op jit(solution)/shard_map/all_to_all | solution.py:368
  115.2 17.2 %all_gather.19.state = bf16[256,256]{1,0:T(8,128)(2,1)S(1)} all-gather(bf16[32,256]{1,0:T(8,128)(2,1)S(1)} %get-tuple-element.23), channel_id=1, replica_groups=mesh['ep_0'=8,'ep_1'=4,'ep_2'=2,'tp'=4] {'ep_1','ep_2'}, dimensions={0}, use_global_device_ids=true | all-gather | bytes 147456 | tf_op jit(solution)/shard_map/all_gather | solution.py:498
  132.4 1.7 shard_map.180
  134.7 2.6 %collective-permute-start.8 = (bf16[128,256]{1,0:T(8,128)(2,1)S(1)}, bf16[128,256]{1,0:T(8,128)(2,1)S(1)}, u32[]{:S(2)}, u32[]{:S(2)}) collective-permute-start(bf16[128,256]{1,0:T(8,128)(2,1)S(1)} %get-tuple-element.33), channel_id=1, source_target_pairs={{0,2},{1,3},{2,0},{3,1},{4,6},{5,7},{6,4},{7,5},{8,10},{9,11},{10,... | collective-permute-start | bytes 196616 | tf_op jit(solution)/shard_map/ppermute | solution.py:523
  137.3 1.9 collective-permute-start.7
  139.7 0.9 copy-done.13
  141.8 2.2 %shard_map.181 = bf16[128,2048]{1,0:T(8,128)(2,1)} custom-call(s32[3]{0:T(128)S(1)} %pad_add_fusion.where, bf16[128,256]{1,0:T(8,128)(2,1)S(1)} %get-tuple-element.35.refs_0_, bf16[128,256]{1,0:T(8,128)(2,1)S(1)} %collective-permute-done.7.refs_1_, bf16[128,256]{1,0:T(8,128)(2,1)S(1)} %collective-permute-done.8.refs_2_, ...), custom_call_target="tpu_custom_call" | custom-call | flops 5368709120 | bytes 10737418 | tf_op jit(solution)/shard_map/pallas_call | solution.py:53
  144.0 44.9 %all-to-all-done.1 = bf16[64,8,3072]{2,1,0:T(8,128)(2,1)} async-done(((bf16[64,8,3072]{2,1,0:T(8,128)(2,1)}), bf16[64,8,3072]{2,1,0:T(8,128)(2,1)}, u32[]{:S(2)}, u32[]{:S(2)}) %all-to-all-start.1) | async-done | bytes 3145760 | tf_op jit(solution)/shard_map/all_to_all | solution.py:368
  188.9 5.5 %shard_map.184 = bf16[192,2048]{1,0:T(8,128)(2,1)} custom-call(bf16[384,512]{1,0:T(8,128)(2,1)} %copy-done.14, bf16[2,384,512]{2,1,0:T(8,128)(2,1)} %copy-done.13, bf16[512,3072]{1,0:T(8,128)(2,1)} %bitcast.17.early.late, bf16[512,3072]{1,0:T(8,128)(2,1)} %bitcast.17.early.late), custom_call_target="tpu_custom_call" | custom-call | flops 2415919104 | bytes 4831838 | tf_op jit(solution)/shard_map/pallas_call | solution.py:53
  (46 shorter events, 3.9 us)
Async XLA Ops:
  5.2 12.4 %copy-start.3 = (bf16[512,256]{1,0:T(8,128)(2,1)S(1)}, bf16[512,256]{1,0:T(8,128)(2,1)}, u32[]{:S(2)}) copy-start(bf16[512,256]{1,0:T(8,128)(2,1)} %keys.2) | copy-start | bytes 786436
  5.2 12.4 %copy-start.4 = (bf16[512,256]{1,0:T(8,128)(2,1)S(1)}, bf16[512,256]{1,0:T(8,128)(2,1)}, u32[]{:S(2)}) copy-start(bf16[512,256]{1,0:T(8,128)(2,1)} %values.3) | copy-start | bytes 786436
  5.3 12.4 %copy-start.6 = (f32[1,512]{1,0:T(1,128)S(1)}, f32[1,512]{1,0:T(1,128)}, u32[]{:S(2)}) copy-start(f32[1,512]{1,0:T(1,128)} %gates.3) | copy-start | bytes 6148
  5.3 12.4 %copy-start.7 = (f32[1,512]{1,0:T(1,128)S(1)}, f32[1,512]{1,0:T(1,128)}, u32[]{:S(2)}) copy-start(f32[1,512]{1,0:T(1,128)} %forget.3) | copy-start | bytes 6148
  5.3 12.4 %copy-start.8 = (f32[1,512]{1,0:T(1,128)S(1)}, f32[1,512]{1,0:T(1,128)}, u32[]{:S(2)}) copy-start(f32[1,512]{1,0:T(1,128)} %boosts.3) | copy-start | bytes 6148
  5.3 87.4 %all-to-all-start = ((bf16[64,8,3072]{2,1,0:T(8,128)(2,1)}), bf16[64,8,3072]{2,1,0:T(8,128)(2,1)}, u32[]{:S(2)}, u32[]{:S(2)}) async-start(bf16[64,8,3072]{2,1,0:T(8,128)(2,1)} %bitcast.28), calls=%async_computation | async-start | bytes 6291456 | tf_op jit(solution)/shard_map/all_to_all | solution.py:368
  17.6 75.1 %copy-start.1 = (bf16[1,2048,512]{2,1,0:T(8,128)(2,1)S(1)}, bf16[1,2048,512]{2,1,0:T(8,128)(2,1)}, u32[]{:S(2)}) copy-start(bf16[1,2048,512]{2,1,0:T(8,128)(2,1)} %param.31) | copy-start | bytes 6291460
  52.4 32.0 %collective-permute-start.6 = (bf16[40,256]{1,0:T(8,128)(2,1)S(1)}, bf16[40,256]{1,0:T(8,128)(2,1)S(1)}, u32[]{:S(2)}, u32[]{:S(2)}) collective-permute-start(bf16[40,256]{1,0:T(8,128)(2,1)S(1)} %get-tuple-element.22), channel_id=1, source_target_pairs={{0,224},{1,225},{2,226},{3,227},{4,228},{5,229},{6,230},{7,231},{8... | collective-permute-start | bytes 61448 | tf_op jit(solution)/shard_map/ppermute | solution.py:454
  60.3 25.3 %collective-permute-start.5 = (bf16[40,256]{1,0:T(8,128)(2,1)S(1)}, bf16[40,256]{1,0:T(8,128)(2,1)S(1)}, u32[]{:S(2)}, u32[]{:S(2)}) collective-permute-start(bf16[40,256]{1,0:T(8,128)(2,1)S(1)} %get-tuple-element.22), channel_id=1, source_target_pairs={{0,192},{32,224},{1,193},{33,225},{2,194},{34,226},{3,195},{35,227... | collective-permute-start | bytes 61448 | tf_op jit(solution)/shard_map/ppermute | solution.py:454
  61.6 28.7 %collective-permute-start.4 = (bf16[40,256]{1,0:T(8,128)(2,1)S(1)}, bf16[40,256]{1,0:T(8,128)(2,1)S(1)}, u32[]{:S(2)}, u32[]{:S(2)}) collective-permute-start(bf16[40,256]{1,0:T(8,128)(2,1)S(1)} %get-tuple-element.22), channel_id=1, source_target_pairs={{0,160},{32,192},{64,224},{1,161},{33,193},{65,225},{2,162},{34,19... | collective-permute-start | bytes 61448 | tf_op jit(solution)/shard_map/ppermute | solution.py:454
  62.9 27.4 %collective-permute-start.3 = (bf16[40,256]{1,0:T(8,128)(2,1)S(1)}, bf16[40,256]{1,0:T(8,128)(2,1)S(1)}, u32[]{:S(2)}, u32[]{:S(2)}) collective-permute-start(bf16[40,256]{1,0:T(8,128)(2,1)S(1)} %get-tuple-element.22), channel_id=1, source_target_pairs={{0,128},{32,160},{64,192},{96,224},{1,129},{33,161},{65,193},{97,2... | collective-permute-start | bytes 61448 | tf_op jit(solution)/shard_map/ppermute | solution.py:454
  65.1 25.3 %collective-permute-start.2 = (bf16[40,256]{1,0:T(8,128)(2,1)S(1)}, bf16[40,256]{1,0:T(8,128)(2,1)S(1)}, u32[]{:S(2)}, u32[]{:S(2)}) collective-permute-start(bf16[40,256]{1,0:T(8,128)(2,1)S(1)} %get-tuple-element.22), channel_id=1, source_target_pairs={{0,96},{32,128},{64,160},{96,192},{128,224},{1,97},{33,129},{65,16... | collective-permute-start | bytes 61448 | tf_op jit(solution)/shard_map/ppermute | solution.py:454
  84.4 6.0 %collective-permute-start.1 = (bf16[40,256]{1,0:T(8,128)(2,1)S(1)}, bf16[40,256]{1,0:T(8,128)(2,1)S(1)}, u32[]{:S(2)}, u32[]{:S(2)}) collective-permute-start(bf16[40,256]{1,0:T(8,128)(2,1)S(1)} %get-tuple-element.22), channel_id=1, source_target_pairs={{0,64},{32,96},{64,128},{96,160},{128,192},{160,224},{1,65},{33,97... | collective-permute-start | bytes 61448 | tf_op jit(solution)/shard_map/ppermute | solution.py:454
  85.7 6.1 %collective-permute-start = (bf16[40,256]{1,0:T(8,128)(2,1)S(1)}, bf16[40,256]{1,0:T(8,128)(2,1)S(1)}, u32[]{:S(2)}, u32[]{:S(2)}) collective-permute-start(bf16[40,256]{1,0:T(8,128)(2,1)S(1)} %get-tuple-element.22), channel_id=1, source_target_pairs={{0,32},{32,64},{64,96},{96,128},{128,160},{160,192},{192,224},{1,3... | collective-permute-start | bytes 61448 | tf_op jit(solution)/shard_map/ppermute | solution.py:454
  102.9 29.4 %copy-start.2 = (bf16[512,256]{1,0:T(8,128)(2,1)S(1)}, bf16[512,256]{1,0:T(8,128)(2,1)}, u32[]{:S(2)}) copy-start(bf16[512,256]{1,0:T(8,128)(2,1)} %query.1) | copy-start | bytes 786436
  103.0 29.4 %copy-start.11 = (f32[256]{0:T(256)S(1)}, f32[256]{0:T(256)}, u32[]{:S(2)}) copy-start(f32[256]{0:T(256)} %param.23) | copy-start | bytes 3076
  103.0 85.9 %all-to-all-start.1 = ((bf16[64,8,3072]{2,1,0:T(8,128)(2,1)}), bf16[64,8,3072]{2,1,0:T(8,128)(2,1)}, u32[]{:S(2)}, u32[]{:S(2)}) async-start(bf16[64,8,3072]{2,1,0:T(8,128)(2,1)} %bitcast.27), calls=%async_computation.1 | async-start | bytes 6291456 | tf_op jit(solution)/shard_map/all_to_all | solution.py:368
  132.4 6.8 %copy-start.9 = (s32[192,2]{0,1:T(2,128)S(1)}, s32[192,2]{0,1:T(2,128)}, u32[]{:S(2)}) copy-start(s32[192,2]{0,1:T(2,128)} %param.28) | copy-start | bytes 4612
  132.4 6.8 %copy-start.10 = (f32[192,2]{0,1:T(2,128)S(1)}, f32[192,2]{0,1:T(2,128)}, u32[]{:S(2)}) copy-start(f32[192,2]{0,1:T(2,128)} %param.30) | copy-start | bytes 4612
  132.4 9.4 %copy-start = (bf16[1024,2048]{1,0:T(8,128)(2,1)S(1)}, bf16[1024,2048]{1,0:T(8,128)(2,1)}, u32[]{:S(2)}) copy-start(bf16[1024,2048]{1,0:T(8,128)(2,1)} %refs_4_.1) | copy-start | bytes 12582916
  132.4 9.4 %copy-start.5 = (f32[2048]{0:T(1024)S(1)}, f32[2048]{0:T(1024)}, u32[]{:S(2)}) copy-start(f32[2048]{0:T(1024)} %param.25) | copy-start | bytes 24580
  134.2 7.1 %collective-permute-start.9 = (bf16[128,256]{1,0:T(8,128)(2,1)S(1)}, bf16[128,256]{1,0:T(8,128)(2,1)S(1)}, u32[]{:S(2)}, u32[]{:S(2)}) collective-permute-start(bf16[128,256]{1,0:T(8,128)(2,1)S(1)} %get-tuple-element.32), channel_id=1, source_target_pairs={{0,3},{1,0},{2,1},{3,2},{4,7},{5,4},{6,5},{7,6},{8,11},{9,8},{10,9... | collective-permute-start | bytes 196616 | tf_op jit(solution)/shard_map/ppermute | solution.py:523
  134.7 6.6 %collective-permute-start.8 = (bf16[128,256]{1,0:T(8,128)(2,1)S(1)}, bf16[128,256]{1,0:T(8,128)(2,1)S(1)}, u32[]{:S(2)}, u32[]{:S(2)}) collective-permute-start(bf16[128,256]{1,0:T(8,128)(2,1)S(1)} %get-tuple-element.33), channel_id=1, source_target_pairs={{0,2},{1,3},{2,0},{3,1},{4,6},{5,7},{6,4},{7,5},{8,10},{9,11},{10,... | collective-permute-start | bytes 196616 | tf_op jit(solution)/shard_map/ppermute | solution.py:523
  137.3 4.5 %collective-permute-start.7 = (bf16[128,256]{1,0:T(8,128)(2,1)S(1)}, bf16[128,256]{1,0:T(8,128)(2,1)S(1)}, u32[]{:S(2)}, u32[]{:S(2)}) collective-permute-start(bf16[128,256]{1,0:T(8,128)(2,1)S(1)} %get-tuple-element.34), channel_id=1, source_target_pairs={{0,1},{1,2},{2,3},{3,0},{4,5},{5,6},{6,7},{7,4},{8,9},{9,10},{10,1... | collective-permute-start | bytes 196616 | tf_op jit(solution)/shard_map/ppermute | solution.py:523
  (4 other events, 15.2 us)

commit v3 on v2

--- a/solution.py
+++ b/solution.py
@@ -36,10 +36,6 @@
 def halves(x):
     hi = x.astype(bf16)
     return hi, (x - hi.astype(f32)).astype(bf16)
-
-
-def whole(*shape):
-    return pl.BlockSpec(shape, lambda *_: (0,) * len(shape))
 
 
 def call(body, out_shape, *args, cost, scratch=(), specs=None, out_specs=None, grid=None, vmem=24):
@@ -64,39 +60,125 @@
     return jax.ShapeDtypeStruct(shape, dtype)
 
 
-def build_body(ids, rows, gain, out, ranks, normed, held):
-    d = rows.shape[1]
+def build_body(ids_far, rows_far, gain_far, out, ranks, ids, rows, gain, made, sems, out_sems):
+    tokens, d = rows.shape
     half = d // 2
-    experts, tokens = ranks.shape
-
-    @pl.when(pl.program_id(0) == 0)
-    def _():
-        x = rows[...].astype(f32)
-        mean = jnp.mean(x * x, axis=-1, keepdims=True)
-        normed[...] = (x * lax.rsqrt(mean + norm_eps) * gain[...]).astype(bf16)
-        expert = iota((experts, tokens), 0)
-        chosen = (ids[0:1, :] == expert) | (ids[1:2, :] == expert)
-        ahead = (iota((tokens, tokens), 0) < iota((tokens, tokens), 1)).astype(f32).astype(bf16)
-        count = mm(chosen.astype(f32).astype(bf16), ahead)
-        rank = jnp.where(chosen, count, -1.0)
-        ranks[...] = rank
-        held[...] = rank
-
-    part = out.shape[0] // 8
-    first_expert = pl.multiple_of(pl.program_id(0) * part, 8)
-    rank = held[pl.ds(first_expert, part), :][:, None, :]
+    experts = ranks.shape[0]
+    loads = [
+        pltpu.make_async_copy(far, near, sems.at[k])
+        for k, (far, near) in enumerate(((ids_far, ids), (rows_far, rows), (gain_far, gain)))
+    ]
+    for load in loads:
+        load.start()
+    ahead = (iota((tokens, tokens), 0) < iota((tokens, tokens), 1)).astype(f32).astype(bf16)
+    expert = iota((experts, tokens), 0)
+    loads[0].wait()
+    chosen = (ids[0:1, :] == expert) | (ids[1:2, :] == expert)
+    count = mm(chosen.astype(f32).astype(bf16), ahead)
+    rank = jnp.where(chosen, count, -1.0)
+    ranks[...] = rank
+    loads[1].wait()
+    x = rows[...].astype(f32)
+    mean = jnp.mean(x * x, axis=-1, keepdims=True)
+    loads[2].wait()
+    xn = (x * lax.rsqrt(mean + norm_eps) * gain[...]).astype(bf16)
+    steps, block, _ = made.shape
+    part = block // 8
     row = iota((part, 8, tokens), 1)
+    slot = row.astype(f32)
+    late_slot = ((row & 3) + 8).astype(f32)
 
     def placing(hit):
-        return hit.astype(f32).reshape(part * 8, tokens).astype(bf16)
-
-    out[:, :d] = mm(placing(rank == row.astype(f32)), normed[...]).astype(bf16)
-    late = rank == ((row & 3) + 8).astype(f32)
-    first, last = placing(late & (row < 4)), placing(late & (row >= 4))
-    out[:, d:] = (mm(first, normed[:, :half]) + mm(last, normed[:, half:])).astype(bf16)
-
-
-def shares_body(ids, prob, scores, ranks, share8, share4):
+        return hit.astype(f32).reshape(block, tokens).astype(bf16)
+
+    def store(step):
+        return pltpu.make_async_copy(
+            made.at[step], out.at[pl.ds(step * block, block), :], out_sems.at[step]
+        )
+
+    for step in range(steps):
+        held = rank[step * part : (step + 1) * part, None, :]
+        made[step, :, :d] = mm(placing(held == slot), xn).astype(bf16)
+        late = held == late_slot
+        first, last = placing(late & (row < 4)), placing(late & (row >= 4))
+        made[step, :, d:] = (mm(first, xn[:, :half]) + mm(last, xn[:, half:])).astype(bf16)
+        store(step).start()
+    for step in range(steps):
+        store(step).wait()
+
+
+def silu_mul(gate, upper):
+    return (gate / (1.0 + jnp.exp(-gate)) * upper).astype(bf16)
+
+
+def ffn_body(x_far, wg_far, wu_far, wd_far, out, x, wg, wu, wd, made, in_sems, sems):
+    d, _ = wg.shape
+    half = d // 2
+    slots = x.shape[0]
+    pieces = (
+        (x_far.at[:, pl.ds(d, half)], x.at[:, pl.ds(d, half)]),
+        (wg_far.at[pl.ds(0, half), :], wg.at[pl.ds(0, half), :]),
+        (wg_far.at[pl.ds(half, half), :], wg.at[pl.ds(half, half), :]),
+        (wu_far, wu),
+        (x_far.at[:, pl.ds(0, d)], x.at[:, pl.ds(0, d)]),
+        (wd_far, wd),
+    )
+    loads = [
+        pltpu.make_async_copy(far, near, in_sems.at[k]) for k, (far, near) in enumerate(pieces)
+    ]
+    for load in loads:
+        load.start()
+    pairs = slots // 16
+
+    def crossed(left, right):
+        upper = (iota((1, 8, 1), 1) & 4) == 0
+        return (
+            jnp.where(upper, left, pltpu.roll(right, 4, 1)),
+            jnp.where(upper, pltpu.roll(left, 4, 1), right),
+        )
+
+    loads[0].wait()
+    x4 = x[:, d:].astype(f32).reshape(pairs, 2, 8, half)
+    top, bottom = crossed(x4[:, 0], x4[:, 1])
+    top = top.reshape(pairs * 8, half).astype(bf16)
+    bottom = bottom.reshape(pairs * 8, half).astype(bf16)
+    loads[1].wait()
+    gate4 = mm(top, wg[:half, :])
+    loads[2].wait()
+    gate4 += mm(bottom, wg[half:, :])
+    loads[3].wait()
+    hidden4 = silu_mul(gate4, mm(top, wu[:half, :]) + mm(bottom, wu[half:, :]))
+    loads[4].wait()
+    x8 = x[:, :d]
+    hidden8 = silu_mul(mm(x8, wg[...]), mm(x8, wu[...]))
+    loads[5].wait()
+    part = made.shape[2]
+    stores = []
+
+    def send(step, values):
+        made[step] = values.astype(bf16)
+        stores.append(
+            pltpu.make_async_copy(
+                made.at[step], out.at[:, pl.ds(step * part, part)], sems.at[step]
+            )
+        )
+        stores[-1].start()
+
+    early = d // part
+    for step in range(early):
+        send(step, mm(hidden8, wd[:, step * part : (step + 1) * part]))
+    for step in range(half // part):
+        cols = slice(step * part, (step + 1) * part)
+        far = slice(half + step * part, half + (step + 1) * part)
+        left = mm(hidden4, wd[:, cols]).reshape(pairs, 8, part)
+        right = mm(hidden4, wd[:, far]).reshape(pairs, 8, part)
+        both = jnp.stack(crossed(left, right), axis=1)
+        send(early + step, both.reshape(slots, part))
+    for store in stores:
+        store.wait()
+
+
+def combine_body(ids, prob, scores, ranks, back, out):
     rank = ranks[...]
     experts, tokens = rank.shape
     s0, s1 = scores[0:1, :], scores[1:2, :]
@@ -108,77 +190,18 @@
     share = jnp.where(ids[0:1, :] == expert, w0, 0.0) + jnp.where(ids[1:2, :] == expert, w1, 0.0)
     row = iota((experts, 8, tokens), 1)
 
-    def placed(hit, out):
-        at = jnp.where(hit, share[:, None, :], 0.0).reshape(experts * 8, tokens).T
-        out[:tokens], out[tokens:] = halves(at)
-
-    placed(rank[:, None, :] == row.astype(f32), share8)
+    def placed(hit):
+        at = jnp.where(hit, share[:, None, :], 0.0).reshape(experts * 8, tokens)
+        return at.T.astype(bf16)
+
+    early = placed(rank[:, None, :] == row.astype(f32))
     hit = rank[:, None, :] == ((row & 3) + 8).astype(f32)
+    half = out.shape[1] // 2
+    late = back[:, 2 * half :]
     for h in range(2):
-        placed(hit & ((row >> 2) == h), share4.at[h])
-
-
-def silu_mul(gate, upper):
-    return (gate / (1.0 + jnp.exp(-gate)) * upper).astype(bf16)
-
-
-def ffn_body(x_far, wg_far, wu_far, wd_far, out, x, wg, wu, wd, made, sems, x_sems, out_sems):
-    d, width = wg.shape
-    half = d // 2
-    loads = [
-        pltpu.make_async_copy(far, near, sems.at[k])
-        for k, (far, near) in enumerate(((wg_far, wg), (wu_far, wu), (wd_far, wd)))
-    ]
-    block = made.shape[1]
-    steps = out.shape[0] // block
-    arrivals = [
-        pltpu.make_async_copy(
-            x_far.at[pl.ds(step * block, block), :],
-            x.at[pl.ds(step * block, block), :],
-            x_sems.at[step],
-        )
-        for step in range(steps)
-    ]
-    for load in (arrivals[0], *loads, *arrivals[1:]):
-        load.start()
-    first = (iota((block, 1), 0) & 4) == 0
-
-    def joined(x4, w):
-        z = jnp.where(first, mm(x4, w[:half, :]), mm(x4, w[half:, :]))
-        z3 = z.reshape(block // 8, 8, width)
-        return (z3 + pltpu.roll(z3, 4, 1)).reshape(block, width)
-
-    def store(step):
-        return pltpu.make_async_copy(
-            made.at[step], out.at[pl.ds(step * block, block), :], out_sems.at[step]
-        )
-
-    for step in range(steps):
-        rows = slice(step * block, (step + 1) * block)
-        arrivals[step].wait()
-        x8, x4 = x[rows, :d], x[rows, d:]
-        if step == 0:
-            loads[0].wait()
-        gate8, gate4 = mm(x8, wg[...]), joined(x4, wg)
-        if step == 0:
-            loads[1].wait()
-        hidden8 = silu_mul(gate8, mm(x8, wu[...]))
-        hidden4 = silu_mul(gate4, joined(x4, wu))
-        if step == 0:
-            loads[2].wait()
-        made[step, :, :d] = mm(hidden8, wd[...]).astype(bf16)
-        made[step, :, d:] = jnp.where(
-            first, mm(hidden4, wd[:, :half]), mm(hidden4, wd[:, half:])
-        ).astype(bf16)
-        store(step).start()
-    for step in range(steps):
-        store(step).wait()
-
-
-def combine_body(share8, share4, early, late, out):
-    tokens = out.shape[0]
-    total = mm(share8[...], early[...]) + mm(share4[0], late[...])
-    out[...] = (total[:tokens] + total[tokens:]).astype(bf16)
+        cols = slice(h * half, (h + 1) * half)
+        extra = mm(placed(hit & ((row >> 2) == h)), late)
+        out[:, cols] = (mm(early, back[:, cols]) + extra).astype(bf16)
 
 
 def running_keep(forget, boosts):
@@ -398,7 +421,6 @@
     slots = devices * 8
     line, plane = lax.axis_size("ep_0"), lax.axis_size(("ep_1", "ep_2"))
     planes = lax.axis_size("tp")
-    wg, wu, wd = w_gate[0], w_up[0], w_down[0]
     ids_t = ids.T
     vm = pl.BlockSpec(memory_space=pltpu.VMEM)
     sm = pl.BlockSpec(memory_space=pltpu.SMEM)
@@ -414,13 +436,16 @@
         rows,
         row_gain.reshape(1, d),
         cost=4 * slots * tokens * d,
-        grid=(4,),
-        specs=[whole(2, tokens), whole(tokens, d), whole(1, d)],
-        out_specs=(
-            pl.BlockSpec((slots // 4, d + d // 2), lambda i: (i, 0)),
-            whole(devices, tokens),
+        specs=[far_away] * 3,
+        out_specs=(far_away, vm),
+        scratch=(
+            pltpu.VMEM((2, tokens), i32),
+            pltpu.VMEM((tokens, d), bf16),
+            pltpu.VMEM((1, d), f32),
+            pltpu.VMEM((4, slots // 4, d + d // 2), bf16),
+            pltpu.SemaphoreType.DMA((3,)),
+            pltpu.SemaphoreType.DMA((4,)),
         ),
-        scratch=(pltpu.VMEM((tokens, d), bf16), pltpu.VMEM((devices, tokens), f32)),
         vmem=60,
     )
     got = exchanged(out.reshape(devices, 8, d + d // 2), EP)
@@ -462,23 +487,13 @@
         cost=4 * width * width * 100,
         specs=[sm] + [vm] * (line - 1),
     )
-    share8, share4 = call(
-        shares_body,
-        (struct((2 * tokens, slots), bf16), struct((2, 2 * tokens, slots), bf16)),
-        ids_t,
-        prob.reshape(1, tokens),
-        scores.T,
-        after(ranks, out),
-        cost=slots * tokens * 1000,
-    )
-    block = 128
     answers = call(
         ffn_body,
         struct((slots, d + d // 2), bf16),
         after(got, send).reshape(slots, d + d // 2),
-        wg,
-        wu,
-        wd,
+        w_gate[0],
+        w_up[0],
+        w_down[0],
         cost=12 * slots * d * hidden,
         specs=[far_away] * 4,
         out_specs=far_away,
@@ -487,12 +502,11 @@
             pltpu.VMEM((d, hidden), bf16),
             pltpu.VMEM((d, hidden), bf16),
             pltpu.VMEM((hidden, d), bf16),
-            pltpu.VMEM((slots // block, block, d + d // 2), bf16),
-            pltpu.SemaphoreType.DMA((3,)),
-            pltpu.SemaphoreType.DMA((slots // block,)),
-            pltpu.SemaphoreType.DMA((slots // block,)),
+            pltpu.VMEM((6, slots, d // 4), bf16),
+            pltpu.SemaphoreType.DMA((6,)),
+            pltpu.SemaphoreType.DMA((6,)),
         ),
-        vmem=50,
+        vmem=60,
     )
     back = exchanged(answers.reshape(devices, 8, d + d // 2), EP)
     state = lax.all_gather(send, ("ep_1", "ep_2"), tiled=True)
@@ -532,25 +546,16 @@
         cost=20 * positions * width * d,
         specs=[sm] + [vm] * (planes + 2),
     )
-    part = d // 4
-    back = back.reshape(slots, d + d // 2)
     routed_rows = call(
         combine_body,
         struct((tokens, d), bf16),
-        share8,
-        share4,
-        back,
-        back,
+        ids_t,
+        prob.reshape(1, tokens),
+        scores.T,
+        ranks,
+        back.reshape(slots, d + d // 2),
         cost=12 * tokens * slots * d,
-        grid=(4,),
-        specs=[
-            whole(2 * tokens, slots),
-            pl.BlockSpec((1, 2 * tokens, slots), lambda i: (i // 2, 0, 0)),
-            pl.BlockSpec((slots, part), lambda i: (0, i)),
-            pl.BlockSpec((slots, part), lambda i: (0, 4 + i % 2)),
-        ],
-        out_specs=pl.BlockSpec((tokens, part), lambda i: (0, i)),
-        vmem=60,
+        vmem=16,
     )
     return (mixed_rows, routed_rows)
 

time: 195 us -> 189 us (0.969)
  Pallas kernels: 27.8 us -> 21.7 us
  waiting for transfers between devices: 61.8 us -> 58.6 us
    pallas_call x9 -> x8, Pallas kernels: 27.8 us -> 21.7 us  [call(): pl.pallas_call(body, out_shape=out_shape, scratch_shapes=list(scratch), c...]
    ppermute x7, starting transfers between devices: 22.9 us -> 28.3 us  [shards(): lax.ppermute(send, 'ep_0', [(i, i + step) for i in range(line - step)])]
    all_to_all x2, starting transfers between devices: 24.5 us -> 20.6 us  [exchanged(): return lax.all_to_all(array, axes, split_axis=0, concat_axis=0, tiled=True)]
    all_to_all x2, waiting for transfers between devices: 44.9 us -> 41.6 us  [exchanged(): return lax.all_to_all(array, axes, split_axis=0, concat_axis=0, tiled=True)]
    ppermute x3, waiting for transfers between devices: 0.48 us -> 2.93 us  [shards(): piece = lax.ppermute(piece, 'tp', ring)]
    ppermute x7, waiting for transfers between devices: 16.4 us -> 14 us  [shards(): lax.ppermute(send, 'ep_0', [(i, i + step) for i in range(line - step)])]
  transfers between devices with their start and end apart: 12 -> 12, of which waited for: 4 -> 5; matrix products, arithmetic and copies ran while one was open for 0% -> 0% of each run, Pallas kernels for 4% -> 4%
where the time goes in v3:
time: 189 us
  waiting for transfers between devices  58.6 us (31%)
  starting transfers between devices  53.9 us (29%)
  blocking collectives  49.9 us (26%)
  Pallas kernels  21.7 us (11%)
  local copies, waits for them, and re-layouts  3.65 us (2%)
    all_to_all x2, waiting for transfers between devices, exchanged(): return lax.all_to_all(array, axes, split_axis=0, concat_axis=0, tiled=True)  41.6 us
    ppermute x7, starting transfers between devices, shards(): lax.ppermute(send, 'ep_0', [(i, i + step) for i in range(line - step)])  28.3 us
    pallas_call x8, Pallas kernels, call(): pl.pallas_call(body, out_shape=out_shape, scratch_shapes=list(scratch), c...  21.7 us
    all_to_all x2, starting transfers between devices, exchanged(): return lax.all_to_all(array, axes, split_axis=0, concat_axis=0, tiled=True)  20.6 us
    all_gather x1, blocking collectives, shards(): states = lax.all_gather(send, ('ep_1', 'ep_2'))  18.5 us
    all_gather x1, blocking collectives, shards(): state = lax.all_gather(send, ('ep_1', 'ep_2'), tiled=True)  17.4 us
    all_gather x1, blocking collectives, shards(): more = lax.all_gather(after(rest, states), ('ep_1', 'ep_2'))  14 us
    ppermute x7, waiting for transfers between devices, shards(): lax.ppermute(send, 'ep_0', [(i, i + step) for i in range(line - step)])  14 us
  transfers between devices with their start and end apart: 12, of which 5 were waited for; matrix products, arithmetic and copies ran while one was open for 0% of the time, Pallas kernels for 4%

profile of v3, /device:TPU:8, one launch (start us, length us, event | category | flops | bytes accessed | tf_op | source)
XLA Modules:
  0.0 188.8 jit_solution(15265564525937705113)
XLA Ops:
  0.6 4.3 %shard_map.176 = (bf16[512,3072]{1,0:T(8,128)(2,1)}, f32[64,192]{1,0:T(8,128)}) custom-call(s32[2,192]{1,0:T(2,128)} %bitcast.22, bf16[192,2048]{1,0:T(8,128)(2,1)} %rows_far.1, f32[1,2048]{1,0:T(1,128)} %bitcast.32), custom_call_target="tpu_custom_call" | custom-call | flops 805306368 | bytes 1610612 | tf_op jit(solution)/shard_map/pallas_call | solution.py:49
  5.0 12.3 %all-to-all-start = ((bf16[64,8,3072]{2,1,0:T(8,128)(2,1)}), bf16[64,8,3072]{2,1,0:T(8,128)(2,1)}, u32[]{:S(2)}, u32[]{:S(2)}) async-start(bf16[64,8,3072]{2,1,0:T(8,128)(2,1)} %bitcast.28), calls=%async_computation | async-start | bytes 6291456 | tf_op jit(solution)/shard_map/all_to_all | solution.py:391
  18.0 18.5 %all-gather = bf16[1088,256]{1,0:T(8,128)(2,1)S(1)} all-gather(bf16[136,256]{1,0:T(8,128)(2,1)S(1)} %get-tuple-element.16), channel_id=2, replica_groups=mesh['ep_0'=8,'ep_1'=4,'ep_2'=2,'tp'=4] {'ep_1','ep_2'}, dimensions={0}, use_global_device_ids=true | all-gather | bytes 626688 | tf_op jit(solution)/shard_map/all_gather | solution.py:462
  36.6 14.0 %all-gather.1 = bf16[1024,256]{1,0:T(8,128)(2,1)S(1)} all-gather(bf16[128,256]{1,0:T(8,128)(2,1)S(1)} %get-tuple-element.18), channel_id=3, replica_groups=mesh['ep_0'=8,'ep_1'=4,'ep_2'=2,'tp'=4] {'ep_1','ep_2'}, dimensions={0}, use_global_device_ids=true | all-gather | bytes 589824 | tf_op jit(solution)/shard_map/all_gather | solution.py:463
  50.6 1.5 shard_map.178
  52.9 7.1 %collective-permute-start = (bf16[40,256]{1,0:T(8,128)(2,1)S(1)}, bf16[40,256]{1,0:T(8,128)(2,1)S(1)}, u32[]{:S(2)}, u32[]{:S(2)}) collective-permute-start(bf16[40,256]{1,0:T(8,128)(2,1)S(1)} %get-tuple-element.19), channel_id=1, source_target_pairs={{0,32},{32,64},{64,96},{96,128},{128,160},{160,192},{192,224},{1,3... | collective-permute-start | bytes 61448 | tf_op jit(solution)/shard_map/ppermute | solution.py:479
  60.0 5.4 %collective-permute-start.1 = (bf16[40,256]{1,0:T(8,128)(2,1)S(1)}, bf16[40,256]{1,0:T(8,128)(2,1)S(1)}, u32[]{:S(2)}, u32[]{:S(2)}) collective-permute-start(bf16[40,256]{1,0:T(8,128)(2,1)S(1)} %get-tuple-element.19), channel_id=1, source_target_pairs={{0,64},{32,96},{64,128},{96,160},{128,192},{160,224},{1,65},{33,97... | collective-permute-start | bytes 61448 | tf_op jit(solution)/shard_map/ppermute | solution.py:479
  65.3 2.5 %collective-permute-start.2 = (bf16[40,256]{1,0:T(8,128)(2,1)S(1)}, bf16[40,256]{1,0:T(8,128)(2,1)S(1)}, u32[]{:S(2)}, u32[]{:S(2)}) collective-permute-start(bf16[40,256]{1,0:T(8,128)(2,1)S(1)} %get-tuple-element.19), channel_id=1, source_target_pairs={{0,96},{32,128},{64,160},{96,192},{128,224},{1,97},{33,129},{65,16... | collective-permute-start | bytes 61448 | tf_op jit(solution)/shard_map/ppermute | solution.py:479
  67.9 2.5 %collective-permute-start.3 = (bf16[40,256]{1,0:T(8,128)(2,1)S(1)}, bf16[40,256]{1,0:T(8,128)(2,1)S(1)}, u32[]{:S(2)}, u32[]{:S(2)}) collective-permute-start(bf16[40,256]{1,0:T(8,128)(2,1)S(1)} %get-tuple-element.19), channel_id=1, source_target_pairs={{0,128},{32,160},{64,192},{96,224},{1,129},{33,161},{65,193},{97,2... | collective-permute-start | bytes 61448 | tf_op jit(solution)/shard_map/ppermute | solution.py:479
  70.3 1.3 collective-permute-start.4
  71.6 12.6 %collective-permute-done.refs_0_ = bf16[40,256]{1,0:T(8,128)(2,1)S(1)} collective-permute-done((bf16[40,256]{1,0:T(8,128)(2,1)S(1)}, bf16[40,256]{1,0:T(8,128)(2,1)S(1)}, u32[]{:S(2)}, u32[]{:S(2)}) %collective-permute-start) | collective-permute-done | bytes 20512 | tf_op jit(solution)/shard_map/ppermute | solution.py:479
  84.2 8.2 %collective-permute-start.5 = (bf16[40,256]{1,0:T(8,128)(2,1)S(1)}, bf16[40,256]{1,0:T(8,128)(2,1)S(1)}, u32[]{:S(2)}, u32[]{:S(2)}) collective-permute-start(bf16[40,256]{1,0:T(8,128)(2,1)S(1)} %get-tuple-element.19), channel_id=1, source_target_pairs={{0,192},{32,224},{1,193},{33,225},{2,194},{34,226},{3,195},{35,227... | collective-permute-start | bytes 61448 | tf_op jit(solution)/shard_map/ppermute | solution.py:479
  92.4 1.3 collective-permute-start.6
  93.9 1.3 collective-permute-done.6.refs_6_
  96.0 8.5 %shard_map.182 = bf16[512,3072]{1,0:T(8,128)(2,1)} custom-call(bf16[512,3072]{1,0:T(8,128)(2,1)} %bitcast.12.x_far, bf16[2048,512]{1,0:T(8,128)(2,1)} %bitcast.29, bf16[2048,512]{1,0:T(8,128)(2,1)} %bitcast.30, bf16[512,2048]{1,0:T(8,128)(2,1)} %bitcast.31), custom_call_target="tpu_custom_call" | custom-call | flops 6442450944 | bytes 12884901 | tf_op jit(solution)/shard_map/pallas_call | solution.py:49
  104.5 8.3 %all-to-all-start.1 = ((bf16[64,8,3072]{2,1,0:T(8,128)(2,1)}), bf16[64,8,3072]{2,1,0:T(8,128)(2,1)S(1)}, u32[]{:S(2)}, u32[]{:S(2)}) async-start(bf16[64,8,3072]{2,1,0:T(8,128)(2,1)} %bitcast.27), calls=%async_computation.1 | async-start | bytes 6291456 | tf_op jit(solution)/shard_map/all_to_all | solution.py:391
  112.9 17.4 %all_gather.19.state = bf16[256,256]{1,0:T(8,128)(2,1)S(1)} all-gather(bf16[32,256]{1,0:T(8,128)(2,1)S(1)} %get-tuple-element.20), channel_id=1, replica_groups=mesh['ep_0'=8,'ep_1'=4,'ep_2'=2,'tp'=4] {'ep_1','ep_2'}, dimensions={0}, use_global_device_ids=true | all-gather | bytes 147456 | tf_op jit(solution)/shard_map/all_gather | solution.py:512
  133.1 1.7 shard_map.180
  134.9 1.7 collective-permute-start.7
  137.5 2.4 %collective-permute-start.9 = (bf16[128,256]{1,0:T(8,128)(2,1)S(1)}, bf16[128,256]{1,0:T(8,128)(2,1)S(1)}, u32[]{:S(2)}, u32[]{:S(2)}) collective-permute-start(bf16[128,256]{1,0:T(8,128)(2,1)S(1)} %get-tuple-element.26), channel_id=1, source_target_pairs={{0,3},{1,0},{2,1},{3,2},{4,7},{5,4},{6,5},{7,6},{8,11},{9,8},{10,9... | collective-permute-start | bytes 196616 | tf_op jit(solution)/shard_map/ppermute | solution.py:537
  139.9 2.9 %collective-permute-done.8.refs_2_ = bf16[128,256]{1,0:T(8,128)(2,1)S(1)} collective-permute-done((bf16[128,256]{1,0:T(8,128)(2,1)S(1)}, bf16[128,256]{1,0:T(8,128)(2,1)S(1)}, u32[]{:S(2)}, u32[]{:S(2)}) %collective-permute-start.8) | collective-permute-done | bytes 65568 | tf_op jit(solution)/shard_map/ppermute | solution.py:537
  142.9 2.2 %shard_map.181 = bf16[128,2048]{1,0:T(8,128)(2,1)} custom-call(s32[3]{0:T(128)S(1)} %pad_add_fusion.where, bf16[128,256]{1,0:T(8,128)(2,1)S(1)} %get-tuple-element.29.refs_0_, bf16[128,256]{1,0:T(8,128)(2,1)S(1)} %collective-permute-done.7.refs_1_, bf16[128,256]{1,0:T(8,128)(2,1)S(1)} %collective-permute-done.8.refs_2_, ...), custom_call_target="tpu_custom_call" | custom-call | flops 5368709120 | bytes 10737418 | tf_op jit(solution)/shard_map/pallas_call | solution.py:49
  145.1 41.6 %all-to-all-done.1 = bf16[64,8,3072]{2,1,0:T(8,128)(2,1)S(1)} async-done(((bf16[64,8,3072]{2,1,0:T(8,128)(2,1)}), bf16[64,8,3072]{2,1,0:T(8,128)(2,1)S(1)}, u32[]{:S(2)}, u32[]{:S(2)}) %all-to-all-start.1) | async-done | bytes 3145760 | tf_op jit(solution)/shard_map/all_to_all | solution.py:391
  186.7 2.0 %shard_map.183 = bf16[192,2048]{1,0:T(8,128)(2,1)} custom-call(s32[2,192]{1,0:T(2,128)S(1)} %bitcast.23, f32[1,192]{1,0:T(1,128)S(1)} %bitcast.26, f32[2,192]{1,0:T(2,128)S(1)} %bitcast.24, f32[64,192]{1,0:T(8,128)S(1)} %copy-done.16, bf16[512,3072]{1,0:T(8,128)(2,1)S(1)} %bitcast.18), custom_call_target="tpu_custom_call" | custom-call | flops 2415919104 | bytes 4831838 | tf_op jit(solution)/shard_map/pallas_call | solution.py:49
  (47 shorter events, 6.3 us)
Async XLA Ops:
  4.9 12.4 %copy-start.2 = (bf16[512,256]{1,0:T(8,128)(2,1)S(1)}, bf16[512,256]{1,0:T(8,128)(2,1)}, u32[]{:S(2)}) copy-start(bf16[512,256]{1,0:T(8,128)(2,1)} %keys.2) | copy-start | bytes 786436
  5.0 12.4 %copy-start.4 = (bf16[512,256]{1,0:T(8,128)(2,1)S(1)}, bf16[512,256]{1,0:T(8,128)(2,1)}, u32[]{:S(2)}) copy-start(bf16[512,256]{1,0:T(8,128)(2,1)} %values.3) | copy-start | bytes 786436
  5.0 12.4 %copy-start.9 = (f32[1,512]{1,0:T(1,128)S(1)}, f32[1,512]{1,0:T(1,128)}, u32[]{:S(2)}) copy-start(f32[1,512]{1,0:T(1,128)} %gates.3) | copy-start | bytes 6148
  5.0 12.4 %copy-start.10 = (f32[1,512]{1,0:T(1,128)S(1)}, f32[1,512]{1,0:T(1,128)}, u32[]{:S(2)}) copy-start(f32[1,512]{1,0:T(1,128)} %forget.3) | copy-start | bytes 6148
  5.0 12.4 %copy-start.11 = (f32[1,512]{1,0:T(1,128)S(1)}, f32[1,512]{1,0:T(1,128)}, u32[]{:S(2)}) copy-start(f32[1,512]{1,0:T(1,128)} %boosts.3) | copy-start | bytes 6148
  5.0 91.0 %all-to-all-start = ((bf16[64,8,3072]{2,1,0:T(8,128)(2,1)}), bf16[64,8,3072]{2,1,0:T(8,128)(2,1)}, u32[]{:S(2)}, u32[]{:S(2)}) async-start(bf16[64,8,3072]{2,1,0:T(8,128)(2,1)} %bitcast.28), calls=%async_computation | async-start | bytes 6291456 | tf_op jit(solution)/shard_map/all_to_all | solution.py:391
  52.9 31.3 %collective-permute-start = (bf16[40,256]{1,0:T(8,128)(2,1)S(1)}, bf16[40,256]{1,0:T(8,128)(2,1)S(1)}, u32[]{:S(2)}, u32[]{:S(2)}) collective-permute-start(bf16[40,256]{1,0:T(8,128)(2,1)S(1)} %get-tuple-element.19), channel_id=1, source_target_pairs={{0,32},{32,64},{64,96},{96,128},{128,160},{160,192},{192,224},{1,3... | collective-permute-start | bytes 61448 | tf_op jit(solution)/shard_map/ppermute | solution.py:479
  60.0 32.5 %collective-permute-start.1 = (bf16[40,256]{1,0:T(8,128)(2,1)S(1)}, bf16[40,256]{1,0:T(8,128)(2,1)S(1)}, u32[]{:S(2)}, u32[]{:S(2)}) collective-permute-start(bf16[40,256]{1,0:T(8,128)(2,1)S(1)} %get-tuple-element.19), channel_id=1, source_target_pairs={{0,64},{32,96},{64,128},{96,160},{128,192},{160,224},{1,65},{33,97... | collective-permute-start | bytes 61448 | tf_op jit(solution)/shard_map/ppermute | solution.py:479
  65.3 28.4 %collective-permute-start.2 = (bf16[40,256]{1,0:T(8,128)(2,1)S(1)}, bf16[40,256]{1,0:T(8,128)(2,1)S(1)}, u32[]{:S(2)}, u32[]{:S(2)}) collective-permute-start(bf16[40,256]{1,0:T(8,128)(2,1)S(1)} %get-tuple-element.19), channel_id=1, source_target_pairs={{0,96},{32,128},{64,160},{96,192},{128,224},{1,97},{33,129},{65,16... | collective-permute-start | bytes 61448 | tf_op jit(solution)/shard_map/ppermute | solution.py:479
  67.9 25.9 %collective-permute-start.3 = (bf16[40,256]{1,0:T(8,128)(2,1)S(1)}, bf16[40,256]{1,0:T(8,128)(2,1)S(1)}, u32[]{:S(2)}, u32[]{:S(2)}) collective-permute-start(bf16[40,256]{1,0:T(8,128)(2,1)S(1)} %get-tuple-element.19), channel_id=1, source_target_pairs={{0,128},{32,160},{64,192},{96,224},{1,129},{33,161},{65,193},{97,2... | collective-permute-start | bytes 61448 | tf_op jit(solution)/shard_map/ppermute | solution.py:479
  70.3 23.4 %collective-permute-start.4 = (bf16[40,256]{1,0:T(8,128)(2,1)S(1)}, bf16[40,256]{1,0:T(8,128)(2,1)S(1)}, u32[]{:S(2)}, u32[]{:S(2)}) collective-permute-start(bf16[40,256]{1,0:T(8,128)(2,1)S(1)} %get-tuple-element.19), channel_id=1, source_target_pairs={{0,160},{32,192},{64,224},{1,161},{33,193},{65,225},{2,162},{34,19... | collective-permute-start | bytes 61448 | tf_op jit(solution)/shard_map/ppermute | solution.py:479
  84.2 9.7 %collective-permute-start.5 = (bf16[40,256]{1,0:T(8,128)(2,1)S(1)}, bf16[40,256]{1,0:T(8,128)(2,1)S(1)}, u32[]{:S(2)}, u32[]{:S(2)}) collective-permute-start(bf16[40,256]{1,0:T(8,128)(2,1)S(1)} %get-tuple-element.19), channel_id=1, source_target_pairs={{0,192},{32,224},{1,193},{33,225},{2,194},{34,226},{3,195},{35,227... | collective-permute-start | bytes 61448 | tf_op jit(solution)/shard_map/ppermute | solution.py:479
  92.4 2.8 %collective-permute-start.6 = (bf16[40,256]{1,0:T(8,128)(2,1)S(1)}, bf16[40,256]{1,0:T(8,128)(2,1)S(1)}, u32[]{:S(2)}, u32[]{:S(2)}) collective-permute-start(bf16[40,256]{1,0:T(8,128)(2,1)S(1)} %get-tuple-element.19), channel_id=1, source_target_pairs={{0,224},{1,225},{2,226},{3,227},{4,228},{5,229},{6,230},{7,231},{8... | collective-permute-start | bytes 61448 | tf_op jit(solution)/shard_map/ppermute | solution.py:479
  104.5 25.8 %copy-start.1 = (bf16[512,256]{1,0:T(8,128)(2,1)S(1)}, bf16[512,256]{1,0:T(8,128)(2,1)}, u32[]{:S(2)}) copy-start(bf16[512,256]{1,0:T(8,128)(2,1)} %query.1) | copy-start | bytes 786436
  104.5 25.7 %copy-start.14 = (f32[256]{0:T(256)S(1)}, f32[256]{0:T(256)}, u32[]{:S(2)}) copy-start(f32[256]{0:T(256)} %param.23) | copy-start | bytes 3076
  104.5 82.2 %all-to-all-start.1 = ((bf16[64,8,3072]{2,1,0:T(8,128)(2,1)}), bf16[64,8,3072]{2,1,0:T(8,128)(2,1)S(1)}, u32[]{:S(2)}, u32[]{:S(2)}) async-start(bf16[64,8,3072]{2,1,0:T(8,128)(2,1)} %bitcast.27), calls=%async_computation.1 | async-start | bytes 6291456 | tf_op jit(solution)/shard_map/all_to_all | solution.py:391
  133.1 9.7 %copy-start.8 = (f32[2048]{0:T(1024)S(1)}, f32[2048]{0:T(1024)}, u32[]{:S(2)}) copy-start(f32[2048]{0:T(1024)} %param.25) | copy-start | bytes 24580
  134.9 5.0 %collective-permute-start.7 = (bf16[128,256]{1,0:T(8,128)(2,1)S(1)}, bf16[128,256]{1,0:T(8,128)(2,1)S(1)}, u32[]{:S(2)}, u32[]{:S(2)}) collective-permute-start(bf16[128,256]{1,0:T(8,128)(2,1)S(1)} %get-tuple-element.28), channel_id=1, source_target_pairs={{0,1},{1,2},{2,3},{3,0},{4,5},{5,6},{6,7},{7,4},{8,9},{9,10},{10,1... | collective-permute-start | bytes 196616 | tf_op jit(solution)/shard_map/ppermute | solution.py:537
  136.5 6.3 %collective-permute-start.8 = (bf16[128,256]{1,0:T(8,128)(2,1)S(1)}, bf16[128,256]{1,0:T(8,128)(2,1)S(1)}, u32[]{:S(2)}, u32[]{:S(2)}) collective-permute-start(bf16[128,256]{1,0:T(8,128)(2,1)S(1)} %get-tuple-element.27), channel_id=1, source_target_pairs={{0,2},{1,3},{2,0},{3,1},{4,6},{5,7},{6,4},{7,5},{8,10},{9,11},{10,... | collective-permute-start | bytes 196616 | tf_op jit(solution)/shard_map/ppermute | solution.py:537
  137.5 5.3 %collective-permute-start.9 = (bf16[128,256]{1,0:T(8,128)(2,1)S(1)}, bf16[128,256]{1,0:T(8,128)(2,1)S(1)}, u32[]{:S(2)}, u32[]{:S(2)}) collective-permute-start(bf16[128,256]{1,0:T(8,128)(2,1)S(1)} %get-tuple-element.26), channel_id=1, source_target_pairs={{0,3},{1,0},{2,1},{3,2},{4,7},{5,4},{6,5},{7,6},{8,11},{9,8},{10,9... | collective-permute-start | bytes 196616 | tf_op jit(solution)/shard_map/ppermute | solution.py:537
  142.8 43.9 %copy-start.12 = (s32[192,2]{0,1:T(2,128)S(1)}, s32[192,2]{0,1:T(2,128)}, u32[]{:S(2)}) copy-start(s32[192,2]{0,1:T(2,128)} %param.28) | copy-start | bytes 4612
  142.8 43.9 %copy-start.13 = (f32[192,2]{0,1:T(2,128)S(1)}, f32[192,2]{0,1:T(2,128)}, u32[]{:S(2)}) copy-start(f32[192,2]{0,1:T(2,128)} %param.30) | copy-start | bytes 4612
  142.8 43.9 %copy-start.15 = (f32[192]{0:T(256)S(1)}, f32[192]{0:T(256)}, u32[]{:S(2)}) copy-start(f32[192]{0:T(256)} %param.29) | copy-start | bytes 2308
  142.9 43.9 %copy-start.16 = (f32[64,192]{1,0:T(8,128)S(1)}, f32[64,192]{1,0:T(8,128)}, u32[]{:S(2)}) copy-start(f32[64,192]{1,0:T(8,128)} %get-tuple-element.24.ranks) | copy-start | bytes 147460
  (5 other events, 13.2 us)

commit v4 on v3

--- a/solution.py
+++ b/solution.py
@@ -60,7 +60,9 @@
     return jax.ShapeDtypeStruct(shape, dtype)
 
 
-def build_body(ids_far, rows_far, gain_far, out, ranks, ids, rows, gain, made, sems, out_sems):
+def build_body(
+    ids_far, rows_far, gain_far, out, ranks, ids, rows, gain, places, made, sems, out_sems
+):
     tokens, d = rows.shape
     half = d // 2
     experts = ranks.shape[0]
@@ -77,50 +79,56 @@
     count = mm(chosen.astype(f32).astype(bf16), ahead)
     rank = jnp.where(chosen, count, -1.0)
     ranks[...] = rank
+    _, slots, part = made.shape
+    row = iota((experts, 8, tokens), 1)
+    held = rank[:, None, :]
+
+    def placing(hit):
+        return hit.astype(f32).reshape(slots, tokens).astype(bf16)
+
+    late = held == ((row & 3) + 8).astype(f32)
+    places[0] = placing(held == row.astype(f32))
+    places[1] = placing(late & (row < 4))
+    places[2] = placing(late & (row >= 4))
     loads[1].wait()
     x = rows[...].astype(f32)
     mean = jnp.mean(x * x, axis=-1, keepdims=True)
     loads[2].wait()
     xn = (x * lax.rsqrt(mean + norm_eps) * gain[...]).astype(bf16)
-    steps, block, _ = made.shape
-    part = block // 8
-    row = iota((part, 8, tokens), 1)
-    slot = row.astype(f32)
-    late_slot = ((row & 3) + 8).astype(f32)
-
-    def placing(hit):
-        return hit.astype(f32).reshape(block, tokens).astype(bf16)
-
-    def store(step):
-        return pltpu.make_async_copy(
-            made.at[step], out.at[pl.ds(step * block, block), :], out_sems.at[step]
+    stores = []
+
+    def send(step, values):
+        made[step] = values.astype(bf16)
+        stores.append(
+            pltpu.make_async_copy(
+                made.at[step], out.at[:, pl.ds(step * part, part)], out_sems.at[step]
+            )
         )
-
-    for step in range(steps):
-        held = rank[step * part : (step + 1) * part, None, :]
-        made[step, :, :d] = mm(placing(held == slot), xn).astype(bf16)
-        late = held == late_slot
-        first, last = placing(late & (row < 4)), placing(late & (row >= 4))
-        made[step, :, d:] = (mm(first, xn[:, :half]) + mm(last, xn[:, half:])).astype(bf16)
-        store(step).start()
-    for step in range(steps):
-        store(step).wait()
+        stores[-1].start()
+
+    early = d // part
+    for step in range(early):
+        send(step, mm(places[0], xn[:, step * part : (step + 1) * part]))
+    for step in range(half // part):
+        left = xn[:, step * part : (step + 1) * part]
+        right = xn[:, half + step * part : half + (step + 1) * part]
+        send(early + step, mm(places[1], left) + mm(places[2], right))
+    for store in stores:
+        store.wait()
 
 
 def silu_mul(gate, upper):
     return (gate / (1.0 + jnp.exp(-gate)) * upper).astype(bf16)
 
 
-def ffn_body(x_far, wg_far, wu_far, wd_far, out, x, wg, wu, wd, made, in_sems, sems):
+def ffn_body(x_far, wg, wu_far, wd_far, out, x, wu, wd, made, in_sems, sems):
     d, _ = wg.shape
     half = d // 2
     slots = x.shape[0]
     pieces = (
         (x_far.at[:, pl.ds(d, half)], x.at[:, pl.ds(d, half)]),
-        (wg_far.at[pl.ds(0, half), :], wg.at[pl.ds(0, half), :]),
-        (wg_far.at[pl.ds(half, half), :], wg.at[pl.ds(half, half), :]),
+        (x_far.at[:, pl.ds(0, d)], x.at[:, pl.ds(0, d)]),
         (wu_far, wu),
-        (x_far.at[:, pl.ds(0, d)], x.at[:, pl.ds(0, d)]),
         (wd_far, wd),
     )
     loads = [
@@ -142,16 +150,14 @@
     top, bottom = crossed(x4[:, 0], x4[:, 1])
     top = top.reshape(pairs * 8, half).astype(bf16)
     bottom = bottom.reshape(pairs * 8, half).astype(bf16)
+    gate4 = mm(top, wg[:half, :]) + mm(bottom, wg[half:, :])
     loads[1].wait()
-    gate4 = mm(top, wg[:half, :])
+    x8 = x[:, :d]
+    gate8 = mm(x8, wg[...])
     loads[2].wait()
-    gate4 += mm(bottom, wg[half:, :])
+    hidden4 = silu_mul(gate4, mm(top, wu[:half, :]) + mm(bottom, wu[half:, :]))
+    hidden8 = silu_mul(gate8, mm(x8, wu[...]))
     loads[3].wait()
-    hidden4 = silu_mul(gate4, mm(top, wu[:half, :]) + mm(bottom, wu[half:, :]))
-    loads[4].wait()
-    x8 = x[:, :d]
-    hidden8 = silu_mul(mm(x8, wg[...]), mm(x8, wu[...]))
-    loads[5].wait()
     part = made.shape[2]
     stores = []
 
@@ -442,9 +448,10 @@
             pltpu.VMEM((2, tokens), i32),
             pltpu.VMEM((tokens, d), bf16),
             pltpu.VMEM((1, d), f32),
-            pltpu.VMEM((4, slots // 4, d + d // 2), bf16),
+            pltpu.VMEM((3, slots, tokens), bf16),
+            pltpu.VMEM((6, slots, d // 4), bf16),
             pltpu.SemaphoreType.DMA((3,)),
-            pltpu.SemaphoreType.DMA((4,)),
+            pltpu.SemaphoreType.DMA((6,)),
         ),
         vmem=60,
     )
@@ -495,18 +502,17 @@
         w_up[0],
         w_down[0],
         cost=12 * slots * d * hidden,
-        specs=[far_away] * 4,
+        specs=[far_away, vm, far_away, far_away],
         out_specs=far_away,
         scratch=(
             pltpu.VMEM((slots, d + d // 2), bf16),
             pltpu.VMEM((d, hidden), bf16),
-            pltpu.VMEM((d, hidden), bf16),
             pltpu.VMEM((hidden, d), bf16),
             pltpu.VMEM((6, slots, d // 4), bf16),
-            pltpu.SemaphoreType.DMA((6,)),
+            pltpu.SemaphoreType.DMA((4,)),
             pltpu.SemaphoreType.DMA((6,)),
         ),
-        vmem=60,
+        vmem=50,
     )
     back = exchanged(answers.reshape(devices, 8, d + d // 2), EP)
     state = lax.all_gather(send, ("ep_1", "ep_2"), tiled=True)

time: 189 us -> 189 us (level)
  no operation moved by 1% of the time
where the time goes in v4:
time: 189 us; the launch traced here: 188 us
  waiting for transfers between devices  58.6 us (31%)
  starting transfers between devices  53.9 us (29%)
  blocking collectives  49.9 us (26%)
  Pallas kernels  21 us (11%)
  local copies, waits for them, and re-layouts  3.66 us (2%)
    all_to_all x2, waiting for transfers between devices, exchanged(): return lax.all_to_all(array, axes, split_axis=0, concat_axis=0, tiled=True)  41.6 us
    ppermute x7, starting transfers between devices, shards(): lax.ppermute(send, 'ep_0', [(i, i + step) for i in range(line - step)])  28.3 us
    pallas_call x8, Pallas kernels, call(): pl.pallas_call(body, out_shape=out_shape, scratch_shapes=list(scratch), c...  21 us
    all_to_all x2, starting transfers between devices, exchanged(): return lax.all_to_all(array, axes, split_axis=0, concat_axis=0, tiled=True)  20.6 us
    all_gather x1, blocking collectives, shards(): states = lax.all_gather(send, ('ep_1', 'ep_2'))  18.5 us
    all_gather x1, blocking collectives, shards(): state = lax.all_gather(send, ('ep_1', 'ep_2'), tiled=True)  17.4 us
    all_gather x1, blocking collectives, shards(): more = lax.all_gather(after(rest, states), ('ep_1', 'ep_2'))  14 us
    ppermute x7, waiting for transfers between devices, shards(): lax.ppermute(send, 'ep_0', [(i, i + step) for i in range(line - step)])  14 us
  transfers between devices with their start and end apart: 12, of which 5 were waited for; matrix products, arithmetic and copies ran while one was open for 0% of the time, Pallas kernels for 4%

profile of v4, /device:TPU:8, one launch (start us, length us, event | category | flops | bytes accessed | tf_op | source)
XLA Modules:
  0.0 188.1 jit_solution(2759170539802316695)
XLA Ops:
  0.6 4.2 %shard_map.176 = (bf16[512,3072]{1,0:T(8,128)(2,1)}, f32[64,192]{1,0:T(8,128)}) custom-call(s32[2,192]{1,0:T(2,128)} %bitcast.23, bf16[192,2048]{1,0:T(8,128)(2,1)} %rows_far.1, f32[1,2048]{1,0:T(1,128)} %bitcast.32), custom_call_target="tpu_custom_call" | custom-call | flops 805306368 | bytes 1610612 | tf_op jit(solution)/shard_map/pallas_call | solution.py:49
  4.9 12.3 %all-to-all-start = ((bf16[64,8,3072]{2,1,0:T(8,128)(2,1)}), bf16[64,8,3072]{2,1,0:T(8,128)(2,1)}, u32[]{:S(2)}, u32[]{:S(2)}) async-start(bf16[64,8,3072]{2,1,0:T(8,128)(2,1)} %bitcast.29), calls=%async_computation | async-start | bytes 6291456 | tf_op jit(solution)/shard_map/all_to_all | solution.py:397
  18.0 18.5 %all-gather = bf16[1088,256]{1,0:T(8,128)(2,1)S(1)} all-gather(bf16[136,256]{1,0:T(8,128)(2,1)S(1)} %get-tuple-element.16), channel_id=2, replica_groups=mesh['ep_0'=8,'ep_1'=4,'ep_2'=2,'tp'=4] {'ep_1','ep_2'}, dimensions={0}, use_global_device_ids=true | all-gather | bytes 626688 | tf_op jit(solution)/shard_map/all_gather | solution.py:469
  36.5 14.0 %all-gather.1 = bf16[1024,256]{1,0:T(8,128)(2,1)S(1)} all-gather(bf16[128,256]{1,0:T(8,128)(2,1)S(1)} %get-tuple-element.18), channel_id=3, replica_groups=mesh['ep_0'=8,'ep_1'=4,'ep_2'=2,'tp'=4] {'ep_1','ep_2'}, dimensions={0}, use_global_device_ids=true | all-gather | bytes 589824 | tf_op jit(solution)/shard_map/all_gather | solution.py:470
  50.5 1.5 shard_map.178
  52.8 7.0 %collective-permute-start = (bf16[40,256]{1,0:T(8,128)(2,1)S(1)}, bf16[40,256]{1,0:T(8,128)(2,1)S(1)}, u32[]{:S(2)}, u32[]{:S(2)}) collective-permute-start(bf16[40,256]{1,0:T(8,128)(2,1)S(1)} %get-tuple-element.19), channel_id=1, source_target_pairs={{0,32},{32,64},{64,96},{96,128},{128,160},{160,192},{192,224},{1,3... | collective-permute-start | bytes 61448 | tf_op jit(solution)/shard_map/ppermute | solution.py:486
  59.8 5.4 %collective-permute-start.1 = (bf16[40,256]{1,0:T(8,128)(2,1)S(1)}, bf16[40,256]{1,0:T(8,128)(2,1)S(1)}, u32[]{:S(2)}, u32[]{:S(2)}) collective-permute-start(bf16[40,256]{1,0:T(8,128)(2,1)S(1)} %get-tuple-element.19), channel_id=1, source_target_pairs={{0,64},{32,96},{64,128},{96,160},{128,192},{160,224},{1,65},{33,97... | collective-permute-start | bytes 61448 | tf_op jit(solution)/shard_map/ppermute | solution.py:486
  65.2 2.5 %collective-permute-start.2 = (bf16[40,256]{1,0:T(8,128)(2,1)S(1)}, bf16[40,256]{1,0:T(8,128)(2,1)S(1)}, u32[]{:S(2)}, u32[]{:S(2)}) collective-permute-start(bf16[40,256]{1,0:T(8,128)(2,1)S(1)} %get-tuple-element.19), channel_id=1, source_target_pairs={{0,96},{32,128},{64,160},{96,192},{128,224},{1,97},{33,129},{65,16... | collective-permute-start | bytes 61448 | tf_op jit(solution)/shard_map/ppermute | solution.py:486
  67.8 2.5 %collective-permute-start.3 = (bf16[40,256]{1,0:T(8,128)(2,1)S(1)}, bf16[40,256]{1,0:T(8,128)(2,1)S(1)}, u32[]{:S(2)}, u32[]{:S(2)}) collective-permute-start(bf16[40,256]{1,0:T(8,128)(2,1)S(1)} %get-tuple-element.19), channel_id=1, source_target_pairs={{0,128},{32,160},{64,192},{96,224},{1,129},{33,161},{65,193},{97,2... | collective-permute-start | bytes 61448 | tf_op jit(solution)/shard_map/ppermute | solution.py:486
  70.3 1.3 collective-permute-start.4
  71.6 12.6 %collective-permute-done.refs_0_ = bf16[40,256]{1,0:T(8,128)(2,1)S(1)} collective-permute-done((bf16[40,256]{1,0:T(8,128)(2,1)S(1)}, bf16[40,256]{1,0:T(8,128)(2,1)S(1)}, u32[]{:S(2)}, u32[]{:S(2)}) %collective-permute-start) | collective-permute-done | bytes 20512 | tf_op jit(solution)/shard_map/ppermute | solution.py:486
  84.1 8.2 %collective-permute-start.5 = (bf16[40,256]{1,0:T(8,128)(2,1)S(1)}, bf16[40,256]{1,0:T(8,128)(2,1)S(1)}, u32[]{:S(2)}, u32[]{:S(2)}) collective-permute-start(bf16[40,256]{1,0:T(8,128)(2,1)S(1)} %get-tuple-element.19), channel_id=1, source_target_pairs={{0,192},{32,224},{1,193},{33,225},{2,194},{34,226},{3,195},{35,227... | collective-permute-start | bytes 61448 | tf_op jit(solution)/shard_map/ppermute | solution.py:486
  92.4 1.3 collective-permute-start.6
  93.8 1.3 collective-permute-done.6.refs_6_
  96.0 7.8 %shard_map.182 = bf16[512,3072]{1,0:T(8,128)(2,1)} custom-call(bf16[512,3072]{1,0:T(8,128)(2,1)} %bitcast.12.x_far, bf16[2048,512]{1,0:T(8,128)(2,1)S(1)} %bitcast.21, bf16[2048,512]{1,0:T(8,128)(2,1)} %bitcast.30, bf16[512,2048]{1,0:T(8,128)(2,1)} %bitcast.31), custom_call_target="tpu_custom_call" | custom-call | flops 6442450944 | bytes 12884901 | tf_op jit(solution)/shard_map/pallas_call | solution.py:49
  103.9 8.3 %all-to-all-start.1 = ((bf16[64,8,3072]{2,1,0:T(8,128)(2,1)}), bf16[64,8,3072]{2,1,0:T(8,128)(2,1)S(1)}, u32[]{:S(2)}, u32[]{:S(2)}) async-start(bf16[64,8,3072]{2,1,0:T(8,128)(2,1)} %bitcast.28), calls=%async_computation.1 | async-start | bytes 6291456 | tf_op jit(solution)/shard_map/all_to_all | solution.py:397
  112.2 17.4 %all_gather.19.state = bf16[256,256]{1,0:T(8,128)(2,1)S(1)} all-gather(bf16[32,256]{1,0:T(8,128)(2,1)S(1)} %get-tuple-element.20), channel_id=1, replica_groups=mesh['ep_0'=8,'ep_1'=4,'ep_2'=2,'tp'=4] {'ep_1','ep_2'}, dimensions={0}, use_global_device_ids=true | all-gather | bytes 147456 | tf_op jit(solution)/shard_map/all_gather | solution.py:518
  132.5 1.7 shard_map.180
  134.2 1.7 collective-permute-start.7
  136.8 2.4 %collective-permute-start.9 = (bf16[128,256]{1,0:T(8,128)(2,1)S(1)}, bf16[128,256]{1,0:T(8,128)(2,1)S(1)}, u32[]{:S(2)}, u32[]{:S(2)}) collective-permute-start(bf16[128,256]{1,0:T(8,128)(2,1)S(1)} %get-tuple-element.26), channel_id=1, source_target_pairs={{0,3},{1,0},{2,1},{3,2},{4,7},{5,4},{6,5},{7,6},{8,11},{9,8},{10,9... | collective-permute-start | bytes 196616 | tf_op jit(solution)/shard_map/ppermute | solution.py:543
  139.2 2.9 %collective-permute-done.8.refs_2_ = bf16[128,256]{1,0:T(8,128)(2,1)S(1)} collective-permute-done((bf16[128,256]{1,0:T(8,128)(2,1)S(1)}, bf16[128,256]{1,0:T(8,128)(2,1)S(1)}, u32[]{:S(2)}, u32[]{:S(2)}) %collective-permute-start.8) | collective-permute-done | bytes 65568 | tf_op jit(solution)/shard_map/ppermute | solution.py:543
  142.2 2.2 %shard_map.181 = bf16[128,2048]{1,0:T(8,128)(2,1)} custom-call(s32[3]{0:T(128)S(1)} %pad_add_fusion.where, bf16[128,256]{1,0:T(8,128)(2,1)S(1)} %get-tuple-element.29.refs_0_, bf16[128,256]{1,0:T(8,128)(2,1)S(1)} %collective-permute-done.7.refs_1_, bf16[128,256]{1,0:T(8,128)(2,1)S(1)} %collective-permute-done.8.refs_2_, ...), custom_call_target="tpu_custom_call" | custom-call | flops 5368709120 | bytes 10737418 | tf_op jit(solution)/shard_map/pallas_call | solution.py:49
  144.4 41.6 %all-to-all-done.1 = bf16[64,8,3072]{2,1,0:T(8,128)(2,1)S(1)} async-done(((bf16[64,8,3072]{2,1,0:T(8,128)(2,1)}), bf16[64,8,3072]{2,1,0:T(8,128)(2,1)S(1)}, u32[]{:S(2)}, u32[]{:S(2)}) %all-to-all-start.1) | async-done | bytes 3145760 | tf_op jit(solution)/shard_map/all_to_all | solution.py:397
  186.0 2.0 %shard_map.183 = bf16[192,2048]{1,0:T(8,128)(2,1)} custom-call(s32[2,192]{1,0:T(2,128)S(1)} %bitcast.24, f32[1,192]{1,0:T(1,128)S(1)} %bitcast.27, f32[2,192]{1,0:T(2,128)S(1)} %bitcast.25, f32[64,192]{1,0:T(8,128)S(1)} %copy-done.17, bf16[512,3072]{1,0:T(8,128)(2,1)S(1)} %bitcast.18), custom_call_target="tpu_custom_call" | custom-call | flops 2415919104 | bytes 4831838 | tf_op jit(solution)/shard_map/pallas_call | solution.py:49
  (49 shorter events, 6.3 us)
Async XLA Ops:
  4.9 12.4 %copy-start.3 = (bf16[512,256]{1,0:T(8,128)(2,1)S(1)}, bf16[512,256]{1,0:T(8,128)(2,1)}, u32[]{:S(2)}) copy-start(bf16[512,256]{1,0:T(8,128)(2,1)} %keys.2) | copy-start | bytes 786436
  4.9 12.4 %copy-start.5 = (bf16[512,256]{1,0:T(8,128)(2,1)S(1)}, bf16[512,256]{1,0:T(8,128)(2,1)}, u32[]{:S(2)}) copy-start(bf16[512,256]{1,0:T(8,128)(2,1)} %values.3) | copy-start | bytes 786436
  4.9 12.4 %copy-start.10 = (f32[1,512]{1,0:T(1,128)S(1)}, f32[1,512]{1,0:T(1,128)}, u32[]{:S(2)}) copy-start(f32[1,512]{1,0:T(1,128)} %gates.3) | copy-start | bytes 6148
  4.9 12.4 %copy-start.11 = (f32[1,512]{1,0:T(1,128)S(1)}, f32[1,512]{1,0:T(1,128)}, u32[]{:S(2)}) copy-start(f32[1,512]{1,0:T(1,128)} %forget.3) | copy-start | bytes 6148
  4.9 12.4 %copy-start.12 = (f32[1,512]{1,0:T(1,128)S(1)}, f32[1,512]{1,0:T(1,128)}, u32[]{:S(2)}) copy-start(f32[1,512]{1,0:T(1,128)} %boosts.3) | copy-start | bytes 6148
  4.9 91.0 %all-to-all-start = ((bf16[64,8,3072]{2,1,0:T(8,128)(2,1)}), bf16[64,8,3072]{2,1,0:T(8,128)(2,1)}, u32[]{:S(2)}, u32[]{:S(2)}) async-start(bf16[64,8,3072]{2,1,0:T(8,128)(2,1)} %bitcast.29), calls=%async_computation | async-start | bytes 6291456 | tf_op jit(solution)/shard_map/all_to_all | solution.py:397
  17.2 78.7 %copy-start.1 = (bf16[1,2048,512]{2,1,0:T(8,128)(2,1)S(1)}, bf16[1,2048,512]{2,1,0:T(8,128)(2,1)}, u32[]{:S(2)}) copy-start(bf16[1,2048,512]{2,1,0:T(8,128)(2,1)} %param.31) | copy-start | bytes 6291460
  52.8 31.3 %collective-permute-start = (bf16[40,256]{1,0:T(8,128)(2,1)S(1)}, bf16[40,256]{1,0:T(8,128)(2,1)S(1)}, u32[]{:S(2)}, u32[]{:S(2)}) collective-permute-start(bf16[40,256]{1,0:T(8,128)(2,1)S(1)} %get-tuple-element.19), channel_id=1, source_target_pairs={{0,32},{32,64},{64,96},{96,128},{128,160},{160,192},{192,224},{1,3... | collective-permute-start | bytes 61448 | tf_op jit(solution)/shard_map/ppermute | solution.py:486
  59.8 32.5 %collective-permute-start.1 = (bf16[40,256]{1,0:T(8,128)(2,1)S(1)}, bf16[40,256]{1,0:T(8,128)(2,1)S(1)}, u32[]{:S(2)}, u32[]{:S(2)}) collective-permute-start(bf16[40,256]{1,0:T(8,128)(2,1)S(1)} %get-tuple-element.19), channel_id=1, source_target_pairs={{0,64},{32,96},{64,128},{96,160},{128,192},{160,224},{1,65},{33,97... | collective-permute-start | bytes 61448 | tf_op jit(solution)/shard_map/ppermute | solution.py:486
  65.2 28.4 %collective-permute-start.2 = (bf16[40,256]{1,0:T(8,128)(2,1)S(1)}, bf16[40,256]{1,0:T(8,128)(2,1)S(1)}, u32[]{:S(2)}, u32[]{:S(2)}) collective-permute-start(bf16[40,256]{1,0:T(8,128)(2,1)S(1)} %get-tuple-element.19), channel_id=1, source_target_pairs={{0,96},{32,128},{64,160},{96,192},{128,224},{1,97},{33,129},{65,16... | collective-permute-start | bytes 61448 | tf_op jit(solution)/shard_map/ppermute | solution.py:486
  67.8 25.9 %collective-permute-start.3 = (bf16[40,256]{1,0:T(8,128)(2,1)S(1)}, bf16[40,256]{1,0:T(8,128)(2,1)S(1)}, u32[]{:S(2)}, u32[]{:S(2)}) collective-permute-start(bf16[40,256]{1,0:T(8,128)(2,1)S(1)} %get-tuple-element.19), channel_id=1, source_target_pairs={{0,128},{32,160},{64,192},{96,224},{1,129},{33,161},{65,193},{97,2... | collective-permute-start | bytes 61448 | tf_op jit(solution)/shard_map/ppermute | solution.py:486
  70.3 23.4 %collective-permute-start.4 = (bf16[40,256]{1,0:T(8,128)(2,1)S(1)}, bf16[40,256]{1,0:T(8,128)(2,1)S(1)}, u32[]{:S(2)}, u32[]{:S(2)}) collective-permute-start(bf16[40,256]{1,0:T(8,128)(2,1)S(1)} %get-tuple-element.19), channel_id=1, source_target_pairs={{0,160},{32,192},{64,224},{1,161},{33,193},{65,225},{2,162},{34,19... | collective-permute-start | bytes 61448 | tf_op jit(solution)/shard_map/ppermute | solution.py:486
  84.1 9.7 %collective-permute-start.5 = (bf16[40,256]{1,0:T(8,128)(2,1)S(1)}, bf16[40,256]{1,0:T(8,128)(2,1)S(1)}, u32[]{:S(2)}, u32[]{:S(2)}) collective-permute-start(bf16[40,256]{1,0:T(8,128)(2,1)S(1)} %get-tuple-element.19), channel_id=1, source_target_pairs={{0,192},{32,224},{1,193},{33,225},{2,194},{34,226},{3,195},{35,227... | collective-permute-start | bytes 61448 | tf_op jit(solution)/shard_map/ppermute | solution.py:486
  92.4 2.8 %collective-permute-start.6 = (bf16[40,256]{1,0:T(8,128)(2,1)S(1)}, bf16[40,256]{1,0:T(8,128)(2,1)S(1)}, u32[]{:S(2)}, u32[]{:S(2)}) collective-permute-start(bf16[40,256]{1,0:T(8,128)(2,1)S(1)} %get-tuple-element.19), channel_id=1, source_target_pairs={{0,224},{1,225},{2,226},{3,227},{4,228},{5,229},{6,230},{7,231},{8... | collective-permute-start | bytes 61448 | tf_op jit(solution)/shard_map/ppermute | solution.py:486
  103.8 25.8 %copy-start.2 = (bf16[512,256]{1,0:T(8,128)(2,1)S(1)}, bf16[512,256]{1,0:T(8,128)(2,1)}, u32[]{:S(2)}) copy-start(bf16[512,256]{1,0:T(8,128)(2,1)} %query.1) | copy-start | bytes 786436
  103.8 25.7 %copy-start.15 = (f32[256]{0:T(256)S(1)}, f32[256]{0:T(256)}, u32[]{:S(2)}) copy-start(f32[256]{0:T(256)} %param.23) | copy-start | bytes 3076
  103.9 82.2 %all-to-all-start.1 = ((bf16[64,8,3072]{2,1,0:T(8,128)(2,1)}), bf16[64,8,3072]{2,1,0:T(8,128)(2,1)S(1)}, u32[]{:S(2)}, u32[]{:S(2)}) async-start(bf16[64,8,3072]{2,1,0:T(8,128)(2,1)} %bitcast.28), calls=%async_computation.1 | async-start | bytes 6291456 | tf_op jit(solution)/shard_map/all_to_all | solution.py:397
  134.2 5.0 %collective-permute-start.7 = (bf16[128,256]{1,0:T(8,128)(2,1)S(1)}, bf16[128,256]{1,0:T(8,128)(2,1)S(1)}, u32[]{:S(2)}, u32[]{:S(2)}) collective-permute-start(bf16[128,256]{1,0:T(8,128)(2,1)S(1)} %get-tuple-element.28), channel_id=1, source_target_pairs={{0,1},{1,2},{2,3},{3,0},{4,5},{5,6},{6,7},{7,4},{8,9},{9,10},{10,1... | collective-permute-start | bytes 196616 | tf_op jit(solution)/shard_map/ppermute | solution.py:543
  135.8 6.3 %collective-permute-start.8 = (bf16[128,256]{1,0:T(8,128)(2,1)S(1)}, bf16[128,256]{1,0:T(8,128)(2,1)S(1)}, u32[]{:S(2)}, u32[]{:S(2)}) collective-permute-start(bf16[128,256]{1,0:T(8,128)(2,1)S(1)} %get-tuple-element.27), channel_id=1, source_target_pairs={{0,2},{1,3},{2,0},{3,1},{4,6},{5,7},{6,4},{7,5},{8,10},{9,11},{10,... | collective-permute-start | bytes 196616 | tf_op jit(solution)/shard_map/ppermute | solution.py:543
  136.8 5.3 %collective-permute-start.9 = (bf16[128,256]{1,0:T(8,128)(2,1)S(1)}, bf16[128,256]{1,0:T(8,128)(2,1)S(1)}, u32[]{:S(2)}, u32[]{:S(2)}) collective-permute-start(bf16[128,256]{1,0:T(8,128)(2,1)S(1)} %get-tuple-element.26), channel_id=1, source_target_pairs={{0,3},{1,0},{2,1},{3,2},{4,7},{5,4},{6,5},{7,6},{8,11},{9,8},{10,9... | collective-permute-start | bytes 196616 | tf_op jit(solution)/shard_map/ppermute | solution.py:543
  142.1 43.9 %copy-start.13 = (s32[192,2]{0,1:T(2,128)S(1)}, s32[192,2]{0,1:T(2,128)}, u32[]{:S(2)}) copy-start(s32[192,2]{0,1:T(2,128)} %param.28) | copy-start | bytes 4612
  142.1 43.9 %copy-start.14 = (f32[192,2]{0,1:T(2,128)S(1)}, f32[192,2]{0,1:T(2,128)}, u32[]{:S(2)}) copy-start(f32[192,2]{0,1:T(2,128)} %param.30) | copy-start | bytes 4612
  142.2 43.9 %copy-start.16 = (f32[192]{0:T(256)S(1)}, f32[192]{0:T(256)}, u32[]{:S(2)}) copy-start(f32[192]{0:T(256)} %param.29) | copy-start | bytes 2308
  142.2 43.9 %copy-start.17 = (f32[64,192]{1,0:T(8,128)S(1)}, f32[64,192]{1,0:T(8,128)}, u32[]{:S(2)}) copy-start(f32[64,192]{1,0:T(8,128)} %get-tuple-element.24.ranks) | copy-start | bytes 147460
  (6 other events, 22.9 us)

commit v5 on v4

--- a/solution.py
+++ b/solution.py
@@ -468,7 +468,7 @@
     )
     states = lax.all_gather(send, ("ep_1", "ep_2"))
     more = lax.all_gather(after(rest, states), ("ep_1", "ep_2"))
-    send, own, near = call(
+    plane_send, own, near = call(
         plane_body,
         (
             struct((width // plane + 8, width), bf16),
@@ -483,7 +483,7 @@
         specs=[sm, vm, vm],
     )
     states = [
-        lax.ppermute(send, "ep_0", [(i, i + step) for i in range(line - step)])
+        lax.ppermute(plane_send, "ep_0", [(i, i + step) for i in range(line - step)])
         for step in range(1, line)
     ]
     send, far = call(
@@ -497,7 +497,7 @@
     answers = call(
         ffn_body,
         struct((slots, d + d // 2), bf16),
-        after(got, send).reshape(slots, d + d // 2),
+        after(got, plane_send).reshape(slots, d + d // 2),
         w_gate[0],
         w_up[0],
         w_down[0],

time: 189 us -> 217 us (1.15); the launches traced: 188 us -> 213 us
  waiting for transfers between devices: 58.6 us -> 95.2 us
  starting transfers between devices: 53.9 us -> 42.7 us
  blocking collectives: 49.9 us -> 45.7 us
  local copies, waits for them, and re-layouts: 3.66 us -> 7.07 us
    ppermute x7, waiting for transfers between devices: 14 us -> 54.6 us  [shards(): lax.ppermute(plane_send, 'ep_0', [(i, i + step) for i in range(line - ste...]
    ppermute x7, starting transfers between devices: 28.3 us -> 20 us  [shards(): lax.ppermute(plane_send, 'ep_0', [(i, i + step) for i in range(line - ste...]
    all_gather x1, blocking collectives: 17.4 us -> 13.2 us  [shards(): state = lax.all_gather(send, ('ep_1', 'ep_2'), tiled=True)]
    all_to_all x2, waiting for transfers between devices: 41.6 us -> 38 us  [exchanged(): return lax.all_to_all(array, axes, split_axis=0, concat_axis=0, tiled=True)]
    unnamed x36 -> x46, local copies, waits for them, and re-layouts: 3.63 us -> 7.04 us
    all_to_all x2, starting transfers between devices: 20.6 us -> 17.7 us  [exchanged(): return lax.all_to_all(array, axes, split_axis=0, concat_axis=0, tiled=True)]
  transfers between devices with their start and end apart: 12 -> 12, of which waited for: 5 -> 5; matrix products, arithmetic and copies ran while one was open for 0% -> 0% of each run, Pallas kernels for 4% -> 3%
where the time goes in v5:
time: 217 us; the launch traced here: 213 us
  waiting for transfers between devices  95.2 us (44%)
  blocking collectives  45.7 us (21%)
  starting transfers between devices  42.7 us (20%)
  Pallas kernels  21.4 us (10%)
  local copies, waits for them, and re-layouts  7.07 us (3%)
    ppermute x7, waiting for transfers between devices, shards(): lax.ppermute(plane_send, 'ep_0', [(i, i + step) for i in range(line - ste...  54.6 us
    all_to_all x2, waiting for transfers between devices, exchanged(): return lax.all_to_all(array, axes, split_axis=0, concat_axis=0, tiled=True)  38 us
    pallas_call x8, Pallas kernels, call(): pl.pallas_call(body, out_shape=out_shape, scratch_shapes=list(scratch), c...  21.4 us
    ppermute x7, starting transfers between devices, shards(): lax.ppermute(plane_send, 'ep_0', [(i, i + step) for i in range(line - ste...  20 us
    all_gather x1, blocking collectives, shards(): states = lax.all_gather(send, ('ep_1', 'ep_2'))  18.5 us
    all_to_all x2, starting transfers between devices, exchanged(): return lax.all_to_all(array, axes, split_axis=0, concat_axis=0, tiled=True)  17.7 us
    all_gather x1, blocking collectives, shards(): more = lax.all_gather(after(rest, states), ('ep_1', 'ep_2'))  14 us
    all_gather x1, blocking collectives, shards(): state = lax.all_gather(send, ('ep_1', 'ep_2'), tiled=True)  13.2 us
  transfers between devices with their start and end apart: 12, of which 5 were waited for; matrix products, arithmetic and copies ran while one was open for 0% of the time, Pallas kernels for 3%

profile of v5, /device:TPU:8, one launch (start us, length us, event | category | flops | bytes accessed | tf_op | source)
XLA Modules:
  0.0 213.1 jit_solution(16760036611509092027)
XLA Ops:
  0.6 4.2 %shard_map.176 = (bf16[512,3072]{1,0:T(8,128)(2,1)}, f32[64,192]{1,0:T(8,128)}) custom-call(s32[2,192]{1,0:T(2,128)} %bitcast.23, bf16[192,2048]{1,0:T(8,128)(2,1)} %rows_far.1, f32[1,2048]{1,0:T(1,128)} %bitcast.32), custom_call_target="tpu_custom_call" | custom-call | flops 805306368 | bytes 1610612 | tf_op jit(solution)/shard_map/pallas_call | solution.py:49
  4.9 12.3 %all-to-all-start = ((bf16[64,8,3072]{2,1,0:T(8,128)(2,1)}), bf16[64,8,3072]{2,1,0:T(8,128)(2,1)}, u32[]{:S(2)}, u32[]{:S(2)}) async-start(bf16[64,8,3072]{2,1,0:T(8,128)(2,1)} %bitcast.29), calls=%async_computation | async-start | bytes 6291456 | tf_op jit(solution)/shard_map/all_to_all | solution.py:397
  18.0 18.5 %all-gather = bf16[1088,256]{1,0:T(8,128)(2,1)S(1)} all-gather(bf16[136,256]{1,0:T(8,128)(2,1)S(1)} %get-tuple-element.16), channel_id=2, replica_groups=mesh['ep_0'=8,'ep_1'=4,'ep_2'=2,'tp'=4] {'ep_1','ep_2'}, dimensions={0}, use_global_device_ids=true | all-gather | bytes 626688 | tf_op jit(solution)/shard_map/all_gather | solution.py:469
  36.5 14.0 %all-gather.1 = bf16[1024,256]{1,0:T(8,128)(2,1)S(1)} all-gather(bf16[128,256]{1,0:T(8,128)(2,1)S(1)} %get-tuple-element.18), channel_id=3, replica_groups=mesh['ep_0'=8,'ep_1'=4,'ep_2'=2,'tp'=4] {'ep_1','ep_2'}, dimensions={0}, use_global_device_ids=true | all-gather | bytes 589824 | tf_op jit(solution)/shard_map/all_gather | solution.py:470
  50.6 1.7 shard_map.178
  53.0 38.0 %all-to-all-done = bf16[64,8,3072]{2,1,0:T(8,128)(2,1)} async-done(((bf16[64,8,3072]{2,1,0:T(8,128)(2,1)}), bf16[64,8,3072]{2,1,0:T(8,128)(2,1)}, u32[]{:S(2)}, u32[]{:S(2)}) %all-to-all-start) | async-done | bytes 3145760 | tf_op jit(solution)/shard_map/all_to_all | solution.py:397
  91.0 7.9 %shard_map.182 = bf16[512,3072]{1,0:T(8,128)(2,1)} custom-call(bf16[512,3072]{1,0:T(8,128)(2,1)} %bitcast.12.x_far, bf16[2048,512]{1,0:T(8,128)(2,1)S(1)} %bitcast.21, bf16[2048,512]{1,0:T(8,128)(2,1)} %bitcast.30, bf16[512,2048]{1,0:T(8,128)(2,1)} %bitcast.31), custom_call_target="tpu_custom_call" | custom-call | flops 6442450944 | bytes 12884901 | tf_op jit(solution)/shard_map/pallas_call | solution.py:49
  99.0 5.4 %all-to-all-start.1 = ((bf16[64,8,3072]{2,1,0:T(8,128)(2,1)}), bf16[64,8,3072]{2,1,0:T(8,128)(2,1)S(1)}, u32[]{:S(2)}, u32[]{:S(2)}) async-start(bf16[64,8,3072]{2,1,0:T(8,128)(2,1)} %bitcast.28), calls=%async_computation.1 | async-start | bytes 6291456 | tf_op jit(solution)/shard_map/all_to_all | solution.py:397
  104.4 5.0 %collective-permute-start.6 = (bf16[40,256]{1,0:T(8,128)(2,1)}, bf16[40,256]{1,0:T(8,128)(2,1)S(1)}, u32[]{:S(2)}, u32[]{:S(2)}) collective-permute-start(bf16[40,256]{1,0:T(8,128)(2,1)} %get-tuple-element.19), channel_id=1, source_target_pairs={{0,224},{1,225},{2,226},{3,227},{4,228},{5,229},{6,230},{7,231},{8... | collective-permute-start | bytes 61448 | tf_op jit(solution)/shard_map/ppermute | solution.py:486
  109.4 1.5 collective-permute-start.5
  110.9 1.5 collective-permute-start.4
  112.4 1.5 collective-permute-start.3
  113.9 4.5 %collective-permute-start.2 = (bf16[40,256]{1,0:T(8,128)(2,1)}, bf16[40,256]{1,0:T(8,128)(2,1)S(1)}, u32[]{:S(2)}, u32[]{:S(2)}) collective-permute-start(bf16[40,256]{1,0:T(8,128)(2,1)} %get-tuple-element.19), channel_id=1, source_target_pairs={{0,96},{32,128},{64,160},{96,192},{128,224},{1,97},{33,129},{65,16... | collective-permute-start | bytes 61448 | tf_op jit(solution)/shard_map/ppermute | solution.py:486
  118.4 53.0 %collective-permute-done.6.refs_6_ = bf16[40,256]{1,0:T(8,128)(2,1)S(1)} collective-permute-done((bf16[40,256]{1,0:T(8,128)(2,1)}, bf16[40,256]{1,0:T(8,128)(2,1)S(1)}, u32[]{:S(2)}, u32[]{:S(2)}) %collective-permute-start.6) | collective-permute-done | bytes 20512 | tf_op jit(solution)/shard_map/ppermute | solution.py:486
  171.4 1.3 collective-permute-start.1
  172.7 4.7 %collective-permute-start = (bf16[40,256]{1,0:T(8,128)(2,1)}, bf16[40,256]{1,0:T(8,128)(2,1)S(1)}, u32[]{:S(2)}, u32[]{:S(2)}) collective-permute-start(bf16[40,256]{1,0:T(8,128)(2,1)} %get-tuple-element.19), channel_id=1, source_target_pairs={{0,32},{32,64},{64,96},{96,128},{128,160},{160,192},{192,224},{1,3... | collective-permute-start | bytes 61448 | tf_op jit(solution)/shard_map/ppermute | solution.py:486
  177.4 1.6 collective-permute-done.refs_0_
  179.9 13.2 %all_gather.19.state = bf16[256,256]{1,0:T(8,128)(2,1)S(1)} all-gather(bf16[32,256]{1,0:T(8,128)(2,1)S(1)} %get-tuple-element.20), channel_id=1, replica_groups=mesh['ep_0'=8,'ep_1'=4,'ep_2'=2,'tp'=4] {'ep_1','ep_2'}, dimensions={0}, use_global_device_ids=true | all-gather | bytes 147456 | tf_op jit(solution)/shard_map/all_gather | solution.py:518
  199.4 1.7 shard_map.180
  201.7 2.6 %collective-permute-start.8 = (bf16[128,256]{1,0:T(8,128)(2,1)S(1)}, bf16[128,256]{1,0:T(8,128)(2,1)S(1)}, u32[]{:S(2)}, u32[]{:S(2)}) collective-permute-start(bf16[128,256]{1,0:T(8,128)(2,1)S(1)} %get-tuple-element.27), channel_id=1, source_target_pairs={{0,2},{1,3},{2,0},{3,1},{4,6},{5,7},{6,4},{7,5},{8,10},{9,11},{10,... | collective-permute-start | bytes 196616 | tf_op jit(solution)/shard_map/ppermute | solution.py:543
  204.3 1.9 collective-permute-start.7
  206.2 1.8 collective-permute-done.8.refs_2_
  208.8 2.3 %shard_map.181 = bf16[128,2048]{1,0:T(8,128)(2,1)} custom-call(s32[3]{0:T(128)S(1)} %pad_add_fusion.where, bf16[128,256]{1,0:T(8,128)(2,1)S(1)} %get-tuple-element.29.refs_0_, bf16[128,256]{1,0:T(8,128)(2,1)S(1)} %collective-permute-done.7.refs_1_, bf16[128,256]{1,0:T(8,128)(2,1)S(1)} %collective-permute-done.8.refs_2_, ...), custom_call_target="tpu_custom_call" | custom-call | flops 5368709120 | bytes 10737418 | tf_op jit(solution)/shard_map/pallas_call | solution.py:49
  211.1 2.0 shard_map.183
  (59 shorter events, 9.9 us)
Async XLA Ops:
  4.9 12.4 %copy-start.3 = (bf16[512,256]{1,0:T(8,128)(2,1)S(1)}, bf16[512,256]{1,0:T(8,128)(2,1)}, u32[]{:S(2)}) copy-start(bf16[512,256]{1,0:T(8,128)(2,1)} %keys.2) | copy-start | bytes 786436
  4.9 12.4 %copy-start.5 = (bf16[512,256]{1,0:T(8,128)(2,1)S(1)}, bf16[512,256]{1,0:T(8,128)(2,1)}, u32[]{:S(2)}) copy-start(bf16[512,256]{1,0:T(8,128)(2,1)} %values.3) | copy-start | bytes 786436
  4.9 12.4 %copy-start.12 = (f32[1,512]{1,0:T(1,128)S(1)}, f32[1,512]{1,0:T(1,128)}, u32[]{:S(2)}) copy-start(f32[1,512]{1,0:T(1,128)} %gates.3) | copy-start | bytes 6148
  4.9 12.4 %copy-start.14 = (f32[1,512]{1,0:T(1,128)S(1)}, f32[1,512]{1,0:T(1,128)}, u32[]{:S(2)}) copy-start(f32[1,512]{1,0:T(1,128)} %forget.3) | copy-start | bytes 6148
  4.9 12.4 %copy-start.16 = (f32[1,512]{1,0:T(1,128)S(1)}, f32[1,512]{1,0:T(1,128)}, u32[]{:S(2)}) copy-start(f32[1,512]{1,0:T(1,128)} %boosts.3) | copy-start | bytes 6148
  4.9 86.1 %all-to-all-start = ((bf16[64,8,3072]{2,1,0:T(8,128)(2,1)}), bf16[64,8,3072]{2,1,0:T(8,128)(2,1)}, u32[]{:S(2)}, u32[]{:S(2)}) async-start(bf16[64,8,3072]{2,1,0:T(8,128)(2,1)} %bitcast.29), calls=%async_computation | async-start | bytes 6291456 | tf_op jit(solution)/shard_map/all_to_all | solution.py:397
  17.3 73.7 %copy-start.1 = (bf16[1,2048,512]{2,1,0:T(8,128)(2,1)S(1)}, bf16[1,2048,512]{2,1,0:T(8,128)(2,1)}, u32[]{:S(2)}) copy-start(bf16[1,2048,512]{2,1,0:T(8,128)(2,1)} %param.31) | copy-start | bytes 6291460
  53.0 46.0 %copy-start.10 = (f32[8,256]{1,0:T(8,128)}, f32[8,256]{1,0:T(8,128)S(1)}, u32[]{:S(2)}) copy-start(f32[8,256]{1,0:T(8,128)S(1)} %get-tuple-element.23.near) | copy-start | bytes 24580
  99.0 94.2 %copy-start.2 = (bf16[512,256]{1,0:T(8,128)(2,1)S(1)}, bf16[512,256]{1,0:T(8,128)(2,1)}, u32[]{:S(2)}) copy-start(bf16[512,256]{1,0:T(8,128)(2,1)} %query.1) | copy-start | bytes 786436
  99.0 112.1 %all-to-all-start.1 = ((bf16[64,8,3072]{2,1,0:T(8,128)(2,1)}), bf16[64,8,3072]{2,1,0:T(8,128)(2,1)S(1)}, u32[]{:S(2)}, u32[]{:S(2)}) async-start(bf16[64,8,3072]{2,1,0:T(8,128)(2,1)} %bitcast.28), calls=%async_computation.1 | async-start | bytes 6291456 | tf_op jit(solution)/shard_map/all_to_all | solution.py:397
  104.4 67.0 %collective-permute-start.6 = (bf16[40,256]{1,0:T(8,128)(2,1)}, bf16[40,256]{1,0:T(8,128)(2,1)S(1)}, u32[]{:S(2)}, u32[]{:S(2)}) collective-permute-start(bf16[40,256]{1,0:T(8,128)(2,1)} %get-tuple-element.19), channel_id=1, source_target_pairs={{0,224},{1,225},{2,226},{3,227},{4,228},{5,229},{6,230},{7,231},{8... | collective-permute-start | bytes 61448 | tf_op jit(solution)/shard_map/ppermute | solution.py:486
  109.4 63.3 %collective-permute-start.5 = (bf16[40,256]{1,0:T(8,128)(2,1)}, bf16[40,256]{1,0:T(8,128)(2,1)S(1)}, u32[]{:S(2)}, u32[]{:S(2)}) collective-permute-start(bf16[40,256]{1,0:T(8,128)(2,1)} %get-tuple-element.19), channel_id=1, source_target_pairs={{0,192},{32,224},{1,193},{33,225},{2,194},{34,226},{3,195},{35,227... | collective-permute-start | bytes 61448 | tf_op jit(solution)/shard_map/ppermute | solution.py:486
  110.9 66.5 %collective-permute-start.4 = (bf16[40,256]{1,0:T(8,128)(2,1)}, bf16[40,256]{1,0:T(8,128)(2,1)S(1)}, u32[]{:S(2)}, u32[]{:S(2)}) collective-permute-start(bf16[40,256]{1,0:T(8,128)(2,1)} %get-tuple-element.19), channel_id=1, source_target_pairs={{0,160},{32,192},{64,224},{1,161},{33,193},{65,225},{2,162},{34,19... | collective-permute-start | bytes 61448 | tf_op jit(solution)/shard_map/ppermute | solution.py:486
  112.4 65.0 %collective-permute-start.3 = (bf16[40,256]{1,0:T(8,128)(2,1)}, bf16[40,256]{1,0:T(8,128)(2,1)S(1)}, u32[]{:S(2)}, u32[]{:S(2)}) collective-permute-start(bf16[40,256]{1,0:T(8,128)(2,1)} %get-tuple-element.19), channel_id=1, source_target_pairs={{0,128},{32,160},{64,192},{96,224},{1,129},{33,161},{65,193},{97,2... | collective-permute-start | bytes 61448 | tf_op jit(solution)/shard_map/ppermute | solution.py:486
  113.9 63.5 %collective-permute-start.2 = (bf16[40,256]{1,0:T(8,128)(2,1)}, bf16[40,256]{1,0:T(8,128)(2,1)S(1)}, u32[]{:S(2)}, u32[]{:S(2)}) collective-permute-start(bf16[40,256]{1,0:T(8,128)(2,1)} %get-tuple-element.19), channel_id=1, source_target_pairs={{0,96},{32,128},{64,160},{96,192},{128,224},{1,97},{33,129},{65,16... | collective-permute-start | bytes 61448 | tf_op jit(solution)/shard_map/ppermute | solution.py:486
  171.4 6.1 %collective-permute-start.1 = (bf16[40,256]{1,0:T(8,128)(2,1)}, bf16[40,256]{1,0:T(8,128)(2,1)S(1)}, u32[]{:S(2)}, u32[]{:S(2)}) collective-permute-start(bf16[40,256]{1,0:T(8,128)(2,1)} %get-tuple-element.19), channel_id=1, source_target_pairs={{0,64},{32,96},{64,128},{96,160},{128,192},{160,224},{1,65},{33,97... | collective-permute-start | bytes 61448 | tf_op jit(solution)/shard_map/ppermute | solution.py:486
  172.7 6.4 %collective-permute-start = (bf16[40,256]{1,0:T(8,128)(2,1)}, bf16[40,256]{1,0:T(8,128)(2,1)S(1)}, u32[]{:S(2)}, u32[]{:S(2)}) collective-permute-start(bf16[40,256]{1,0:T(8,128)(2,1)} %get-tuple-element.19), channel_id=1, source_target_pairs={{0,32},{32,64},{64,96},{96,128},{128,160},{160,192},{192,224},{1,3... | collective-permute-start | bytes 61448 | tf_op jit(solution)/shard_map/ppermute | solution.py:486
  199.4 9.4 %copy-start = (bf16[1024,2048]{1,0:T(8,128)(2,1)S(1)}, bf16[1024,2048]{1,0:T(8,128)(2,1)}, u32[]{:S(2)}) copy-start(bf16[1024,2048]{1,0:T(8,128)(2,1)} %refs_4_.1) | copy-start | bytes 12582916
  199.4 9.4 %copy-start.9 = (f32[2048]{0:T(1024)S(1)}, f32[2048]{0:T(1024)}, u32[]{:S(2)}) copy-start(f32[2048]{0:T(1024)} %param.25) | copy-start | bytes 24580
  201.2 5.0 %collective-permute-start.9 = (bf16[128,256]{1,0:T(8,128)(2,1)S(1)}, bf16[128,256]{1,0:T(8,128)(2,1)S(1)}, u32[]{:S(2)}, u32[]{:S(2)}) collective-permute-start(bf16[128,256]{1,0:T(8,128)(2,1)S(1)} %get-tuple-element.26), channel_id=1, source_target_pairs={{0,3},{1,0},{2,1},{3,2},{4,7},{5,4},{6,5},{7,6},{8,11},{9,8},{10,9... | collective-permute-start | bytes 196616 | tf_op jit(solution)/shard_map/ppermute | solution.py:543
  201.7 6.3 %collective-permute-start.8 = (bf16[128,256]{1,0:T(8,128)(2,1)S(1)}, bf16[128,256]{1,0:T(8,128)(2,1)S(1)}, u32[]{:S(2)}, u32[]{:S(2)}) collective-permute-start(bf16[128,256]{1,0:T(8,128)(2,1)S(1)} %get-tuple-element.27), channel_id=1, source_target_pairs={{0,2},{1,3},{2,0},{3,1},{4,6},{5,7},{6,4},{7,5},{8,10},{9,11},{10,... | collective-permute-start | bytes 196616 | tf_op jit(solution)/shard_map/ppermute | solution.py:543
  204.3 4.5 %collective-permute-start.7 = (bf16[128,256]{1,0:T(8,128)(2,1)S(1)}, bf16[128,256]{1,0:T(8,128)(2,1)S(1)}, u32[]{:S(2)}, u32[]{:S(2)}) collective-permute-start(bf16[128,256]{1,0:T(8,128)(2,1)S(1)} %get-tuple-element.28), channel_id=1, source_target_pairs={{0,1},{1,2},{2,3},{3,0},{4,5},{5,6},{6,7},{7,4},{8,9},{9,10},{10,1... | collective-permute-start | bytes 196616 | tf_op jit(solution)/shard_map/ppermute | solution.py:543
  208.8 2.3 %copy-start.18 = (s32[192,2]{0,1:T(2,128)S(1)}, s32[192,2]{0,1:T(2,128)}, u32[]{:S(2)}) copy-start(s32[192,2]{0,1:T(2,128)} %param.28) | copy-start | bytes 4612
  208.8 2.3 %copy-start.19 = (f32[192,2]{0,1:T(2,128)S(1)}, f32[192,2]{0,1:T(2,128)}, u32[]{:S(2)}) copy-start(f32[192,2]{0,1:T(2,128)} %param.30) | copy-start | bytes 4612
  (11 other events, 11.6 us)

commit v6 on v5

--- a/solution.py
+++ b/solution.py
@@ -60,8 +60,34 @@
     return jax.ShapeDtypeStruct(shape, dtype)
 
 
+def crossed(left, right):
+    upper = (iota((1, 8, 1), 1) & 4) == 0
+    return (
+        jnp.where(upper, left, pltpu.roll(right, 4, 1)),
+        jnp.where(upper, pltpu.roll(left, 4, 1), right),
+    )
+
+
+def unpacked(left, right):
+    rows, part = left.shape
+    pair = crossed(left.reshape(rows // 8, 8, part), right.reshape(rows // 8, 8, part))
+    return jnp.stack(pair, axis=1).reshape(2 * rows, part)
+
+
 def build_body(
-    ids_far, rows_far, gain_far, out, ranks, ids, rows, gain, places, made, sems, out_sems
+    ids_far,
+    rows_far,
+    gain_far,
+    out,
+    ranks,
+    ids,
+    rows,
+    gain,
+    early_places,
+    late_places,
+    made,
+    sems,
+    out_sems,
 ):
     tokens, d = rows.shape
     half = d // 2
@@ -80,16 +106,15 @@
     rank = jnp.where(chosen, count, -1.0)
     ranks[...] = rank
     _, slots, part = made.shape
-    row = iota((experts, 8, tokens), 1)
     held = rank[:, None, :]
-
-    def placing(hit):
-        return hit.astype(f32).reshape(slots, tokens).astype(bf16)
-
-    late = held == ((row & 3) + 8).astype(f32)
-    places[0] = placing(held == row.astype(f32))
-    places[1] = placing(late & (row < 4))
-    places[2] = placing(late & (row >= 4))
+    row = iota((experts, 8, tokens), 1).astype(f32)
+    early_places[...] = (held == row).astype(f32).reshape(slots, tokens).astype(bf16)
+    pairs = experts // 2
+    held = held.reshape(pairs, 2, 1, tokens)
+    row = iota((pairs, 8, tokens), 1)
+    held = jnp.where(row < 4, held[:, 0], held[:, 1])
+    hit = held == ((row & 3) + 8).astype(f32)
+    late_places[...] = hit.astype(f32).reshape(slots // 2, tokens).astype(bf16)
     loads[1].wait()
     x = rows[...].astype(f32)
     mean = jnp.mean(x * x, axis=-1, keepdims=True)
@@ -107,12 +132,12 @@
         stores[-1].start()
 
     early = d // part
-    for step in range(early):
-        send(step, mm(places[0], xn[:, step * part : (step + 1) * part]))
     for step in range(half // part):
         left = xn[:, step * part : (step + 1) * part]
         right = xn[:, half + step * part : half + (step + 1) * part]
-        send(early + step, mm(places[1], left) + mm(places[2], right))
+        send(early + step, unpacked(mm(late_places[...], left), mm(late_places[...], right)))
+    for step in range(early):
+        send(step, mm(early_places[...], xn[:, step * part : (step + 1) * part]))
     for store in stores:
         store.wait()
 
@@ -126,8 +151,8 @@
     half = d // 2
     slots = x.shape[0]
     pieces = (
+        (x_far.at[:, pl.ds(0, d)], x.at[:, pl.ds(0, d)]),
         (x_far.at[:, pl.ds(d, half)], x.at[:, pl.ds(d, half)]),
-        (x_far.at[:, pl.ds(0, d)], x.at[:, pl.ds(0, d)]),
         (wu_far, wu),
         (wd_far, wd),
     )
@@ -138,22 +163,15 @@
         load.start()
     pairs = slots // 16
 
-    def crossed(left, right):
-        upper = (iota((1, 8, 1), 1) & 4) == 0
-        return (
-            jnp.where(upper, left, pltpu.roll(right, 4, 1)),
-            jnp.where(upper, pltpu.roll(left, 4, 1), right),
-        )
-
     loads[0].wait()
+    loads[1].wait()
+    x8 = x[:, :d]
+    gate8 = mm(x8, wg[...])
     x4 = x[:, d:].astype(f32).reshape(pairs, 2, 8, half)
     top, bottom = crossed(x4[:, 0], x4[:, 1])
     top = top.reshape(pairs * 8, half).astype(bf16)
     bottom = bottom.reshape(pairs * 8, half).astype(bf16)
     gate4 = mm(top, wg[:half, :]) + mm(bottom, wg[half:, :])
-    loads[1].wait()
-    x8 = x[:, :d]
-    gate8 = mm(x8, wg[...])
     loads[2].wait()
     hidden4 = silu_mul(gate4, mm(top, wu[:half, :]) + mm(bottom, wu[half:, :]))
     hidden8 = silu_mul(gate8, mm(x8, wu[...]))
@@ -174,12 +192,9 @@
     for step in range(early):
         send(step, mm(hidden8, wd[:, step * part : (step + 1) * part]))
     for step in range(half // part):
-        cols = slice(step * part, (step + 1) * part)
-        far = slice(half + step * part, half + (step + 1) * part)
-        left = mm(hidden4, wd[:, cols]).reshape(pairs, 8, part)
-        right = mm(hidden4, wd[:, far]).reshape(pairs, 8, part)
-        both = jnp.stack(crossed(left, right), axis=1)
-        send(early + step, both.reshape(slots, part))
+        left = mm(hidden4, wd[:, step * part : (step + 1) * part])
+        right = mm(hidden4, wd[:, half + step * part : half + (step + 1) * part])
+        send(early + step, unpacked(left, right))
     for store in stores:
         store.wait()
 
@@ -448,7 +463,8 @@
             pltpu.VMEM((2, tokens), i32),
             pltpu.VMEM((tokens, d), bf16),
             pltpu.VMEM((1, d), f32),
-            pltpu.VMEM((3, slots, tokens), bf16),
+            pltpu.VMEM((slots, tokens), bf16),
+            pltpu.VMEM((slots // 2, tokens), bf16),
             pltpu.VMEM((6, slots, d // 4), bf16),
             pltpu.SemaphoreType.DMA((3,)),
             pltpu.SemaphoreType.DMA((6,)),

time: 217 us -> 217 us (level)
  no operation moved by 1% of the time
where the time goes in v6:
time: 217 us; the launch traced here: 214 us
  waiting for transfers between devices  95.2 us (44%)
  blocking collectives  45.7 us (21%)
  starting transfers between devices  42.7 us (20%)
  Pallas kernels  21.8 us (10%)
  local copies, waits for them, and re-layouts  7.07 us (3%)
    ppermute x7, waiting for transfers between devices, shards(): lax.ppermute(plane_send, 'ep_0', [(i, i + step) for i in range(line - ste...  54.6 us
    all_to_all x2, waiting for transfers between devices, exchanged(): return lax.all_to_all(array, axes, split_axis=0, concat_axis=0, tiled=True)  38 us
    pallas_call x8, Pallas kernels, call(): pl.pallas_call(body, out_shape=out_shape, scratch_shapes=list(scratch), c...  21.8 us
    ppermute x7, starting transfers between devices, shards(): lax.ppermute(plane_send, 'ep_0', [(i, i + step) for i in range(line - ste...  20 us
    all_gather x1, blocking collectives, shards(): states = lax.all_gather(send, ('ep_1', 'ep_2'))  18.5 us
    all_to_all x2, starting transfers between devices, exchanged(): return lax.all_to_all(array, axes, split_axis=0, concat_axis=0, tiled=True)  17.7 us
    all_gather x1, blocking collectives, shards(): more = lax.all_gather(after(rest, states), ('ep_1', 'ep_2'))  14 us
    all_gather x1, blocking collectives, shards(): state = lax.all_gather(send, ('ep_1', 'ep_2'), tiled=True)  13.2 us
  transfers between devices with their start and end apart: 12, of which 5 were waited for; matrix products, arithmetic and copies ran while one was open for 0% of the time, Pallas kernels for 3%

profile of v6, /device:TPU:8, one launch (start us, length us, event | category | flops | bytes accessed | tf_op | source)
XLA Modules:
  0.0 213.5 jit_solution(5667223128528586824)
XLA Ops:
  0.6 4.2 %shard_map.176 = (bf16[512,3072]{1,0:T(8,128)(2,1)}, f32[64,192]{1,0:T(8,128)}) custom-call(s32[2,192]{1,0:T(2,128)} %bitcast.23, bf16[192,2048]{1,0:T(8,128)(2,1)} %rows_far.1, f32[1,2048]{1,0:T(1,128)} %bitcast.32), custom_call_target="tpu_custom_call" | custom-call | flops 805306368 | bytes 1610612 | tf_op jit(solution)/shard_map/pallas_call | solution.py:49
  4.9 12.3 %all-to-all-start = ((bf16[64,8,3072]{2,1,0:T(8,128)(2,1)}), bf16[64,8,3072]{2,1,0:T(8,128)(2,1)}, u32[]{:S(2)}, u32[]{:S(2)}) async-start(bf16[64,8,3072]{2,1,0:T(8,128)(2,1)} %bitcast.29), calls=%async_computation | async-start | bytes 6291456 | tf_op jit(solution)/shard_map/all_to_all | solution.py:412
  17.9 18.5 %all-gather = bf16[1088,256]{1,0:T(8,128)(2,1)S(1)} all-gather(bf16[136,256]{1,0:T(8,128)(2,1)S(1)} %get-tuple-element.16), channel_id=2, replica_groups=mesh['ep_0'=8,'ep_1'=4,'ep_2'=2,'tp'=4] {'ep_1','ep_2'}, dimensions={0}, use_global_device_ids=true | all-gather | bytes 626688 | tf_op jit(solution)/shard_map/all_gather | solution.py:485
  36.5 14.0 %all-gather.1 = bf16[1024,256]{1,0:T(8,128)(2,1)S(1)} all-gather(bf16[128,256]{1,0:T(8,128)(2,1)S(1)} %get-tuple-element.18), channel_id=3, replica_groups=mesh['ep_0'=8,'ep_1'=4,'ep_2'=2,'tp'=4] {'ep_1','ep_2'}, dimensions={0}, use_global_device_ids=true | all-gather | bytes 589824 | tf_op jit(solution)/shard_map/all_gather | solution.py:486
  50.5 1.7 shard_map.178
  52.9 38.0 %all-to-all-done = bf16[64,8,3072]{2,1,0:T(8,128)(2,1)} async-done(((bf16[64,8,3072]{2,1,0:T(8,128)(2,1)}), bf16[64,8,3072]{2,1,0:T(8,128)(2,1)}, u32[]{:S(2)}, u32[]{:S(2)}) %all-to-all-start) | async-done | bytes 3145760 | tf_op jit(solution)/shard_map/all_to_all | solution.py:412
  90.9 8.4 %shard_map.182 = bf16[512,3072]{1,0:T(8,128)(2,1)} custom-call(bf16[512,3072]{1,0:T(8,128)(2,1)} %bitcast.12.x_far, bf16[2048,512]{1,0:T(8,128)(2,1)S(1)} %bitcast.21, bf16[2048,512]{1,0:T(8,128)(2,1)} %bitcast.30, bf16[512,2048]{1,0:T(8,128)(2,1)} %bitcast.31), custom_call_target="tpu_custom_call" | custom-call | flops 6442450944 | bytes 12884901 | tf_op jit(solution)/shard_map/pallas_call | solution.py:49
  99.4 5.4 %all-to-all-start.1 = ((bf16[64,8,3072]{2,1,0:T(8,128)(2,1)}), bf16[64,8,3072]{2,1,0:T(8,128)(2,1)S(1)}, u32[]{:S(2)}, u32[]{:S(2)}) async-start(bf16[64,8,3072]{2,1,0:T(8,128)(2,1)} %bitcast.28), calls=%async_computation.1 | async-start | bytes 6291456 | tf_op jit(solution)/shard_map/all_to_all | solution.py:412
  104.8 5.0 %collective-permute-start.6 = (bf16[40,256]{1,0:T(8,128)(2,1)}, bf16[40,256]{1,0:T(8,128)(2,1)S(1)}, u32[]{:S(2)}, u32[]{:S(2)}) collective-permute-start(bf16[40,256]{1,0:T(8,128)(2,1)} %get-tuple-element.19), channel_id=1, source_target_pairs={{0,224},{1,225},{2,226},{3,227},{4,228},{5,229},{6,230},{7,231},{8... | collective-permute-start | bytes 61448 | tf_op jit(solution)/shard_map/ppermute | solution.py:502
  109.8 1.5 collective-permute-start.5
  111.3 1.5 collective-permute-start.4
  112.8 1.5 collective-permute-start.3
  114.3 4.5 %collective-permute-start.2 = (bf16[40,256]{1,0:T(8,128)(2,1)}, bf16[40,256]{1,0:T(8,128)(2,1)S(1)}, u32[]{:S(2)}, u32[]{:S(2)}) collective-permute-start(bf16[40,256]{1,0:T(8,128)(2,1)} %get-tuple-element.19), channel_id=1, source_target_pairs={{0,96},{32,128},{64,160},{96,192},{128,224},{1,97},{33,129},{65,16... | collective-permute-start | bytes 61448 | tf_op jit(solution)/shard_map/ppermute | solution.py:502
  118.8 53.0 %collective-permute-done.6.refs_6_ = bf16[40,256]{1,0:T(8,128)(2,1)S(1)} collective-permute-done((bf16[40,256]{1,0:T(8,128)(2,1)}, bf16[40,256]{1,0:T(8,128)(2,1)S(1)}, u32[]{:S(2)}, u32[]{:S(2)}) %collective-permute-start.6) | collective-permute-done | bytes 20512 | tf_op jit(solution)/shard_map/ppermute | solution.py:502
  171.8 1.3 collective-permute-start.1
  173.1 4.7 %collective-permute-start = (bf16[40,256]{1,0:T(8,128)(2,1)}, bf16[40,256]{1,0:T(8,128)(2,1)S(1)}, u32[]{:S(2)}, u32[]{:S(2)}) collective-permute-start(bf16[40,256]{1,0:T(8,128)(2,1)} %get-tuple-element.19), channel_id=1, source_target_pairs={{0,32},{32,64},{64,96},{96,128},{128,160},{160,192},{192,224},{1,3... | collective-permute-start | bytes 61448 | tf_op jit(solution)/shard_map/ppermute | solution.py:502
  177.9 1.6 collective-permute-done.refs_0_
  180.3 13.2 %all_gather.19.state = bf16[256,256]{1,0:T(8,128)(2,1)S(1)} all-gather(bf16[32,256]{1,0:T(8,128)(2,1)S(1)} %get-tuple-element.20), channel_id=1, replica_groups=mesh['ep_0'=8,'ep_1'=4,'ep_2'=2,'tp'=4] {'ep_1','ep_2'}, dimensions={0}, use_global_device_ids=true | all-gather | bytes 147456 | tf_op jit(solution)/shard_map/all_gather | solution.py:534
  199.8 1.7 shard_map.180
  202.1 2.6 %collective-permute-start.8 = (bf16[128,256]{1,0:T(8,128)(2,1)S(1)}, bf16[128,256]{1,0:T(8,128)(2,1)S(1)}, u32[]{:S(2)}, u32[]{:S(2)}) collective-permute-start(bf16[128,256]{1,0:T(8,128)(2,1)S(1)} %get-tuple-element.27), channel_id=1, source_target_pairs={{0,2},{1,3},{2,0},{3,1},{4,6},{5,7},{6,4},{7,5},{8,10},{9,11},{10,... | collective-permute-start | bytes 196616 | tf_op jit(solution)/shard_map/ppermute | solution.py:559
  204.7 1.9 collective-permute-start.7
  206.6 1.8 collective-permute-done.8.refs_2_
  209.2 2.3 %shard_map.181 = bf16[128,2048]{1,0:T(8,128)(2,1)} custom-call(s32[3]{0:T(128)S(1)} %pad_add_fusion.where, bf16[128,256]{1,0:T(8,128)(2,1)S(1)} %get-tuple-element.29.refs_0_, bf16[128,256]{1,0:T(8,128)(2,1)S(1)} %collective-permute-done.7.refs_1_, bf16[128,256]{1,0:T(8,128)(2,1)S(1)} %collective-permute-done.8.refs_2_, ...), custom_call_target="tpu_custom_call" | custom-call | flops 5368709120 | bytes 10737418 | tf_op jit(solution)/shard_map/pallas_call | solution.py:49
  211.5 2.0 shard_map.183
  (59 shorter events, 9.9 us)
Async XLA Ops:
  4.8 12.4 %copy-start.3 = (bf16[512,256]{1,0:T(8,128)(2,1)S(1)}, bf16[512,256]{1,0:T(8,128)(2,1)}, u32[]{:S(2)}) copy-start(bf16[512,256]{1,0:T(8,128)(2,1)} %keys.2) | copy-start | bytes 786436
  4.8 12.4 %copy-start.5 = (bf16[512,256]{1,0:T(8,128)(2,1)S(1)}, bf16[512,256]{1,0:T(8,128)(2,1)}, u32[]{:S(2)}) copy-start(bf16[512,256]{1,0:T(8,128)(2,1)} %values.3) | copy-start | bytes 786436
  4.8 12.4 %copy-start.12 = (f32[1,512]{1,0:T(1,128)S(1)}, f32[1,512]{1,0:T(1,128)}, u32[]{:S(2)}) copy-start(f32[1,512]{1,0:T(1,128)} %gates.3) | copy-start | bytes 6148
  4.9 12.4 %copy-start.14 = (f32[1,512]{1,0:T(1,128)S(1)}, f32[1,512]{1,0:T(1,128)}, u32[]{:S(2)}) copy-start(f32[1,512]{1,0:T(1,128)} %forget.3) | copy-start | bytes 6148
  4.9 12.4 %copy-start.16 = (f32[1,512]{1,0:T(1,128)S(1)}, f32[1,512]{1,0:T(1,128)}, u32[]{:S(2)}) copy-start(f32[1,512]{1,0:T(1,128)} %boosts.3) | copy-start | bytes 6148
  4.9 86.1 %all-to-all-start = ((bf16[64,8,3072]{2,1,0:T(8,128)(2,1)}), bf16[64,8,3072]{2,1,0:T(8,128)(2,1)}, u32[]{:S(2)}, u32[]{:S(2)}) async-start(bf16[64,8,3072]{2,1,0:T(8,128)(2,1)} %bitcast.29), calls=%async_computation | async-start | bytes 6291456 | tf_op jit(solution)/shard_map/all_to_all | solution.py:412
  17.2 73.7 %copy-start.1 = (bf16[1,2048,512]{2,1,0:T(8,128)(2,1)S(1)}, bf16[1,2048,512]{2,1,0:T(8,128)(2,1)}, u32[]{:S(2)}) copy-start(bf16[1,2048,512]{2,1,0:T(8,128)(2,1)} %param.31) | copy-start | bytes 6291460
  52.9 46.4 %copy-start.10 = (f32[8,256]{1,0:T(8,128)}, f32[8,256]{1,0:T(8,128)S(1)}, u32[]{:S(2)}) copy-start(f32[8,256]{1,0:T(8,128)S(1)} %get-tuple-element.23.near) | copy-start | bytes 24580
  99.4 94.2 %copy-start.2 = (bf16[512,256]{1,0:T(8,128)(2,1)S(1)}, bf16[512,256]{1,0:T(8,128)(2,1)}, u32[]{:S(2)}) copy-start(bf16[512,256]{1,0:T(8,128)(2,1)} %query.1) | copy-start | bytes 786436
  99.4 112.1 %all-to-all-start.1 = ((bf16[64,8,3072]{2,1,0:T(8,128)(2,1)}), bf16[64,8,3072]{2,1,0:T(8,128)(2,1)S(1)}, u32[]{:S(2)}, u32[]{:S(2)}) async-start(bf16[64,8,3072]{2,1,0:T(8,128)(2,1)} %bitcast.28), calls=%async_computation.1 | async-start | bytes 6291456 | tf_op jit(solution)/shard_map/all_to_all | solution.py:412
  104.8 67.0 %collective-permute-start.6 = (bf16[40,256]{1,0:T(8,128)(2,1)}, bf16[40,256]{1,0:T(8,128)(2,1)S(1)}, u32[]{:S(2)}, u32[]{:S(2)}) collective-permute-start(bf16[40,256]{1,0:T(8,128)(2,1)} %get-tuple-element.19), channel_id=1, source_target_pairs={{0,224},{1,225},{2,226},{3,227},{4,228},{5,229},{6,230},{7,231},{8... | collective-permute-start | bytes 61448 | tf_op jit(solution)/shard_map/ppermute | solution.py:502
  109.8 63.3 %collective-permute-start.5 = (bf16[40,256]{1,0:T(8,128)(2,1)}, bf16[40,256]{1,0:T(8,128)(2,1)S(1)}, u32[]{:S(2)}, u32[]{:S(2)}) collective-permute-start(bf16[40,256]{1,0:T(8,128)(2,1)} %get-tuple-element.19), channel_id=1, source_target_pairs={{0,192},{32,224},{1,193},{33,225},{2,194},{34,226},{3,195},{35,227... | collective-permute-start | bytes 61448 | tf_op jit(solution)/shard_map/ppermute | solution.py:502
  111.3 66.5 %collective-permute-start.4 = (bf16[40,256]{1,0:T(8,128)(2,1)}, bf16[40,256]{1,0:T(8,128)(2,1)S(1)}, u32[]{:S(2)}, u32[]{:S(2)}) collective-permute-start(bf16[40,256]{1,0:T(8,128)(2,1)} %get-tuple-element.19), channel_id=1, source_target_pairs={{0,160},{32,192},{64,224},{1,161},{33,193},{65,225},{2,162},{34,19... | collective-permute-start | bytes 61448 | tf_op jit(solution)/shard_map/ppermute | solution.py:502
  112.8 65.0 %collective-permute-start.3 = (bf16[40,256]{1,0:T(8,128)(2,1)}, bf16[40,256]{1,0:T(8,128)(2,1)S(1)}, u32[]{:S(2)}, u32[]{:S(2)}) collective-permute-start(bf16[40,256]{1,0:T(8,128)(2,1)} %get-tuple-element.19), channel_id=1, source_target_pairs={{0,128},{32,160},{64,192},{96,224},{1,129},{33,161},{65,193},{97,2... | collective-permute-start | bytes 61448 | tf_op jit(solution)/shard_map/ppermute | solution.py:502
  114.3 63.5 %collective-permute-start.2 = (bf16[40,256]{1,0:T(8,128)(2,1)}, bf16[40,256]{1,0:T(8,128)(2,1)S(1)}, u32[]{:S(2)}, u32[]{:S(2)}) collective-permute-start(bf16[40,256]{1,0:T(8,128)(2,1)} %get-tuple-element.19), channel_id=1, source_target_pairs={{0,96},{32,128},{64,160},{96,192},{128,224},{1,97},{33,129},{65,16... | collective-permute-start | bytes 61448 | tf_op jit(solution)/shard_map/ppermute | solution.py:502
  171.8 6.1 %collective-permute-start.1 = (bf16[40,256]{1,0:T(8,128)(2,1)}, bf16[40,256]{1,0:T(8,128)(2,1)S(1)}, u32[]{:S(2)}, u32[]{:S(2)}) collective-permute-start(bf16[40,256]{1,0:T(8,128)(2,1)} %get-tuple-element.19), channel_id=1, source_target_pairs={{0,64},{32,96},{64,128},{96,160},{128,192},{160,224},{1,65},{33,97... | collective-permute-start | bytes 61448 | tf_op jit(solution)/shard_map/ppermute | solution.py:502
  173.1 6.4 %collective-permute-start = (bf16[40,256]{1,0:T(8,128)(2,1)}, bf16[40,256]{1,0:T(8,128)(2,1)S(1)}, u32[]{:S(2)}, u32[]{:S(2)}) collective-permute-start(bf16[40,256]{1,0:T(8,128)(2,1)} %get-tuple-element.19), channel_id=1, source_target_pairs={{0,32},{32,64},{64,96},{96,128},{128,160},{160,192},{192,224},{1,3... | collective-permute-start | bytes 61448 | tf_op jit(solution)/shard_map/ppermute | solution.py:502
  199.8 9.4 %copy-start = (bf16[1024,2048]{1,0:T(8,128)(2,1)S(1)}, bf16[1024,2048]{1,0:T(8,128)(2,1)}, u32[]{:S(2)}) copy-start(bf16[1024,2048]{1,0:T(8,128)(2,1)} %refs_4_.1) | copy-start | bytes 12582916
  199.8 9.4 %copy-start.9 = (f32[2048]{0:T(1024)S(1)}, f32[2048]{0:T(1024)}, u32[]{:S(2)}) copy-start(f32[2048]{0:T(1024)} %param.25) | copy-start | bytes 24580
  201.6 5.0 %collective-permute-start.9 = (bf16[128,256]{1,0:T(8,128)(2,1)S(1)}, bf16[128,256]{1,0:T(8,128)(2,1)S(1)}, u32[]{:S(2)}, u32[]{:S(2)}) collective-permute-start(bf16[128,256]{1,0:T(8,128)(2,1)S(1)} %get-tuple-element.26), channel_id=1, source_target_pairs={{0,3},{1,0},{2,1},{3,2},{4,7},{5,4},{6,5},{7,6},{8,11},{9,8},{10,9... | collective-permute-start | bytes 196616 | tf_op jit(solution)/shard_map/ppermute | solution.py:559
  202.1 6.3 %collective-permute-start.8 = (bf16[128,256]{1,0:T(8,128)(2,1)S(1)}, bf16[128,256]{1,0:T(8,128)(2,1)S(1)}, u32[]{:S(2)}, u32[]{:S(2)}) collective-permute-start(bf16[128,256]{1,0:T(8,128)(2,1)S(1)} %get-tuple-element.27), channel_id=1, source_target_pairs={{0,2},{1,3},{2,0},{3,1},{4,6},{5,7},{6,4},{7,5},{8,10},{9,11},{10,... | collective-permute-start | bytes 196616 | tf_op jit(solution)/shard_map/ppermute | solution.py:559
  204.7 4.5 %collective-permute-start.7 = (bf16[128,256]{1,0:T(8,128)(2,1)S(1)}, bf16[128,256]{1,0:T(8,128)(2,1)S(1)}, u32[]{:S(2)}, u32[]{:S(2)}) collective-permute-start(bf16[128,256]{1,0:T(8,128)(2,1)S(1)} %get-tuple-element.28), channel_id=1, source_target_pairs={{0,1},{1,2},{2,3},{3,0},{4,5},{5,6},{6,7},{7,4},{8,9},{9,10},{10,1... | collective-permute-start | bytes 196616 | tf_op jit(solution)/shard_map/ppermute | solution.py:559
  209.2 2.3 %copy-start.18 = (s32[192,2]{0,1:T(2,128)S(1)}, s32[192,2]{0,1:T(2,128)}, u32[]{:S(2)}) copy-start(s32[192,2]{0,1:T(2,128)} %param.28) | copy-start | bytes 4612
  209.2 2.3 %copy-start.19 = (f32[192,2]{0,1:T(2,128)S(1)}, f32[192,2]{0,1:T(2,128)}, u32[]{:S(2)}) copy-start(f32[192,2]{0,1:T(2,128)} %param.30) | copy-start | bytes 4612
  (11 other events, 11.6 us)
